TPU v7x, 32 devices: a whole 2x2x4 slice. The times are simulated.
32 devices in a mesh: sp: 8 (over z, y), tp: 4 (over x, core).
Axes of the slice: x: 2, y: 2, z: 4, core: 2. Of those that a mesh axis runs over, the one named last changes fastest.
Arguments:
- latent: bfloat16 [2048, 2048], P('sp'), may hold values from -6 to 6
- context: bfloat16 [1024, 2048], P('sp'), may hold values from -6 to 6
- condition: bfloat16 [2048], replicated, may hold values from -6 to 6
- context_condition: bfloat16 [2048], replicated, may hold values from -6 to 6
- gain_pre: float32 [2048], replicated, may hold values from 0.1 to 1.9
- gain_post: float32 [2048], replicated, may hold values from 0.1 to 1.9
- w_shift: bfloat16 [2048, 2048], P('sp', 'tp'), may hold values from -0.125 to 0.125
- w_scale: bfloat16 [2048, 2048], P('sp', 'tp'), may hold values from -0.125 to 0.125
- w_gate: bfloat16 [2048, 2048], P('sp', 'tp'), may hold values from -0.125 to 0.125
- w_query: bfloat16 [2048, 2048], P(None, 'tp'), may hold values from -0.13258252 to 0.13258252
- w_key: bfloat16 [2048, 2048], P(None, 'tp'), may hold values from -6.629126 to 6.629126
- w_value: bfloat16 [2048, 2048], P(None, 'tp'), may hold values from -0.125 to 0.125
- w_silu: bfloat16 [2048, 2048], P(None, 'tp'), may hold values from -0.125 to 0.125
- offset_bias: float32 [32, 15, 31], P('tp'), may hold values from 1.5 to 3.5
- w_out: bfloat16 [2048, 2048], P('tp'), may hold values from -0.125 to 0.125
Outputs:
- updated: bfloat16 [2048, 2048], P(('sp', 'tp'))
All inputs are finite; a program needn't handle non-finite values.
Results may differ from a plain program's by a relative error of at most 0.01.
Values may be sent and summed in bfloat16 or wider, within the bound.
No kernel may reach another device: no remote copies, remote signals or barrier semaphores. Data moves between devices by JAX's collectives and lax.ppermute only.
A program may use at most 64 MiB of HBM per device.

v0:
```python
import jax
import jax.numpy as jnp
import numpy as np
from jax import lax
from jax.sharding import PartitionSpec as P

GRID_W = 64
WIN_ROWS = 8
WIN_COLS = 16


EPSILON = 1e-06


def extended_2(cells, sides, width):
    for axis, dim in sides:
        count = lax.axis_size(axis)
        ends = count - 1
        head = lax.slice_in_dim(cells, 0, width, axis=dim)
        tail = lax.slice_in_dim(cells, cells.shape[dim] - width, cells.shape[dim], axis=dim)
        cells = jnp.concatenate(
            [
                lax.ppermute(tail, axis, [(i, (i + 1) % count) for i in range(ends)]),
                cells,
                lax.ppermute(head, axis, [((i + 1) % count, i) for i in range(ends)]),
            ],
            axis=dim,
        )
    return cells


def normalize(row_block, gain_row):
    values = row_block.astype(jnp.float32)
    return (
        values * lax.rsqrt(jnp.mean(values * values, axis=-1, keepdims=True) + EPSILON) * gain_row
    )


def modulate(row_block, gain_row, shift_row, scale_row):
    return (normalize(row_block, gain_row) * (1.0 + scale_row) + shift_row).astype(jnp.bfloat16)


def product(left, right):
    return jnp.dot(left, right, preferred_element_type=jnp.float32)


def shards(
    latent,
    context,
    condition,
    context_condition,
    gain_pre,
    gain_post,
    w_shift,
    w_scale,
    w_gate,
    w_query,
    w_key,
    w_value,
    w_silu,
    offset_bias,
    w_out,
):
    sp_index = lax.axis_index("sp")
    tp_index = lax.axis_index("tp")
    in_rows, local_cols = w_shift.shape
    tokens, model_width = latent.shape
    active = jax.nn.silu(jnp.stack([condition, context_condition]).astype(jnp.float32)).astype(
        jnp.bfloat16
    )
    own_active = lax.dynamic_slice_in_dim(active, sp_index * in_rows, in_rows, 1)
    stacked = jnp.stack([w_shift, w_scale, w_gate])
    partial_value = jnp.einsum(
        "ai,mij->maj", own_active, stacked, preferred_element_type=jnp.float32
    )
    summed = lax.psum(partial_value, "sp")
    modulation = lax.all_gather(summed, "tp", axis=2, tiled=True)
    shifts, scales, gating = (modulation[0], modulation[1], modulation[2])
    normed = modulate(context, gain_pre, shifts[1], scales[1])
    context_kv = lax.all_gather(
        jnp.concatenate([product(normed, w_key), product(normed, w_value)], axis=1).astype(
            jnp.bfloat16
        ),
        "sp",
        axis=0,
        tiled=True,
    )
    hidden = modulate(latent, gain_pre, shifts[0], scales[0])
    queries = product(hidden, w_query).astype(jnp.bfloat16)
    keys_latent = product(hidden, w_key).astype(jnp.bfloat16)
    values_latent = product(hidden, w_value).astype(jnp.bfloat16)
    silu_gate = product(hidden, w_silu).astype(jnp.bfloat16)
    head_count = offset_bias.shape[0]
    head_width = local_cols // head_count
    grid_rows = tokens // GRID_W
    kv_grid = jnp.concatenate([keys_latent, values_latent], axis=1).reshape(
        grid_rows, GRID_W, 2 * local_cols
    )
    extended = extended_2(kv_grid, (("sp", 0),), WIN_ROWS // 2)
    blocks = GRID_W // WIN_COLS
    key_span = 2 * WIN_COLS
    block_start = np.clip(np.arange(blocks) * WIN_COLS - WIN_COLS // 2, 0, GRID_W - key_span)
    query_col = np.arange(blocks)[:, None] * WIN_COLS + np.arange(WIN_COLS)[None, :]
    key_col = block_start[:, None] + np.arange(key_span)[None, :]
    window_start = np.clip(query_col - WIN_COLS // 2, 0, GRID_W - WIN_COLS)
    inside_cols = (key_col[:, None, :] >= window_start[:, :, None]) & (
        key_col[:, None, :] < window_start[:, :, None] + WIN_COLS
    )
    inside_window = np.broadcast_to(
        inside_cols[:, :, None, :], (blocks, WIN_COLS, WIN_ROWS, key_span)
    ).reshape(blocks, WIN_COLS, WIN_ROWS * key_span)[None, :, None, :, :]
    col_offset = np.clip(
        key_col[:, None, :] - query_col[:, :, None] + WIN_COLS - 1, 0, 2 * WIN_COLS - 2
    )
    col_table = (col_offset[..., None] == np.arange(2 * WIN_COLS - 1)).astype(np.float32)
    total_rows = grid_rows * lax.axis_size("sp")
    local_rows = jnp.arange(grid_rows, dtype=jnp.int32)
    global_row = sp_index * grid_rows + local_rows
    row_start = jnp.clip(global_row - WIN_ROWS // 2, 0, total_rows - WIN_ROWS)
    band_first = row_start - sp_index * grid_rows + WIN_ROWS // 2
    row_offset = (
        row_start[:, None]
        + jnp.arange(WIN_ROWS, dtype=jnp.int32)[None, :]
        - global_row[:, None]
        + WIN_ROWS
        - 1
    )
    row_table = (row_offset[..., None] == jnp.arange(2 * WIN_ROWS - 1, dtype=jnp.int32)).astype(
        jnp.float32
    )
    position = (
        band_first[:, None, None, None] + jnp.arange(WIN_ROWS, dtype=jnp.int32)[None, None, :, None]
    ) * GRID_W + jnp.asarray(key_col, jnp.int32)[None, :, None, :]
    flat_rows = extended.reshape(-1, 2 * local_cols)
    window_kv = jnp.take(flat_rows, position.reshape(-1), axis=0).reshape(
        grid_rows, blocks, WIN_ROWS * key_span, 2 * local_cols
    )
    window_keys = window_kv[..., :local_cols].reshape(
        grid_rows, blocks, WIN_ROWS * key_span, head_count, head_width
    )
    window_values = window_kv[..., local_cols:].reshape(
        grid_rows, blocks, WIN_ROWS * key_span, head_count, head_width
    )
    context_keys = context_kv[:, :local_cols].reshape(-1, head_count, head_width)
    context_values = context_kv[:, local_cols:].reshape(-1, head_count, head_width)
    query_blocks = queries.reshape(grid_rows, blocks, WIN_COLS, head_count, head_width)
    score_scale = head_width ** (-0.5)
    by_column = jnp.einsum(
        "hae,bqwe->hbqwa", offset_bias, jnp.asarray(col_table), precision=lax.Precision.HIGHEST
    )
    offset_terms = jnp.einsum(
        "rva,hbqwa->rbhqvw", row_table, by_column, precision=lax.Precision.HIGHEST
    ).reshape(grid_rows, blocks, head_count, WIN_COLS, WIN_ROWS * key_span)
    window_scores = (
        jnp.einsum(
            "rbqhd,rbkhd->rbhqk", query_blocks, window_keys, preferred_element_type=jnp.float32
        )
        * score_scale
    )
    window_scores = jnp.where(inside_window, window_scores + offset_terms, -jnp.inf)
    context_scores = (
        jnp.einsum(
            "rbqhd,khd->rbhqk", query_blocks, context_keys, preferred_element_type=jnp.float32
        )
        * score_scale
    )
    maximum = jnp.maximum(jnp.max(window_scores, axis=-1), jnp.max(context_scores, axis=-1))[
        ..., None
    ]
    window_exp = jnp.exp(window_scores - maximum)
    context_exp = jnp.exp(context_scores - maximum)
    denominator = jnp.sum(window_exp, axis=-1, keepdims=True) + jnp.sum(
        context_exp, axis=-1, keepdims=True
    )
    window_weights = (window_exp / denominator).astype(jnp.bfloat16)
    context_weights = (context_exp / denominator).astype(jnp.bfloat16)
    attended = jnp.einsum(
        "rbhqk,rbkhd->rbqhd", window_weights, window_values, preferred_element_type=jnp.float32
    )
    attended = attended + jnp.einsum(
        "rbhqk,khd->rbqhd", context_weights, context_values, preferred_element_type=jnp.float32
    )
    attended = attended.reshape(tokens, local_cols)
    gated_heads = (jax.nn.silu(silu_gate.astype(jnp.float32)) * attended).astype(jnp.bfloat16)
    out_rows = tokens // lax.axis_size("tp")
    branch = lax.psum_scatter(
        product(gated_heads, w_out).astype(jnp.bfloat16), "tp", scatter_dimension=0, tiled=True
    )
    own_rows = lax.dynamic_slice_in_dim(latent, tp_index * out_rows, out_rows, 0)
    updated = own_rows.astype(jnp.float32) + gating[0] * normalize(branch, gain_post)
    return updated.astype(jnp.bfloat16)


def solution(mesh):
    in_specs = (
        P("sp", None),
        P("sp", None),
        P(),
        P(),
        P(),
        P(),
        P("sp", "tp"),
        P("sp", "tp"),
        P("sp", "tp"),
        P(None, "tp"),
        P(None, "tp"),
        P(None, "tp"),
        P(None, "tp"),
        P("tp", None, None),
        P("tp", None),
    )
    out_specs = P(("sp", "tp"), None)
    return jax.shard_map(shards, mesh=mesh, in_specs=in_specs, out_specs=out_specs, check_vma=False)
```

profile of v0, /device:TPU:0, one launch (start us, length us, event | category | flops | bytes accessed | tf_op | source)
XLA Modules:
  0.0 194.9 jit_solution(9264720837811773831)
XLA Ops:
  6.6 1.7 fusion.9
  11.0 38.9 %psum.7 = f32[3,2,512]{2,1,0:T(2,128)S(1)} all-reduce(f32[3,2,512]{2,1,0:T(2,128)S(1)} %convolution_bitcast_fusion.1), channel_id=1, replica_groups=mesh['sp'=8,'tp'=4] {'sp'}, use_global_device_ids=true, to_apply=%region_0.1 | all-reduce | flops 3072 | bytes 24576 | tf_op jit(solution)/shard_map/psum | solution.py:76
  49.9 5.2 %all_gather.6 = f32[3,2,2048]{2,1,0:T(2,128)S(1)} all-gather(f32[3,2,512]{2,1,0:T(2,128)S(1)} %psum.7), channel_id=1, replica_groups=mesh['sp'=8,'tp'=4] {'tp'}, dimensions={2}, use_global_device_ids=true | all-gather | bytes 61440 | tf_op jit(solution)/shard_map/all_gather | solution.py:77
  55.1 2.5 %convolution_convert_fusion.3 = bf16[256,512]{1,0:T(8,128)(2,1)S(1)} fusion(bf16[2048,512]{1,0:T(8,128)(2,1)} %param.28, bf16[256,2048]{1,0:T(8,128)(2,1)S(1)} %copy-done.4, f32[2048]{0:T(1024)S(1)} %bitcast.96, f32[2048]{0:T(1024)S(1)} %bitcast.100, f32[2048]{0:T(1024)S(1)} %copy-done.15, f32[256]{0:T(256)S(1)} %add_rsqrt_fusion), kind=kOutput, calls=%fused_computation.33 | convolution fusion | flops 540147712 | bytes 3433472 | tf_op jit(solution)/shard_map/dot_general | solution.py:44
  59.9 5.4 %collective-permute-start = (bf16[4,64,1024]{2,1,0:T(8,128)(2,1)S(1)}, bf16[4,64,1024]{2,1,0:T(8,128)(2,1)}, u32[]{:S(2)}, u32[]{:S(2)}) collective-permute-start(bf16[4,64,1024]{2,1,0:T(8,128)(2,1)S(1)} %bitcast.90), channel_id=1, source_target_pairs={{0,4},{4,8},{8,12},{12,16},{16,20},{20,24},{24,28},{1,5},{5,9},{9,... | collective-permute-start | bytes 1572872 | tf_op jit(solution)/shard_map/ppermute | solution.py:23
  67.7 6.2 %fusion.42 = f32[4,16,32,8,15]{2,4,1,0,3:T(8,128)S(1)} fusion(f32[4,16,32,31,1]{3,2,1,0,4:T(8,128)} %constant.79, f32[8,15,31,1,1]{2,0,1,4,3:T(8,128)S(1)} %bitcast.93), kind=kOutput, calls=%fused_computation.66 | convolution fusion | flops 91422720 | bytes 1251872 | tf_op jit(solution)/shard_map/hae,bqwe->hbqwa/dot_general | solution.py:148
  73.9 5.8 %fusion.6 = f32[4,4,8,16,8,32]{5,4,0,3,1,2:T(8,128)} fusion(f32[4,16,32,8,15]{2,4,1,0,3:T(8,128)S(1)} %fusion.42, s32[4,8]{1,0:T(4,128)S(1)} %subtract_add_fusion), kind=kOutput, calls=%fused_computation.11 | convolution fusion | flops 94372320 | bytes 3080320 | tf_op jit(solution)/shard_map/rva,hbqwa->rbhqvw/dot_general | solution.py:151
  81.0 7.4 %reshape.240 = f32[4,4,8,16,256]{4,0,3,1,2:T(4,128)} reshape(f32[4,4,8,16,8,32]{5,4,0,3,1,2:T(8,128)} %fusion.6) | data formatting | bytes 4194304 | tf_op jit(solution)/shard_map/reshape | solution.py:153
  88.4 2.6 %pad_maximum_fusion = bf16[12,64,1024]{2,1,0:T(8,128)(2,1)} fusion(bf16[4,64,1024]{2,1,0:T(8,128)(2,1)} %collective-permute-done.1, bf16[4,64,1024]{2,1,0:T(8,128)(2,1)S(1)} %bitcast.91, bf16[4,64,1024]{2,1,0:T(8,128)(2,1)} %collective-permute-done), kind=kLoop, calls=%fused_computation.25 | loop fusion | flops 1572864 | bytes 3145728 | tf_op jit(solution)/shard_map/concatenate | solution.py:21
  91.0 22.5 %gather_fusion = bf16[4096,1024]{1,0:T(8,128)(2,1)} fusion(bf16[768,1024]{1,0:T(8,128)(2,1)} %bitcast.84, s32[4096]{0:T(1024)S(1)} %broadcast_clamp_fusion), kind=kCustom, calls=%fused_computation | custom fusion | bytes 16793600 | tf_op jit(solution)/shard_map/jit(_take)/gather | solution.py:135
  113.6 11.4 %copy.50 = bf16[4,4,256,1024]{2,3,1,0:T(8,128)(2,1)} copy(bf16[4,4,256,1024]{3,2,1,0:T(8,128)(2,1)} %bitcast.85) | data formatting | bytes 16777216 | tf_op jit(solution)/shard_map/jit(_take)/gather | solution.py:135
  124.9 7.4 %broadcast_select_fusion = bf16[4,4,256,1024]{2,3,1,0:T(8,128)(2,1)} fusion(bf16[4,4,256,1024]{2,3,1,0:T(8,128)(2,1)} %copy.50, pred[4,4,256]{2,1,0:T(4,128)(4,1)S(1)} %fusion.46), kind=kLoop, calls=%fused_computation.5 | loop fusion | flops 4194304 | bytes 16781312 | tf_op jit(solution)/shard_map/jit(_take)/select_n | solution.py:135
  132.3 5.2 %fusion.64 = (bf16[4,4,256,512]{2,3,1,0:T(8,128)(2,1)}, bf16[4,4,256,512]{2,3,1,0:T(8,128)(2,1)S(1)}) fusion(bf16[4,4,256,1024]{2,3,1,0:T(8,128)(2,1)} %broadcast_select_fusion), kind=kLoop, calls=%fused_computation.97 | loop fusion | bytes 16777216 | tf_op jit(solution)/shard_map/slice | solution.py:141
  137.6 2.2 %fusion.67 = (f32[4,4,8,16]{3,2,1,0:T(8,128)S(1)}, f32[4,4,8,16,256]{4,3,2,1,0:T(8,128)}) fusion(f32[4,4,8,16,256]{4,0,3,1,2:T(4,128)S(1)} %copy-done.1, bf16[4,4,256,8,64]{2,4,3,1,0:T(8,128)(2,1)S(1)} %bitcast.86, bf16[4,4,16,8,64]{4,3,2,1,0:T(8,128)(2,1)S(1)} %reshape.219, pred[4,16,256]{2,1,0:T(8,128)(4,1)S(1)} %copy-done.8), kind=kOutput, calls=%fused_computation.100 | convolution fusion | flops 69203968 | bytes 8675328 | tf_op jit(solution)/shard_map/rbqhd,rbkhd->rbhqk/dot_general | solution.py:155
  139.8 3.0 %fusion.65 = (bf16[1024,512]{1,0:T(8,128)(2,1)}, bf16[1024,512]{1,0:T(8,128)(2,1)}) fusion(bf16[1024,1024]{1,0:T(8,128)(2,1)} %all-gather.2.cloned.1.call-done), kind=kLoop, calls=%fused_computation.98 | loop fusion | bytes 4194304 | tf_op jit(solution)/shard_map/slice | solution.py:144
  142.8 2.3 %copy.54 = bf16[1024,512]{0,1:T(8,128)(2,1)} copy(bf16[1024,512]{1,0:T(8,128)(2,1)} %get-tuple-element.7) | data formatting | bytes 2097152 | tf_op jit(solution)/shard_map/slice | solution.py:144
  145.1 2.3 %copy.59 = bf16[1024,512]{0,1:T(8,128)(2,1)} copy(bf16[1024,512]{1,0:T(8,128)(2,1)} %get-tuple-element.8) | data formatting | bytes 2097152 | tf_op jit(solution)/shard_map/slice | solution.py:145
  147.4 2.7 %bitcast_reduce_fusion = (f32[4,4,8,16]{3,1,0,2:T(4,128)S(1)}, f32[8,1024,4,4,16]{1,4,3,2,0:T(8,128)S(1)}) fusion(bf16[1024,8,64,1,1]{0,2,4,3,1:T(8,128)(2,1)} %bitcast.87, bf16[4,4,16,8,64]{4,3,2,1,0:T(8,128)(2,1)S(1)} %reshape.219), kind=kOutput, calls=%fused_computation.2 | convolution fusion | flops 272627712 | bytes 9707520 | tf_op jit(solution)/shard_map/rbqhd,khd->rbhqk/dot_general | solution.py:162
  150.9 1.8 fusion.1
  152.8 2.4 %fusion.16 = f32[4,4,16,8,64]{4,2,3,1,0:T(8,128)S(1)} fusion(bf16[1024,8,64,1,1]{0,2,1,4,3:T(8,128)(2,1)S(1)} %bitcast.92, f32[8,1024,4,4,16]{1,4,3,2,0:T(8,128)S(1)} %get-tuple-element.17, f32[4,4,8,16]{3,1,0,2:T(4,128)S(1)} %copy.60, f32[4,4,8,16]{3,1,0,2:T(4,128)S(1)} %copy.57), kind=kOutput, calls=%fused_computation.26 | convolution fusion | flops 276824064 | bytes 9977856 | tf_op jit(solution)/shard_map/rbhqk,khd->rbqhd/dot_general | solution.py:180
  155.2 1.7 fusion.19
  158.4 4.4 %convolution_convert_fusion = bf16[256,2048]{1,0:T(8,128)(2,1)} fusion(bf16[512,2048]{1,0:T(8,128)(2,1)S(1)} %copy-done, f32[256,512]{1,0:T(8,128)} %reshape.224, bf16[2048,512]{1,0:T(8,128)(2,1)} %param.30, bf16[256,2048]{1,0:T(8,128)(2,1)} %param.18, f32[2048]{0:T(1024)S(1)} %bitcast.99, f32[2048]{0:T(1024)S(1)} %bitcast.103, f32[2048]{0:T(1024)S(1)} %copy-done.15, ...), kind=kOutput, calls=%fused_computation.14 | convolution fusion | flops 1078460416 | bytes 6841344 | tf_op jit(solution)/shard_map/dot_general | solution.py:44
  162.8 22.2 %reduce-scatter.2.cloned.1.call-done = bf16[64,2048]{1,0:T(8,128)(2,1)} async-done(((bf16[256,2048]{1,0:T(8,128)(2,1)}), bf16[64,2048]{1,0:T(8,128)(2,1)}) %reduce-scatter.2.cloned.1.call-update) | async-done | bytes 262160 | tf_op jit(solution)/shard_map/reduce_scatter | solution.py:186
  186.1 1.9 fusion.37
  (77 shorter events, 12.0 us)
Async XLA Ops:
  6.5 151.8 %copy-start = (bf16[512,2048]{1,0:T(8,128)(2,1)S(1)}, bf16[512,2048]{1,0:T(8,128)(2,1)}, u32[]{:S(2)}) copy-start(bf16[512,2048]{1,0:T(8,128)(2,1)} %param.32) | copy-start | bytes 6291460
  6.5 48.6 %copy-start.4 = (bf16[256,2048]{1,0:T(8,128)(2,1)S(1)}, bf16[256,2048]{1,0:T(8,128)(2,1)}, u32[]{:S(2)}) copy-start(bf16[256,2048]{1,0:T(8,128)(2,1)} %param.18) | copy-start | bytes 3145732
  6.5 48.6 %copy-start.15 = (f32[2048]{0:T(1024)S(1)}, f32[2048]{0:T(1024)}, u32[]{:S(2)}) copy-start(f32[2048]{0:T(1024)} %param.22) | copy-start | bytes 24580
  6.5 133.2 %all-gather.2.cloned.1.call-start = ((), (), s32[]{:S(2)}) async-start(), calls=%async_computation.1 | async-start | bytes 2359296 | tf_op jit(solution)/shard_map/all_gather | solution.py:80
  55.1 2.5 %copy-start.12 = (bf16[2048,512]{1,0:T(8,128)(2,1)S(1)}, bf16[2048,512]{1,0:T(8,128)(2,1)}, u32[]{:S(2)}) copy-start(bf16[2048,512]{1,0:T(8,128)(2,1)} %param.29) | copy-start | bytes 6291460
  57.6 7.6 %copy-start.7 = (bf16[128,2048]{1,0:T(8,128)(2,1)S(1)}, bf16[128,2048]{1,0:T(8,128)(2,1)}, u32[]{:S(2)}) copy-start(bf16[128,2048]{1,0:T(8,128)(2,1)} %param.19) | copy-start | bytes 1572868
  58.5 7.5 %copy-start.13 = (bf16[2048,512]{1,0:T(8,128)(2,1)S(1)}, bf16[2048,512]{1,0:T(8,128)(2,1)}, u32[]{:S(2)}) copy-start(bf16[2048,512]{1,0:T(8,128)(2,1)} %param.28) | copy-start | bytes 6291460
  58.5 29.9 %collective-permute-start.1 = (bf16[4,64,1024]{2,1,0:T(8,128)(2,1)S(1)}, bf16[4,64,1024]{2,1,0:T(8,128)(2,1)}, u32[]{:S(2)}, u32[]{:S(2)}) collective-permute-start(bf16[4,64,1024]{2,1,0:T(8,128)(2,1)S(1)} %bitcast.89), channel_id=1, source_target_pairs={{4,0},{8,4},{12,8},{16,12},{20,16},{24,20},{28,24},{5,1},{9,5},{13... | collective-permute-start | bytes 1572872 | tf_op jit(solution)/shard_map/ppermute | solution.py:25
  59.9 28.5 %collective-permute-start = (bf16[4,64,1024]{2,1,0:T(8,128)(2,1)S(1)}, bf16[4,64,1024]{2,1,0:T(8,128)(2,1)}, u32[]{:S(2)}, u32[]{:S(2)}) collective-permute-start(bf16[4,64,1024]{2,1,0:T(8,128)(2,1)S(1)} %bitcast.90), channel_id=1, source_target_pairs={{0,4},{4,8},{8,12},{12,16},{16,20},{20,24},{24,28},{1,5},{5,9},{9,... | collective-permute-start | bytes 1572872 | tf_op jit(solution)/shard_map/ppermute | solution.py:23
  66.0 1.4 copy-start.11
  66.0 1.6 copy-start.9
  67.3 117.7 %reduce-scatter.2.cloned.1.call-start = ((), (), s32[]{:S(2)}) async-start(), calls=%async_computation.2 | async-start | bytes 1310720 | tf_op jit(solution)/shard_map/reduce_scatter | solution.py:186
  73.9 5.8 %copy-start.5 = (bf16[256,2048]{1,0:T(8,128)(2,1)S(1)}, bf16[256,2048]{1,0:T(8,128)(2,1)}, u32[]{:S(2)}) copy-start(bf16[256,2048]{1,0:T(8,128)(2,1)} %param.18) | copy-start | bytes 3145732
  73.9 5.8 %copy-start.14 = (bf16[2048,512]{1,0:T(8,128)(2,1)S(1)}, bf16[2048,512]{1,0:T(8,128)(2,1)}, u32[]{:S(2)}) copy-start(bf16[2048,512]{1,0:T(8,128)(2,1)} %param.27) | copy-start | bytes 6291460
  132.3 5.2 %copy-start.1 = (f32[4,4,8,16,256]{4,0,3,1,2:T(4,128)S(1)}, f32[4,4,8,16,256]{4,0,3,1,2:T(4,128)}, u32[]{:S(2)}) copy-start(f32[4,4,8,16,256]{4,0,3,1,2:T(4,128)} %reshape.240) | copy-start | bytes 6291460
  132.3 5.2 %copy-start.8 = (pred[4,16,256]{2,1,0:T(8,128)(4,1)S(1)}, pred[4,16,256]{2,1,0:T(8,128)(4,1)}, u32[]{:S(2)}) copy-start(pred[4,16,256]{2,1,0:T(8,128)(4,1)} %constant.78) | copy-start | bytes 49156
  147.4 2.8 %copy-start.2 = (f32[4,4,8,16,256]{4,3,2,1,0:T(8,128)S(1)}, f32[4,4,8,16,256]{4,3,2,1,0:T(8,128)}, u32[]{:S(2)}) copy-start(f32[4,4,8,16,256]{4,3,2,1,0:T(8,128)} %get-tuple-element.15) | copy-start | bytes 6291460
  150.9 1.9 copy-start.6
  152.8 2.4 %copy-start.3 = (bf16[4,4,256,512]{2,3,1,0:T(8,128)(2,1)S(1)}, bf16[4,4,256,512]{2,3,1,0:T(8,128)(2,1)}, u32[]{:S(2)}) copy-start(bf16[4,4,256,512]{2,3,1,0:T(8,128)(2,1)} %get-tuple-element.5) | copy-start | bytes 12582916
  158.4 27.8 %copy-start.10 = (f32[2048]{0:T(1024)S(1)}, f32[2048]{0:T(1024)}, u32[]{:S(2)}) copy-start(f32[2048]{0:T(1024)} %param.23) | copy-start | bytes 24580
Sparse Core Ops, SparseCore 0:
  67.4 48.7 all-gather.1
  162.9 22.0 reduce-scatter.1
where the time goes:
time: 196 us; the launch traced here: 195 us
  local copies, waits for them, and re-layouts  57.6 us (29%)
  blocking collectives  44.1 us (22%)
  matrix products  31.8 us (16%)
  waiting for transfers between devices  22.2 us (11%)
  other arithmetic  18.6 us (9%)
  between operations  13.8 us (7%)
  starting transfers between devices  6.83 us (3%)
    psum x1, blocking collectives, shards(): summed = lax.psum(partial_value, 'sp')  38.9 us
    gather x2, local copies, waits for them, and re-layouts, shards(): jnp.take(flat_rows, position.reshape(-1), axis=0)  33.9 us
    reduce_scatter x1, waiting for transfers between devices, shards(): lax.psum_scatter(product(gated_heads, w_out).astype(jnp.bfloat16), 'tp',...  22.2 us
    dot_general x6, matrix products, product(): return jnp.dot(left, right, preferred_element_type=jnp.float32)  9.43 us
    select_n x2, other arithmetic, shards(): jnp.take(flat_rows, position.reshape(-1), axis=0)  7.45 us
    reshape x1, local copies, waits for them, and re-layouts, shards(): offset_terms = jnp.einsum('rva,hbqwa->rbhqvw', row_table, by_column, prec...  7.36 us
    dot_general x1, matrix products, shards(): jnp.einsum('hae,bqwe->hbqwa', offset_bias, jnp.asarray(col_table), precis...  6.16 us
    dot_general x1, matrix products, shards(): jnp.einsum('rva,hbqwa->rbhqvw', row_table, by_column, precision=lax.Preci...  5.84 us
  transfers between devices with their start and end apart: 4, of which 1 were waited for; matrix products, arithmetic and copies ran while one was open for 38% of the time, Pallas kernels for 0%

commit v1 on v0

--- a/solution.py
+++ b/solution.py
@@ -2,12 +2,15 @@
 import jax.numpy as jnp
 import numpy as np
 from jax import lax
+from jax.experimental import pallas as pl
+from jax.experimental.pallas import tpu as pltpu
 from jax.sharding import PartitionSpec as P
 
 GRID_W = 64
 WIN_ROWS = 8
 WIN_COLS = 16
-
+LANES = 128
+HIDDEN_SCORE = -1e30
 
 EPSILON = 1e-06
 
@@ -44,7 +47,7 @@
     return jnp.dot(left, right, preferred_element_type=jnp.float32)
 
 
-def shards(
+def shards_by_rows(
     latent,
     context,
     condition,
@@ -191,6 +194,370 @@
     return updated.astype(jnp.bfloat16)
 
 
+def whole(shape):
+    return pl.BlockSpec(shape, lambda: (0,) * len(shape))
+
+
+def low_half(shape):
+    return lax.broadcasted_iota(jnp.int32, shape, len(shape) - 1) < LANES // 2
+
+
+def swap_halves(block):
+    return pltpu.roll(block, LANES // 2, len(block.shape) - 1)
+
+
+def partial_kernel(active_ref, shift_ref, scale_ref, gate_ref, out_ref):
+    active = active_ref[...]
+    pieces = []
+    for weight_ref, rows in ((shift_ref, 2), (scale_ref, 2), (gate_ref, 1)):
+        terms = jnp.dot(active, weight_ref[...], preferred_element_type=jnp.float32)
+        pieces += [terms[row : row + 1] for row in range(rows)]
+    width = shift_ref.shape[1] // LANES
+    for index, piece in enumerate(pieces):
+        for lane in range(width):
+            row = index * width + lane
+            block = piece[:, lane * LANES : (lane + 1) * LANES]
+            out_ref[:, row : row + 1, :] = jnp.broadcast_to(block[None], (out_ref.shape[0], 1, LANES))
+
+
+def project_kernel(
+    terms_ref,
+    gain_ref,
+    latent_ref,
+    context_ref,
+    query_hbm,
+    key_hbm,
+    value_hbm,
+    silu_hbm,
+    send_ref,
+    silu_ref,
+    gating_ref,
+    weight_ref,
+    hidden_ref,
+    vectors_ref,
+    semaphores,
+    *,
+    sp_count,
+    tp_count,
+):
+    sources = (key_hbm, value_hbm, query_hbm, silu_hbm)
+    copies = [
+        pltpu.make_async_copy(source, weight_ref.at[index], semaphores.at[index])
+        for index, source in enumerate(sources)
+    ]
+    for copy in copies:
+        copy.start()
+    tokens, model_width = latent_ref.shape
+    context_tokens = context_ref.shape[0]
+    cols = key_hbm.shape[1]
+    width = cols // LANES
+    for part in range(tp_count):
+        total = terms_ref[part]
+        for other in range(1, sp_count):
+            total = total + terms_ref[other * tp_count + part]
+        for index in range(5):
+            for lane in range(width):
+                first = part * cols + lane * LANES
+                row = index * width + lane
+                vectors_ref[index : index + 1, first : first + LANES] = total[row : row + 1]
+    gating_ref[...] = vectors_ref[4:5, :]
+    gain = gain_ref[...]
+    for source, first, count, kind in (
+        (context_ref, tokens, context_tokens, 1),
+        (latent_ref, 0, tokens, 0),
+    ):
+        factor = gain * (1.0 + vectors_ref[2 + kind : 3 + kind, :])
+        shift = vectors_ref[kind : kind + 1, :]
+        step = 32
+
+        def body(index, carry, source=source, first=first, factor=factor, shift=shift):
+            start = pl.multiple_of(index * step, step)
+            values = source[pl.ds(start, step), :].astype(jnp.float32)
+            mean = jnp.sum(values * values, axis=-1, keepdims=True) * (1.0 / model_width)
+            rows = values * lax.rsqrt(mean + EPSILON) * factor + shift
+            hidden_ref[pl.ds(pl.multiple_of(first + start, step), step), :] = rows.astype(jnp.bfloat16)
+            return carry
+
+        lax.fori_loop(0, count // step, body, 0)
+    half = tokens // 2
+    copies[0].wait()
+    keys = jnp.dot(hidden_ref[...], weight_ref[0], preferred_element_type=jnp.float32)
+    copies[1].wait()
+    values = jnp.dot(hidden_ref[...], weight_ref[1], preferred_element_type=jnp.float32)
+    low = low_half((tokens + context_tokens, LANES))
+    for pair in range(width):
+        lanes = slice(pair * LANES, (pair + 1) * LANES)
+        key, value = keys[:, lanes], values[:, lanes]
+        send_ref[2 * pair, : tokens + context_tokens, :] = jnp.where(
+            low, key, swap_halves(value)
+        ).astype(jnp.bfloat16)
+        send_ref[2 * pair + 1, : tokens + context_tokens, :] = jnp.where(
+            low, swap_halves(key), value
+        ).astype(jnp.bfloat16)
+    copies[2].wait()
+    queries = jnp.dot(hidden_ref[:tokens], weight_ref[2], preferred_element_type=jnp.float32)
+    low = low_half((half, LANES))
+    for pair in range(width):
+        lanes = slice(pair * LANES, (pair + 1) * LANES)
+        block = queries[:, lanes].astype(jnp.bfloat16).astype(jnp.float32) * (LANES // 2) ** -0.5
+        top, bottom = block[:half], block[half:]
+        send_ref[2 * pair, tokens + context_tokens :, :] = jnp.where(
+            low, top, swap_halves(bottom)
+        ).astype(jnp.bfloat16)
+        send_ref[2 * pair + 1, tokens + context_tokens :, :] = jnp.where(
+            low, swap_halves(top), bottom
+        ).astype(jnp.bfloat16)
+    copies[3].wait()
+    silu_ref[...] = jnp.dot(
+        hidden_ref[:tokens], weight_ref[3], preferred_element_type=jnp.float32
+    ).astype(jnp.bfloat16)
+
+
+def attend_kernel(
+    base_ref, received_ref, out_ref, bias_ref, pairs_ref, kv_ref, ones_ref, context_ref, context_ones_ref
+):
+    blocks, rows, _ = received_ref.shape
+    tokens = kv_ref.shape[0] // blocks
+    context_tokens = context_ref.shape[0] // blocks
+    grid_rows = tokens // GRID_W
+    total_rows = blocks * grid_rows
+    band_rows = bias_ref.shape[2] // GRID_W
+    half = tokens // 2
+    column = lax.broadcasted_iota(jnp.int32, (GRID_W, LANES), 0)
+    lane = lax.broadcasted_iota(jnp.int32, (GRID_W, LANES), 1)
+    key_column = lane % GRID_W
+    first_column = jnp.clip(column - WIN_COLS // 2, 0, GRID_W - WIN_COLS)
+    inside = (key_column >= first_column) & (key_column < first_column + WIN_COLS)
+    for index in range(base_ref.shape[0]):
+        row = jnp.broadcast_to(base_ref[index : index + 1, :], (GRID_W, LANES))
+        toeplitz = pltpu.roll(row, 0, 1, stride=1, stride_axis=0)
+        pairs_ref[index] = jnp.where(inside, toeplitz, HIDDEN_SCORE)
+    hidden = jnp.full((GRID_W, LANES), HIDDEN_SCORE, jnp.float32)
+    low = lane < LANES // 2
+    for kind, block in enumerate((0, 1, blocks - 1)):
+        band_first = min(max(block * grid_rows - WIN_ROWS // 2, 0), total_rows - band_rows)
+        for query in range(grid_rows):
+            query_row = block * grid_rows + query
+            window_first = min(max(query_row - WIN_ROWS // 2, 0), total_rows - WIN_ROWS)
+            for pair in range(band_rows // 2):
+                key_row = band_first + 2 * pair
+                valid = [
+                    window_first <= key_row + side < window_first + WIN_ROWS for side in range(2)
+                ]
+                offset = key_row - query_row + WIN_ROWS - 1
+                if not any(valid):
+                    tile = hidden
+                elif all(valid):
+                    tile = pairs_ref[offset]
+                elif valid[0]:
+                    tile = jnp.where(low, pairs_ref[min(offset, 2 * WIN_ROWS - 3)], hidden) if offset <= 2 * WIN_ROWS - 3 else jnp.where(low, swap_halves(pairs_ref[offset - 1]), hidden)
+                else:
+                    tile = jnp.where(low, hidden, pairs_ref[offset]) if offset >= 0 else jnp.where(low, hidden, swap_halves(pairs_ref[offset + 1]))
+                bias_ref[
+                    kind,
+                    query * GRID_W : (query + 1) * GRID_W,
+                    pair * LANES : (pair + 1) * LANES,
+                ] = tile
+    for block in range(blocks):
+        kv = received_ref[block, :tokens, :]
+        kv_ref[block * tokens : (block + 1) * tokens, :] = kv
+        ones_ref[block * tokens : (block + 1) * tokens, :] = jnp.where(
+            low_half(kv.shape), jnp.ones_like(kv), kv
+        )
+        kv = received_ref[block, tokens : tokens + context_tokens, :]
+        context_ref[block * context_tokens : (block + 1) * context_tokens, :] = kv
+        context_ones_ref[block * context_tokens : (block + 1) * context_tokens, :] = jnp.where(
+            low_half(kv.shape), jnp.ones_like(kv), kv
+        )
+    low_block = low_half((half, LANES))
+    contract = (((1,), (1,)), ((), ()))
+
+    def body(block, carry):
+        packed = received_ref[block, tokens + context_tokens :, :].astype(jnp.float32)
+        queries = jnp.concatenate(
+            [jnp.where(low_block, packed, 0.0), jnp.where(low_block, swap_halves(packed), 0.0)], axis=0
+        ).astype(jnp.bfloat16)
+        kind = jnp.where(block == 0, 0, jnp.where(block == blocks - 1, 2, 1))
+        band = jnp.clip(block * grid_rows - WIN_ROWS // 2, 0, total_rows - band_rows) * GRID_W
+        band = pl.ds(pl.multiple_of(band, GRID_W), band_rows * GRID_W)
+        window = (
+            lax.dot_general(queries, kv_ref[band, :], contract, preferred_element_type=jnp.float32)
+            + bias_ref[kind]
+        )
+        context = lax.dot_general(
+            queries, context_ref[...], contract, preferred_element_type=jnp.float32
+        )
+        maximum = jnp.maximum(
+            jnp.max(window, axis=-1, keepdims=True), jnp.max(context, axis=-1, keepdims=True)
+        )
+        sums = jnp.dot(
+            jnp.exp(window - maximum).astype(jnp.bfloat16),
+            ones_ref[band, :],
+            preferred_element_type=jnp.float32,
+        ) + jnp.dot(
+            jnp.exp(context - maximum).astype(jnp.bfloat16),
+            context_ones_ref[...],
+            preferred_element_type=jnp.float32,
+        )
+        attended = sums / swap_halves(sums)
+        top, bottom = attended[:half], attended[half:]
+        out_ref[block] = jnp.where(low_block, swap_halves(top), bottom).astype(jnp.bfloat16)
+        return carry
+
+    lax.fori_loop(0, blocks, body, 0)
+
+
+def output_kernel(attended_ref, silu_ref, weight_ref, out_ref, gated_ref):
+    heads, half, _ = attended_ref.shape
+    low = low_half((half, LANES))
+    for pair in range(heads // 2):
+        first = attended_ref[2 * pair].astype(jnp.float32)
+        second = attended_ref[2 * pair + 1].astype(jnp.float32)
+        lanes = slice(pair * LANES, (pair + 1) * LANES)
+        for side, block in enumerate(
+            (
+                jnp.where(low, first, swap_halves(second)),
+                jnp.where(low, swap_halves(first), second),
+            )
+        ):
+            gate = silu_ref[side * half : (side + 1) * half, lanes].astype(jnp.float32)
+            gated_ref[side * half : (side + 1) * half, lanes] = (
+                gate / (1.0 + jnp.exp(-gate)) * block
+            ).astype(jnp.bfloat16)
+    out_ref[...] = jnp.dot(
+        gated_ref[...], weight_ref[...], preferred_element_type=jnp.float32
+    ).astype(jnp.bfloat16)
+
+
+def finish_kernel(terms_ref, latent_ref, gating_ref, gain_ref, out_ref):
+    total = terms_ref[0].astype(jnp.float32)
+    for index in range(1, terms_ref.shape[0]):
+        total = total + terms_ref[index].astype(jnp.float32)
+    branch = total.astype(jnp.bfloat16).astype(jnp.float32)
+    mean = jnp.sum(branch * branch, axis=-1, keepdims=True) * (1.0 / branch.shape[-1])
+    out_ref[...] = (
+        latent_ref[...].astype(jnp.float32)
+        + gating_ref[...] * (branch * lax.rsqrt(mean + EPSILON)) * gain_ref[...]
+    ).astype(jnp.bfloat16)
+
+
+def call(kernel, name, out_shape, scratch=(), **kwargs):
+    return pl.pallas_call(
+        kernel,
+        name=name,
+        out_shape=out_shape,
+        scratch_shapes=scratch,
+        compiler_params=pltpu.CompilerParams(vmem_limit_bytes=56 * 2**20),
+        **kwargs,
+    )
+
+
+def shards_by_heads(
+    latent,
+    context,
+    condition,
+    context_condition,
+    gain_pre,
+    gain_post,
+    w_shift,
+    w_scale,
+    w_gate,
+    w_query,
+    w_key,
+    w_value,
+    w_silu,
+    offset_bias,
+    w_out,
+):
+    sp_index = lax.axis_index("sp")
+    tp_index = lax.axis_index("tp")
+    sp_count, tp_count = lax.axis_size("sp"), lax.axis_size("tp")
+    in_rows, cols = w_shift.shape
+    tokens, model_width = latent.shape
+    context_tokens = context.shape[0]
+    width = cols // LANES
+    active = jax.nn.silu(
+        jnp.stack(
+            [
+                lax.dynamic_slice_in_dim(vector, sp_index * in_rows, in_rows, 0)
+                for vector in (condition, context_condition)
+            ]
+        ).astype(jnp.float32)
+    ).astype(jnp.bfloat16)
+    f32, bf16 = jnp.float32, jnp.bfloat16
+    shape = jax.ShapeDtypeStruct
+    devices = sp_count * tp_count
+    terms = call(partial_kernel, "partial", shape((devices, 5 * width, LANES), f32))(
+        active, w_shift, w_scale, w_gate
+    )
+    terms = lax.all_to_all(terms, ("sp", "tp"), 0, 0, tiled=True)
+    rows = tokens + context_tokens + tokens // 2
+    hbm = pl.BlockSpec(memory_space=pl.ANY)
+    vmem = pl.BlockSpec(memory_space=pltpu.VMEM)
+    send, silu_gate, gating = call(
+        lambda *refs: project_kernel(*refs, sp_count=sp_count, tp_count=tp_count),
+        "project",
+        (
+            shape((sp_count, rows, LANES), bf16),
+            shape((tokens, cols), bf16),
+            shape((1, model_width), f32),
+        ),
+        scratch=[
+            pltpu.VMEM((4, model_width, cols), bf16),
+            pltpu.VMEM((tokens + context_tokens, model_width), bf16),
+            pltpu.VMEM((8, model_width), f32),
+            pltpu.SemaphoreType.DMA((4,)),
+        ],
+        in_specs=[vmem] * 4 + [hbm] * 4,
+    )(
+        terms,
+        gain_pre.reshape(1, -1),
+        latent,
+        context,
+        w_query,
+        w_key,
+        w_value,
+        w_silu,
+    )
+    received = lax.all_to_all(send, "sp", 0, 0, tiled=True)
+    table = lax.dynamic_index_in_dim(offset_bias, sp_index, 0, keepdims=False)
+    rows_of, cols_of = table.shape
+    centre = WIN_COLS - 1
+    gap = jnp.zeros((rows_of - 1, (LANES - 2 * cols_of) // 2), f32)
+    base = jnp.concatenate(
+        [table[:-1, centre:], gap, table[1:], gap, table[:-1, :centre]], axis=1
+    )
+    band_rows = 3 * WIN_ROWS // 2
+    attended = call(
+        attend_kernel,
+        "attend",
+        shape((sp_count, tokens // 2, LANES), bf16),
+        scratch=[
+            pltpu.VMEM((3, tokens, band_rows * GRID_W), f32),
+            pltpu.VMEM((rows_of - 1, GRID_W, LANES), f32),
+            pltpu.VMEM((sp_count * tokens, LANES), bf16),
+            pltpu.VMEM((sp_count * tokens, LANES), bf16),
+            pltpu.VMEM((sp_count * context_tokens, LANES), bf16),
+            pltpu.VMEM((sp_count * context_tokens, LANES), bf16),
+        ],
+    )(base, received)
+    attended = lax.all_to_all(attended, "sp", 0, 0, tiled=True)
+    branch = call(
+        output_kernel,
+        "output",
+        shape((tokens, model_width), bf16),
+        scratch=[pltpu.VMEM((tokens, cols), bf16)],
+    )(attended, silu_gate, w_out)
+    out_rows = tokens // tp_count
+    branch = lax.all_to_all(
+        branch.reshape(tp_count, out_rows, model_width), "tp", 0, 0, tiled=True
+    )
+    own_rows = lax.dynamic_slice_in_dim(latent, tp_index * out_rows, out_rows, 0)
+    return call(finish_kernel, "finish", shape((out_rows, model_width), bf16))(
+        branch, own_rows, gating, gain_post.reshape(1, -1)
+    )
+
+
 def solution(mesh):
     in_specs = (
         P("sp", None),
@@ -210,4 +577,19 @@
         P("tp", None),
     )
     out_specs = P(("sp", "tp"), None)
+    sp_count, tp_count = mesh.shape["sp"], mesh.shape["tp"]
+
+    def shards(*arrays):
+        heads = arrays[13].shape[0]
+        head_width = arrays[6].shape[1] // heads
+        grid_rows = arrays[0].shape[0] // GRID_W
+        one_head_each = (
+            heads == sp_count
+            and sp_count >= 3
+            and 2 * head_width == LANES
+            and 2 * GRID_W == LANES
+            and 2 * grid_rows == WIN_ROWS
+        )
+        return (shards_by_heads if one_head_each else shards_by_rows)(*arrays)
+
     return jax.shard_map(shards, mesh=mesh, in_specs=in_specs, out_specs=out_specs, check_vma=False)

time: 196 us -> 112 us (0.57)
  local copies, waits for them, and re-layouts: 57.6 us -> 5.9 us
  matrix products: 31.8 us -> 0 us
  Pallas kernels: 0 us -> 26.4 us
  other arithmetic: 18.6 us -> 0.59 us
  waiting for transfers between devices: 22.2 us -> 37.5 us
  between operations: 13.8 us -> 0.06 us
  blocking collectives: 44.1 us -> 33.4 us
    psum x1 -> x0, blocking collectives: 38.9 us -> none  [shards(): summed = lax.psum(partial_value, 'sp')]
    all_to_all x0 -> x2, waiting for transfers between devices: none -> 37.5 us  [the longest x1 24.8 us: shards_by_heads(): received = lax.all_to_all(send, 'sp', 0, 0, tiled=True)]
    gather x2 -> x0, local copies, waits for them, and re-layouts: 33.9 us -> none  [shards(): jnp.take(flat_rows, position.reshape(-1), axis=0)]
    all_to_all x0 -> x2, blocking collectives: none -> 33.4 us  [the longest x1 20.7 us: shards_by_heads(): terms = lax.all_to_all(terms, ('sp', 'tp'), 0, 0, tiled=True)]
    dot_general x13 -> x0, matrix products: 31.8 us -> none  [the longest x6 9.43 us: product(): return jnp.dot(left, right, preferred_element_type=jnp.float32)]
    pallas_call x0 -> x5, Pallas kernels: none -> 26.4 us  [the longest x1 10.7 us: shards_by_heads(): call(attend_kernel, 'attend', shape((sp_count, tokens // 2, LANES), bf16)...]
    reduce_scatter x1 -> x0, waiting for transfers between devices: 22.2 us -> none  [shards(): lax.psum_scatter(product(gated_heads, w_out).astype(jnp.bfloat16), 'tp',...]
    slice x4 -> x2, local copies, waits for them, and re-layouts: 12.8 us -> 0.08 us  [the longest x1 0.07 us: shards_by_heads(): table[:-1, centre:]]
  transfers between devices with their start and end apart: 4 -> 2, of which waited for: 1 -> 2; matrix products, arithmetic and copies ran while one was open for 38% -> 2% of each run, Pallas kernels for 0% -> 0%
where the time goes in v1:
time: 112 us; the launch traced here: 111 us
  waiting for transfers between devices  37.5 us (33%)
  blocking collectives  33.4 us (30%)
  Pallas kernels  26.4 us (24%)
  starting transfers between devices  7.08 us (6%)
  local copies, waits for them, and re-layouts  5.9 us (5%)
    all_to_all x1, waiting for transfers between devices, shards_by_heads(): received = lax.all_to_all(send, 'sp', 0, 0, tiled=True)  24.8 us
    all_to_all x1, blocking collectives, shards_by_heads(): terms = lax.all_to_all(terms, ('sp', 'tp'), 0, 0, tiled=True)  20.7 us
    all_to_all x1, blocking collectives, shards_by_heads(): attended = lax.all_to_all(attended, 'sp', 0, 0, tiled=True)  12.7 us
    all_to_all x1, waiting for transfers between devices, shards_by_heads(): lax.all_to_all(branch.reshape(tp_count, out_rows, model_width), 'tp', 0,...  12.7 us
    pallas_call x1, Pallas kernels, shards_by_heads(): call(attend_kernel, 'attend', shape((sp_count, tokens // 2, LANES), bf16)...  10.7 us
    pallas_call x1, Pallas kernels, shards_by_heads(): call(lambda *refs: project_kernel(*refs, sp_count=sp_count, tp_count=tp_c...  7.5 us
    pallas_call x1, Pallas kernels, shards_by_heads(): call(output_kernel, 'output', shape((tokens, model_width), bf16), scratch...  3.62 us
    all_to_all x1, starting transfers between devices, shards_by_heads(): received = lax.all_to_all(send, 'sp', 0, 0, tiled=True)  3.57 us
  transfers between devices with their start and end apart: 2, of which 2 were waited for; matrix products, arithmetic and copies ran while one was open for 2% of the time, Pallas kernels for 0%

profile of v1, /device:TPU:0, one launch (start us, length us, event | category | flops | bytes accessed | tf_op | source)
XLA Modules:
  0.0 110.9 jit_solution(12473361336530350656)
XLA Ops:
  0.0 0.0 copy-start
  0.0 0.8 dynamic_slice.15
  0.8 0.8 dynamic_slice.14
  1.5 0.6 fusion.2.active_ref
  2.1 2.2 %partial.1 = f32[32,20,128]{2,1,0:T(8,128)} custom-call(bf16[2,256]{1,0:T(2,128)(2,1)} %fusion.2.active_ref, bf16[256,512]{1,0:T(8,128)(2,1)} %shift_ref.1, bf16[256,512]{1,0:T(8,128)(2,1)} %scale_ref.1, bf16[256,512]{1,0:T(8,128)(2,1)} %gate_ref.1), custom_call_target="tpu_custom_call" | custom-call | tf_op jit(solution)/shard_map/partial/pallas_call | solution.py:490
  4.3 20.7 %all_to_all.20.refs_0_ = f32[32,20,128]{2,1,0:T(8,128)} all-to-all(f32[32,20,128]{2,1,0:T(8,128)} %partial.1), channel_id=1, replica_groups=mesh['sp'=8,'tp'=4] {'sp','tp'}, dimensions={0} | all-to-all | bytes 655360 | tf_op jit(solution)/shard_map/all_to_all | solution.py:493
  25.0 7.5 %project.1 = (bf16[8,512,128]{2,1,0:T(8,128)(2,1)}, bf16[256,512]{1,0:T(8,128)(2,1)}, f32[1,2048]{1,0:T(1,128)}) custom-call(f32[32,20,128]{2,1,0:T(8,128)} %all_to_all.20.refs_0_, f32[1,2048]{1,0:T(1,128)} %bitcast.12, bf16[256,2048]{1,0:T(8,128)(2,1)} %refs_2_.1, bf16[128,2048]{1,0:T(8,128)(2,1)} %refs_3_.1, bf16[2048,512]{1,0:T(8,128)(2,1)} %refs_4_.1, ...), custom_call_target="tpu_custom_call" | custom-call | tf_op jit(solution)/shard_map/project/pallas_call | solution.py:497
  32.5 3.6 %all-to-all-start.1 = ((bf16[8,512,128]{2,1,0:T(8,128)(2,1)}), bf16[8,512,128]{2,1,0:T(8,128)(2,1)S(1)}, u32[]{:S(2)}, u32[]{:S(2)}) async-start(bf16[8,512,128]{2,1,0:T(8,128)(2,1)} %get-tuple-element.8), calls=%async_computation.1 | async-start | bytes 2097152 | tf_op jit(solution)/shard_map/all_to_all | solution.py:522
  36.1 0.0 copy-done
  36.1 0.1 slice.16
  36.2 0.7 concatenate.3.base_ref
  36.9 24.8 %all-to-all-done.1.received_ref = bf16[8,512,128]{2,1,0:T(8,128)(2,1)S(1)} async-done(((bf16[8,512,128]{2,1,0:T(8,128)(2,1)}), bf16[8,512,128]{2,1,0:T(8,128)(2,1)S(1)}, u32[]{:S(2)}, u32[]{:S(2)}) %all-to-all-start.1) | async-done | bytes 1048608 | tf_op jit(solution)/shard_map/all_to_all | solution.py:522
  61.6 0.0 copy-start.1
  61.6 1.0 copy-done.1
  62.6 10.7 %attend.1 = bf16[8,128,128]{2,1,0:T(8,128)(2,1)} custom-call(f32[14,128]{1,0:T(8,128)} %concatenate.3.base_ref, bf16[8,512,128]{2,1,0:T(8,128)(2,1)} %copy-done.1), custom_call_target="tpu_custom_call" | custom-call | tf_op jit(solution)/shard_map/attend/pallas_call | solution.py:531
  73.3 12.7 %all_to_all.21.attended_ref = bf16[8,128,128]{2,1,0:T(8,128)(2,1)} all-to-all(bf16[8,128,128]{2,1,0:T(8,128)(2,1)} %attend.1), channel_id=1, replica_groups=mesh['sp'=8,'tp'=4] {'sp'}, dimensions={0} | all-to-all | bytes 524288 | tf_op jit(solution)/shard_map/all_to_all | solution.py:544
  86.0 3.6 %output.1 = bf16[256,2048]{1,0:T(8,128)(2,1)} custom-call(bf16[8,128,128]{2,1,0:T(8,128)(2,1)} %all_to_all.21.attended_ref, bf16[256,512]{1,0:T(8,128)(2,1)} %get-tuple-element.9.silu_ref, bf16[512,2048]{1,0:T(8,128)(2,1)} %weight_ref.1), custom_call_target="tpu_custom_call" | custom-call | tf_op jit(solution)/shard_map/output/pallas_call | solution.py:545
  89.7 3.5 %all-to-all-start.3 = ((bf16[4,64,2048]{2,1,0:T(8,128)(2,1)}), bf16[4,64,2048]{2,1,0:T(8,128)(2,1)S(1)}, u32[]{:S(2)}, u32[]{:S(2)}) async-start(bf16[4,64,2048]{2,1,0:T(8,128)(2,1)} %bitcast.8), calls=%async_computation.3 | async-start | bytes 2097152 | tf_op jit(solution)/shard_map/all_to_all | solution.py:552
  93.2 1.7 %constant_dynamic-slice_fusion.latent_ref = bf16[64,2048]{1,0:T(8,128)(2,1)} fusion(bf16[256,2048]{1,0:T(8,128)(2,1)} %refs_2_.1, s32[]{:T(128)S(6)} %select_n.13), kind=kLoop, calls=%fused_computation.6 | loop fusion | bytes 524292 | tf_op jit(solution)/shard_map/dynamic_slice | solution.py:555
  94.9 12.7 %all-to-all-done.3.terms_ref = bf16[4,64,2048]{2,1,0:T(8,128)(2,1)S(1)} async-done(((bf16[4,64,2048]{2,1,0:T(8,128)(2,1)}), bf16[4,64,2048]{2,1,0:T(8,128)(2,1)S(1)}, u32[]{:S(2)}, u32[]{:S(2)}) %all-to-all-start.3) | async-done | bytes 1048608 | tf_op jit(solution)/shard_map/all_to_all | solution.py:552
  107.6 0.0 copy-start.2
  107.6 1.0 copy-done.2
  108.5 2.4 %finish.1 = bf16[64,2048]{1,0:T(8,128)(2,1)} custom-call(bf16[4,64,2048]{2,1,0:T(8,128)(2,1)} %copy-done.2, bf16[64,2048]{1,0:T(8,128)(2,1)} %constant_dynamic-slice_fusion.latent_ref, f32[1,2048]{1,0:T(1,128)} %get-tuple-element.10.gating_ref, f32[1,2048]{1,0:T(1,128)} %bitcast.11), custom_call_target="tpu_custom_call" | custom-call | tf_op jit(solution)/shard_map/finish/pallas_call | solution.py:556
  (6 shorter events, 0.0 us)
Async XLA Ops:
  0.0 36.1 %copy-start = (f32[8,15,31]{2,0,1:T(8,128)S(1)}, f32[8,15,31]{2,0,1:T(8,128)}, u32[]{:S(2)}) copy-start(f32[8,15,31]{2,0,1:T(8,128)} %param.28) | copy-start | bytes 44644
  32.5 29.1 %all-to-all-start.1 = ((bf16[8,512,128]{2,1,0:T(8,128)(2,1)}), bf16[8,512,128]{2,1,0:T(8,128)(2,1)S(1)}, u32[]{:S(2)}, u32[]{:S(2)}) async-start(bf16[8,512,128]{2,1,0:T(8,128)(2,1)} %get-tuple-element.8), calls=%async_computation.1 | async-start | bytes 2097152 | tf_op jit(solution)/shard_map/all_to_all | solution.py:522
  61.6 1.0 copy-start.1
  89.7 17.9 %all-to-all-start.3 = ((bf16[4,64,2048]{2,1,0:T(8,128)(2,1)}), bf16[4,64,2048]{2,1,0:T(8,128)(2,1)S(1)}, u32[]{:S(2)}, u32[]{:S(2)}) async-start(bf16[4,64,2048]{2,1,0:T(8,128)(2,1)} %bitcast.8), calls=%async_computation.3 | async-start | bytes 2097152 | tf_op jit(solution)/shard_map/all_to_all | solution.py:552
  107.6 1.0 copy-start.2

commit v2 on v0

--- a/solution.py
+++ b/solution.py
@@ -1,13 +1,20 @@
+import functools
+
 import jax
 import jax.numpy as jnp
 import numpy as np
 from jax import lax
+from jax.experimental import pallas as pl
+from jax.experimental.pallas import tpu as pltpu
 from jax.sharding import PartitionSpec as P
+
 
 GRID_W = 64
 WIN_ROWS = 8
 WIN_COLS = 16
-
+LANES = 128
+HALF = LANES // 2
+HIDDEN_SCORE = -1e30
 
 EPSILON = 1e-06
 
@@ -44,7 +51,7 @@
     return jnp.dot(left, right, preferred_element_type=jnp.float32)
 
 
-def shards(
+def shards_by_rows(
     latent,
     context,
     condition,
@@ -64,7 +71,7 @@
     sp_index = lax.axis_index("sp")
     tp_index = lax.axis_index("tp")
     in_rows, local_cols = w_shift.shape
-    tokens, model_width = latent.shape
+    tokens, _ = latent.shape
     active = jax.nn.silu(jnp.stack([condition, context_condition]).astype(jnp.float32)).astype(
         jnp.bfloat16
     )
@@ -189,6 +196,447 @@
     own_rows = lax.dynamic_slice_in_dim(latent, tp_index * out_rows, out_rows, 0)
     updated = own_rows.astype(jnp.float32) + gating[0] * normalize(branch, gain_post)
     return updated.astype(jnp.bfloat16)
+
+
+def low_half(shape):
+    return lax.broadcasted_iota(jnp.int32, shape, len(shape) - 1) < HALF
+
+
+def swap_halves(block):
+    return pltpu.roll(block, HALF, len(block.shape) - 1)
+
+
+def head_pair(first, second):
+    low = low_half(first.shape)
+    return (
+        jnp.where(low, first, swap_halves(second)),
+        jnp.where(low, swap_halves(first), second),
+    )
+
+
+def partial_kernel(index_ref, condition_ref, context_ref, shift_ref, scale_ref, gate_ref, out_ref, active_ref):
+    rows = shift_ref.shape[0] // LANES
+    for kind, source in enumerate((condition_ref, context_ref)):
+        values = source[...].astype(jnp.float32)
+        active_ref[kind] = values / (1.0 + jnp.exp(-values))
+    own = pl.ds(index_ref[0] * rows, rows)
+    vectors = [active_ref[kind, own, :].astype(jnp.bfloat16) for kind in range(2)]
+    width = shift_ref.shape[1] // LANES
+    row = 0
+    for weight_ref, kinds in ((shift_ref, 2), (scale_ref, 2), (gate_ref, 1)):
+        both = sum(
+            jnp.dot(
+                jnp.concatenate([vectors[kind][part : part + 1] for kind in range(2)], axis=0),
+                weight_ref[part * LANES : (part + 1) * LANES, :],
+                preferred_element_type=jnp.float32,
+            )
+            for part in range(rows)
+        )
+        for kind in range(kinds):
+            for lane in range(width):
+                block = both[kind : kind + 1, lane * LANES : (lane + 1) * LANES].astype(out_ref.dtype)
+                out_ref[:, row : row + 1, :] = jnp.broadcast_to(block[None], (out_ref.shape[0], 1, LANES))
+                row += 1
+
+
+def norm_kernel(latent_ref, context_ref, out_ref):
+    step = 32
+    first = 0
+    for source in (latent_ref, context_ref):
+
+        def body(index, carry, source=source, first=first):
+            start = pl.multiple_of(index * step, step)
+            values = source[pl.ds(start, step), :].astype(jnp.float32)
+            mean = jnp.sum(values * values, axis=-1, keepdims=True) * (1.0 / values.shape[-1])
+            out_ref[pl.ds(pl.multiple_of(first + start, step), step), :] = jnp.broadcast_to(
+                lax.rsqrt(mean + EPSILON), (step, LANES)
+            )
+            return carry
+
+        lax.fori_loop(0, source.shape[0] // step, body, 0)
+        first += source.shape[0]
+
+
+def project_kernel(
+    terms_ref, gain_ref, norm_ref, context_hbm, latent_hbm, key_hbm, value_hbm, query_hbm,
+    send_ref, hidden_ref, gating_ref,
+    context_ref, latent_ref, key_ref, value_ref, query_ref, context_hidden_ref, vectors_ref, semaphores,
+    *, sp_count, tp_count
+):
+    pairs = (
+        (context_hbm, context_ref),
+        (latent_hbm, latent_ref),
+        (key_hbm, key_ref),
+        (value_hbm, value_ref),
+        (query_hbm, query_ref),
+    )
+    copies = [
+        pltpu.make_async_copy(source, target, semaphores.at[index])
+        for index, (source, target) in enumerate(pairs)
+    ]
+    for copy in copies:
+        copy.start()
+    cols = key_ref.shape[1]
+    width = cols // LANES
+    for part in range(tp_count):
+        total = terms_ref[part].astype(jnp.float32)
+        for other in range(1, sp_count):
+            total = total + terms_ref[other * tp_count + part].astype(jnp.float32)
+        for index in range(5):
+            for lane in range(width):
+                first = part * cols + lane * LANES
+                row = index * width + lane
+                vectors_ref[index : index + 1, first : first + LANES] = total[row : row + 1]
+    gating_ref[...] = vectors_ref[4:5, :]
+    tokens = latent_ref.shape[0]
+    count = context_ref.shape[0]
+
+    def modulate_rows(source, target, first, kind):
+        factor = gain_ref[...] * (1.0 + vectors_ref[2 + kind : 3 + kind, :])
+        shift = vectors_ref[kind : kind + 1, :]
+        step = 32
+
+        def body(index, carry):
+            start = pl.multiple_of(index * step, step)
+            norm = norm_ref[pl.ds(pl.multiple_of(first + start, step), step), :][:, :1]
+            rows = source[pl.ds(start, step), :].astype(jnp.float32) * norm * factor + shift
+            target[pl.ds(start, step), :] = rows.astype(jnp.bfloat16)
+            return carry
+
+        lax.fori_loop(0, source.shape[0] // step, body, 0)
+
+    def store(keys, values, first):
+        for pair in range(width):
+            lanes = slice(pair * LANES, (pair + 1) * LANES)
+            for head, kv in enumerate(head_pair(keys[:, lanes], values[:, lanes])):
+                send_ref[2 * pair + head, first : first + keys.shape[0], :] = kv.astype(jnp.bfloat16)
+
+    copies[0].wait()
+    modulate_rows(context_ref, context_hidden_ref, tokens, 1)
+    copies[1].wait()
+    modulate_rows(latent_ref, hidden_ref, 0, 0)
+    copies[2].wait()
+    context_keys = jnp.dot(context_hidden_ref[...], key_ref[...], preferred_element_type=jnp.float32)
+    keys = jnp.dot(hidden_ref[...], key_ref[...], preferred_element_type=jnp.float32)
+    copies[3].wait()
+    values = jnp.dot(context_hidden_ref[...], value_ref[...], preferred_element_type=jnp.float32)
+    store(context_keys, values, tokens)
+    values = jnp.dot(hidden_ref[...], value_ref[...], preferred_element_type=jnp.float32)
+    store(keys, values, 0)
+    copies[4].wait()
+    queries = jnp.dot(hidden_ref[...], query_ref[...], preferred_element_type=jnp.float32)
+    half = tokens // 2
+    for pair in range(width):
+        lanes = slice(pair * LANES, (pair + 1) * LANES)
+        block = queries[:, lanes].astype(jnp.bfloat16).astype(jnp.float32) * HALF**-0.5
+        for head, packed in enumerate(head_pair(block[:half], block[half:])):
+            send_ref[2 * pair + head, tokens + count :, :] = packed.astype(jnp.bfloat16)
+
+
+def gate_kernel(index_ref, hidden_ref, weight_ref, *out_refs):
+    *out_refs, rows_ref = out_refs
+    rows_ref[...] = jnp.dot(hidden_ref[...], weight_ref[...], preferred_element_type=jnp.float32)
+    for offset, out_ref in enumerate(out_refs):
+        count = out_ref.shape[0]
+        first = pl.multiple_of((index_ref[1] ^ offset) * count, count)
+        out_ref[...] = rows_ref[pl.ds(first, count), :].astype(jnp.bfloat16)
+
+
+def bias_kernel(base_ref, pairs_ref):
+    column = lax.broadcasted_iota(jnp.int32, (GRID_W, LANES), 0)
+    key_column = lax.broadcasted_iota(jnp.int32, (GRID_W, LANES), 1) % GRID_W
+    first_column = jnp.clip(column - WIN_COLS // 2, 0, GRID_W - WIN_COLS)
+    inside = (key_column >= first_column) & (key_column < first_column + WIN_COLS)
+    for index in range(base_ref.shape[0]):
+        row = jnp.broadcast_to(base_ref[index : index + 1, :], (GRID_W, LANES))
+        toeplitz = pltpu.roll(row, 0, 1, stride=1, stride_axis=0)
+        pairs_ref[index] = jnp.where(inside, toeplitz, HIDDEN_SCORE)
+
+
+def fill_bias(bias_ref, pairs_ref, block, blocks):
+    tokens, band = bias_ref.shape
+    grid_rows, band_rows = tokens // GRID_W, band // GRID_W
+    total_rows = blocks * grid_rows
+    hidden = jnp.full((GRID_W, LANES), HIDDEN_SCORE, jnp.float32)
+    low = low_half(hidden.shape)
+    last = pairs_ref.shape[0] - 1
+    band_first = min(max(block * grid_rows - WIN_ROWS // 2, 0), total_rows - band_rows)
+    for query in range(grid_rows):
+        query_row = block * grid_rows + query
+        window_first = min(max(query_row - WIN_ROWS // 2, 0), total_rows - WIN_ROWS)
+        for pair in range(band_rows // 2):
+            key_row = band_first + 2 * pair
+            valid = [window_first <= key_row + side < window_first + WIN_ROWS for side in range(2)]
+            offset = key_row - query_row + WIN_ROWS - 1
+            if not any(valid):
+                tile = hidden
+            elif 0 <= offset <= last:
+                tile = pairs_ref[offset]
+            else:
+                tile = swap_halves(pairs_ref[last if offset > last else 0])
+            if any(valid) and not all(valid):
+                tile = jnp.where(low if valid[0] else ~low, tile, hidden)
+            bias_ref[
+                query * GRID_W : (query + 1) * GRID_W, pair * LANES : (pair + 1) * LANES
+            ] = tile
+
+
+def with_ones(kv):
+    return jnp.where(low_half(kv.shape), jnp.ones_like(kv), kv)
+
+
+CONTRACT_LANES = (((1,), (1,)), ((), ()))
+
+
+def attend_kernel(
+    received_ref, pairs_ref, out_ref, kv_ref, ones_ref, context_ref, context_ones_ref, query_ref, bias_ref
+):
+    blocks = received_ref.shape[0]
+    tokens = kv_ref.shape[0] // blocks
+    context_tokens = context_ref.shape[0] // blocks
+    grid_rows = tokens // GRID_W
+    total_rows = blocks * grid_rows
+    band_rows = bias_ref.shape[1] // GRID_W
+    parts = out_ref.shape[0] // blocks
+    chunk = tokens // parts
+    half = tokens // 2
+    for block in range(blocks):
+        for first, count, values_ref, values_ones_ref in (
+            (0, tokens, kv_ref, ones_ref),
+            (tokens, context_tokens, context_ref, context_ones_ref),
+        ):
+            kv = received_ref[block, first : first + count, :]
+            values_ref[block * count : (block + 1) * count, :] = kv
+            values_ones_ref[block * count : (block + 1) * count, :] = with_ones(kv)
+        packed = received_ref[block, tokens + context_tokens :, :].astype(jnp.float32)
+        low = low_half(packed.shape)
+        query_ref[block, :half, :] = jnp.where(low, packed, 0.0).astype(jnp.bfloat16)
+        query_ref[block, half:, :] = jnp.where(low, swap_halves(packed), 0.0).astype(jnp.bfloat16)
+    low = low_half((chunk // 2, LANES))
+
+    def body(block, carry):
+        for known in (0, 1, blocks - 1):
+            pl.when(block == known)(
+                functools.partial(fill_bias, bias_ref, pairs_ref, known, blocks)
+            )
+        band = jnp.clip(block * grid_rows - WIN_ROWS // 2, 0, total_rows - band_rows) * GRID_W
+        band = pl.ds(pl.multiple_of(band, GRID_W), band_rows * GRID_W)
+        queries = query_ref[block]
+        context = lax.dot_general(
+            queries, context_ref[...], CONTRACT_LANES, preferred_element_type=jnp.float32
+        )
+        window = (
+            lax.dot_general(
+                queries, kv_ref[band, :], CONTRACT_LANES, preferred_element_type=jnp.float32
+            )
+            + bias_ref[...]
+        )
+        maximum = jnp.maximum(
+            jnp.max(window, axis=-1, keepdims=True), jnp.max(context, axis=-1, keepdims=True)
+        )
+        sums = jnp.dot(
+            jnp.exp(context - maximum).astype(jnp.bfloat16),
+            context_ones_ref[...],
+            preferred_element_type=jnp.float32,
+        ) + jnp.dot(
+            jnp.exp(window - maximum).astype(jnp.bfloat16),
+            ones_ref[band, :],
+            preferred_element_type=jnp.float32,
+        )
+        attended = sums / swap_halves(sums)
+        for part in range(parts):
+            rows = attended[part * chunk : (part + 1) * chunk]
+            out_ref[block * parts + part] = jnp.where(
+                low, swap_halves(rows[: chunk // 2]), rows[chunk // 2 :]
+            ).astype(jnp.bfloat16)
+        return carry
+
+    lax.fori_loop(0, blocks, body, 0)
+
+
+def output_kernel(
+    index_ref, attended_ref, latent_ref, gating_ref, gain_ref, *refs, sp_count, tp_count
+):
+    gate_refs, sources = refs[:tp_count], refs[tp_count : 2 * tp_count]
+    out_ref, gated_ref, weight_ref, semaphores = refs[2 * tp_count :]
+    copies = [
+        pltpu.make_async_copy(source, weight_ref.at[index], semaphores.at[index])
+        for index, source in enumerate(sources)
+    ]
+    for copy in copies:
+        copy.start()
+    half = attended_ref.shape[1]
+    total = None
+    for offset, copy in enumerate(copies):
+        group = index_ref[1] ^ offset
+        for pair in range(sp_count // 2):
+            first = attended_ref[2 * pair * tp_count + group].astype(jnp.float32)
+            second = attended_ref[(2 * pair + 1) * tp_count + group].astype(jnp.float32)
+            lanes = slice(pair * LANES, (pair + 1) * LANES)
+            for side, block in enumerate(head_pair(first, second)):
+                gate = gate_refs[offset][side * half : (side + 1) * half, lanes].astype(jnp.float32)
+                gated_ref[offset, side * half : (side + 1) * half, lanes] = (
+                    gate / (1.0 + jnp.exp(-gate)) * block
+                ).astype(jnp.bfloat16)
+        copy.wait()
+        term = jnp.dot(gated_ref[offset], weight_ref[offset], preferred_element_type=jnp.float32)
+        total = term if total is None else total + term
+    branch = total.astype(jnp.bfloat16).astype(jnp.float32)
+    mean = jnp.sum(branch * branch, axis=-1, keepdims=True) * (1.0 / branch.shape[-1])
+    out_ref[...] = (
+        latent_ref[...].astype(jnp.float32)
+        + gating_ref[...] * (branch * lax.rsqrt(mean + EPSILON)) * gain_ref[...]
+    ).astype(jnp.bfloat16)
+
+
+def in_vmem(array):
+    return pltpu.with_memory_space_constraint(array, pltpu.VMEM)
+
+
+def call(kernel, out_shape, operands, scratch=(), scalars=0, raw=0, flops=0, mib=58):
+    vmem = pl.BlockSpec()
+    smem, hbm = pl.BlockSpec(memory_space=pltpu.SMEM), pl.BlockSpec(memory_space=pl.ANY)
+    return pl.pallas_call(
+        kernel,
+        in_specs=[smem] * scalars + [vmem] * (len(operands) - scalars - raw) + [hbm] * raw,
+        out_specs=jax.tree.map(lambda _: vmem, out_shape),
+        out_shape=out_shape,
+        scratch_shapes=scratch,
+        cost_estimate=pl.CostEstimate(flops=flops, transcendentals=0, bytes_accessed=0),
+        compiler_params=pltpu.CompilerParams(vmem_limit_bytes=mib * 2**20),
+    )(*operands)
+
+
+def shards_by_heads(
+    latent,
+    context,
+    condition,
+    context_condition,
+    gain_pre,
+    gain_post,
+    w_shift,
+    w_scale,
+    w_gate,
+    w_query,
+    w_key,
+    w_value,
+    w_silu,
+    offset_bias,
+    w_out,
+):
+    sp_index = lax.axis_index("sp")
+    tp_index = lax.axis_index("tp")
+    sp_count, tp_count = lax.axis_size("sp"), lax.axis_size("tp")
+    indices = jnp.stack([sp_index, tp_index]).astype(jnp.int32)
+    cols = w_shift.shape[1]
+    tokens, model_width = latent.shape
+    context_tokens = context.shape[0]
+    rows = tokens + context_tokens
+    width = cols // LANES
+    f32, bf16 = jnp.float32, jnp.bfloat16
+    vmem = pltpu.VMEM
+
+    shape = jax.ShapeDtypeStruct
+    across = [(index, index ^ (tp_count // 2)) for index in range(tp_count)]
+    beside = [(index, index ^ 1) for index in range(tp_count)]
+    dma = pltpu.SemaphoreType.DMA
+
+    terms = call(
+        partial_kernel,
+        shape((sp_count * tp_count, 5 * width, LANES), bf16),
+        (
+            indices,
+            condition.reshape(-1, LANES),
+            context_condition.reshape(-1, LANES),
+            w_shift,
+            w_scale,
+            w_gate,
+        ),
+        scratch=[vmem((2, model_width // LANES, LANES), f32)],
+        scalars=1,
+    )
+    terms = lax.all_to_all(terms, ("sp", "tp"), 0, 0, tiled=True)
+    far = lax.ppermute(w_out, "tp", across)
+    near = lax.ppermute(w_out, "tp", beside)
+    norm = call(norm_kernel, shape((rows, LANES), f32), (latent, context), flops=3 * 10**9)
+    table = lax.dynamic_index_in_dim(offset_bias, sp_index, 0, keepdims=False)
+    rows_of, cols_of = table.shape
+    centre = WIN_COLS - 1
+    gap = jnp.zeros((rows_of - 1, (LANES - 2 * cols_of) // 2), f32)
+    base = jnp.concatenate([table[:-1, centre:], gap, table[1:], gap, table[:-1, :centre]], axis=1)
+    pairs = call(bias_kernel, shape((rows_of - 1, GRID_W, LANES), f32), (base,), flops=3 * 10**9)
+    send, hidden, gating = call(
+        functools.partial(project_kernel, sp_count=sp_count, tp_count=tp_count),
+        (
+            shape((sp_count, rows + tokens // 2, LANES), bf16),
+            shape((tokens, model_width), bf16),
+            shape((1, model_width), f32),
+        ),
+        (in_vmem(terms), gain_pre.reshape(1, -1), norm, context, latent, w_key, w_value, w_query),
+        raw=5,
+        scratch=[
+            vmem((context_tokens, model_width), bf16),
+            vmem((tokens, model_width), bf16),
+            vmem(w_key.shape, bf16),
+            vmem(w_value.shape, bf16),
+            vmem(w_query.shape, bf16),
+            vmem((context_tokens, model_width), bf16),
+            vmem((8, model_width), f32),
+            dma((5,)),
+        ],
+        flops=10**9,
+    )
+    received = lax.all_to_all(send, "sp", 0, 0, tiled=True)
+    out_rows = tokens // tp_count
+    gates = call(
+        gate_kernel,
+        (shape((out_rows, cols), bf16),) * tp_count,
+        (indices, hidden, w_silu),
+        scratch=[vmem((tokens, cols), f32)],
+        scalars=1,
+        flops=10**9,
+    )
+    gates = [gates[0]] + [
+        lax.ppermute(gates[offset], "tp", [(index, index ^ offset) for index in range(tp_count)])
+        for offset in range(1, tp_count)
+    ]
+    relayed = lax.ppermute(far, "tp", beside)
+    attended = call(
+        attend_kernel,
+        shape((sp_count * tp_count, out_rows // 2, LANES), bf16),
+        (in_vmem(received), pairs),
+        scratch=[
+            vmem((sp_count * tokens, LANES), bf16),
+            vmem((sp_count * tokens, LANES), bf16),
+            vmem((sp_count * context_tokens, LANES), bf16),
+            vmem((sp_count * context_tokens, LANES), bf16),
+            vmem((sp_count, tokens, LANES), bf16),
+            vmem((tokens, 3 * WIN_ROWS // 2 * GRID_W), f32),
+        ],
+        flops=5 * 10**9,
+    )
+    attended = lax.all_to_all(attended, ("sp", "tp"), 0, 0, tiled=True)
+    own_rows = lax.dynamic_slice_in_dim(latent, tp_index * out_rows, out_rows, 0)
+    return call(
+        functools.partial(output_kernel, sp_count=sp_count, tp_count=tp_count),
+        shape((out_rows, model_width), bf16),
+        (
+            indices,
+            in_vmem(attended),
+            own_rows,
+            gating,
+            gain_post.reshape(1, -1),
+            *gates,
+            w_out,
+            near,
+            far,
+            relayed,
+        ),
+        scratch=[vmem((tp_count, out_rows, cols), bf16), vmem((tp_count, cols, model_width), bf16), dma((tp_count,))],
+        scalars=1,
+        raw=tp_count,
+        flops=10**9,
+    )
 
 
 def solution(mesh):
@@ -210,4 +658,20 @@
         P("tp", None),
     )
     out_specs = P(("sp", "tp"), None)
+    sp_count, tp_count = mesh.shape["sp"], mesh.shape["tp"]
+
+    def shards(*arrays):
+        heads = arrays[13].shape[0]
+        head_width = arrays[6].shape[1] // heads
+        grid_rows = arrays[0].shape[0] // GRID_W
+        one_head_each = (
+            heads == sp_count
+            and sp_count >= 3
+            and tp_count == 4
+            and head_width == HALF
+            and GRID_W == HALF
+            and 2 * grid_rows == WIN_ROWS
+        )
+        return (shards_by_heads if one_head_each else shards_by_rows)(*arrays)
+
     return jax.shard_map(shards, mesh=mesh, in_specs=in_specs, out_specs=out_specs, check_vma=False)

time: 196 us -> 121 us (0.62)
  local copies, waits for them, and re-layouts: 57.6 us -> 2.61 us
  blocking collectives: 44.1 us -> 0 us
  waiting for transfers between devices: 22.2 us -> 64.5 us
  Pallas kernels: 0 us -> 34.2 us
  matrix products: 31.8 us -> 0 us
  other arithmetic: 18.6 us -> 0.59 us
  between operations: 13.8 us -> 0.08 us
  starting transfers between devices: 6.83 us -> 19 us
    all_to_all x0 -> x3, waiting for transfers between devices: none -> 61.3 us  [the longest x1 38 us: shards_by_heads(): terms = lax.all_to_all(terms, ('sp', 'tp'), 0, 0, tiled=True)]
    psum x1 -> x0, blocking collectives: 38.9 us -> none  [shards(): summed = lax.psum(partial_value, 'sp')]
    pallas_call x0 -> x7, Pallas kernels: none -> 34.2 us  [call(): pl.pallas_call(kernel, in_specs=[smem] * scalars + [vmem] * (len(operands...]
    gather x2 -> x0, local copies, waits for them, and re-layouts: 33.9 us -> none  [shards(): jnp.take(flat_rows, position.reshape(-1), axis=0)]
    dot_general x13 -> x0, matrix products: 31.8 us -> none  [the longest x6 9.43 us: product(): return jnp.dot(left, right, preferred_element_type=jnp.float32)]
    reduce_scatter x1 -> x0, waiting for transfers between devices: 22.2 us -> none  [shards(): lax.psum_scatter(product(gated_heads, w_out).astype(jnp.bfloat16), 'tp',...]
    all_to_all x0 -> x3, starting transfers between devices: none -> 13.6 us  [the longest x1 5.03 us: shards_by_heads(): received = lax.all_to_all(send, 'sp', 0, 0, tiled=True)]
    slice x4 -> x2, local copies, waits for them, and re-layouts: 12.8 us -> 0.08 us  [the longest x1 0.07 us: shards_by_heads(): table[:-1, centre:]]
  transfers between devices with their start and end apart: 4 -> 9, of which waited for: 1 -> 5; matrix products, arithmetic and copies ran while one was open for 38% -> 3% of each run, Pallas kernels for 0% -> 23%
where the time goes in v2:
time: 121 us
  waiting for transfers between devices  64.5 us (53%)
  Pallas kernels  34.2 us (28%)
  starting transfers between devices  19 us (16%)
  local copies, waits for them, and re-layouts  2.61 us (2%)
    all_to_all x1, waiting for transfers between devices, shards_by_heads(): terms = lax.all_to_all(terms, ('sp', 'tp'), 0, 0, tiled=True)  38 us
    pallas_call x7, Pallas kernels, call(): pl.pallas_call(kernel, in_specs=[smem] * scalars + [vmem] * (len(operands...  34.2 us
    all_to_all x1, waiting for transfers between devices, shards_by_heads(): received = lax.all_to_all(send, 'sp', 0, 0, tiled=True)  22.9 us
    all_to_all x1, starting transfers between devices, shards_by_heads(): received = lax.all_to_all(send, 'sp', 0, 0, tiled=True)  5.03 us
    all_to_all x1, starting transfers between devices, shards_by_heads(): terms = lax.all_to_all(terms, ('sp', 'tp'), 0, 0, tiled=True)  4.92 us
    all_to_all x1, starting transfers between devices, shards_by_heads(): attended = lax.all_to_all(attended, ('sp', 'tp'), 0, 0, tiled=True)  3.65 us
    ppermute x3, waiting for transfers between devices, shards_by_heads(): lax.ppermute(gates[offset], 'tp', [(index, index ^ offset) for index in r...  3.2 us
    ppermute x1, starting transfers between devices, shards_by_heads(): far = lax.ppermute(w_out, 'tp', across)  2.97 us
  transfers between devices with their start and end apart: 9, of which 5 were waited for; matrix products, arithmetic and copies ran while one was open for 3% of the time, Pallas kernels for 23%

profile of v2, /device:TPU:0, one launch (start us, length us, event | category | flops | bytes accessed | tf_op | source)
XLA Modules:
  0.0 121.0 jit_solution(6745387849757715774)
XLA Ops:
  0.0 3.0 %collective-permute-start.4 = (bf16[512,2048]{1,0:T(8,128)(2,1)}, bf16[512,2048]{1,0:T(8,128)(2,1)}, u32[]{:S(2)}, u32[]{:S(2)}) collective-permute-start(bf16[512,2048]{1,0:T(8,128)(2,1)} %refs_4_.1), channel_id=1, source_target_pairs={{0,2},{1,3},{2,0},{3,1},{4,6},{5,7},{6,4},{7,5},{8,10},{9,11},{10,... | collective-permute-start | bytes 6291464 | tf_op jit(solution)/shard_map/ppermute | solution.py:559
  3.0 0.6 pad_add_fusion.index_ref
  3.6 2.2 %shard_map.145 = bf16[32,20,128]{2,1,0:T(8,128)(2,1)} custom-call(s32[2]{0:T(128)} %pad_add_fusion.index_ref, bf16[16,128]{1,0:T(8,128)(2,1)} %bitcast.15, bf16[16,128]{1,0:T(8,128)(2,1)} %bitcast.16, bf16[256,512]{1,0:T(8,128)(2,1)} %shift_ref.1, bf16[256,512]{1,0:T(8,128)(2,1)} %scale_ref.1, bf16[256,512]{1,0:T(8,128)(2,1)} %gate_ref.1), custom_call_target="tpu_custom_call" | custom-call | tf_op jit(solution)/shard_map/pallas_call | solution.py:499
  5.8 4.9 %all-to-all-start = ((bf16[32,20,128]{2,1,0:T(8,128)(2,1)}), bf16[32,20,128]{2,1,0:T(8,128)(2,1)S(1)}, u32[]{:S(2)}, u32[]{:S(2)}) async-start(bf16[32,20,128]{2,1,0:T(8,128)(2,1)} %shard_map.145), calls=%async_computation | async-start | bytes 393216 | tf_op jit(solution)/shard_map/all_to_all | solution.py:558
  10.7 3.4 %shard_map.146.norm_ref = f32[384,128]{1,0:T(8,128)} custom-call(bf16[256,2048]{1,0:T(8,128)(2,1)} %latent_hbm.1, bf16[128,2048]{1,0:T(8,128)(2,1)} %context_hbm.1), custom_call_target="tpu_custom_call" | custom-call | flops 3000000000 | tf_op jit(solution)/shard_map/pallas_call | solution.py:499
  14.1 38.0 %all-to-all-done.terms_ref = bf16[32,20,128]{2,1,0:T(8,128)(2,1)S(1)} async-done(((bf16[32,20,128]{2,1,0:T(8,128)(2,1)}), bf16[32,20,128]{2,1,0:T(8,128)(2,1)S(1)}, u32[]{:S(2)}, u32[]{:S(2)}) %all-to-all-start) | async-done | bytes 163872 | tf_op jit(solution)/shard_map/all_to_all | solution.py:558
  52.1 7.1 %shard_map.147 = (bf16[8,512,128]{2,1,0:T(8,128)(2,1)}, bf16[256,2048]{1,0:T(8,128)(2,1)}, f32[1,2048]{1,0:T(1,128)}) custom-call(bf16[32,20,128]{2,1,0:T(8,128)(2,1)S(1)} %all-to-all-done.terms_ref, f32[1,2048]{1,0:T(1,128)} %bitcast.13, f32[384,128]{1,0:T(8,128)} %shard_map.146.norm_ref, bf16[128,2048]{1,0:T(8,128)(2,1)} %context_hbm.1, ...), custom_call_target="tpu_custom_call" | custom-call | flops 1000000000 | tf_op jit(solution)/shard_map/pallas_call | solution.py:499
  59.3 5.0 %all-to-all-start.1 = ((bf16[8,512,128]{2,1,0:T(8,128)(2,1)}), bf16[8,512,128]{2,1,0:T(8,128)(2,1)S(1)}, u32[]{:S(2)}, u32[]{:S(2)}) async-start(bf16[8,512,128]{2,1,0:T(8,128)(2,1)} %get-tuple-element.12), calls=%async_computation.1 | async-start | bytes 2097152 | tf_op jit(solution)/shard_map/all_to_all | solution.py:589
  64.4 0.5 collective-permute-start.5
  64.9 0.1 slice.16
  65.0 0.7 concatenate.3.base_ref
  65.7 1.7 %shard_map.148.pairs_ref = f32[14,64,128]{2,1,0:T(8,128)} custom-call(f32[14,128]{1,0:T(8,128)} %concatenate.3.base_ref), custom_call_target="tpu_custom_call" | custom-call | flops 3000000000 | tf_op jit(solution)/shard_map/pallas_call | solution.py:499
  67.4 22.9 %all-to-all-done.1.received_ref = bf16[8,512,128]{2,1,0:T(8,128)(2,1)S(1)} async-done(((bf16[8,512,128]{2,1,0:T(8,128)(2,1)}), bf16[8,512,128]{2,1,0:T(8,128)(2,1)S(1)}, u32[]{:S(2)}, u32[]{:S(2)}) %all-to-all-start.1) | async-done | bytes 1048608 | tf_op jit(solution)/shard_map/all_to_all | solution.py:589
  90.2 10.4 %shard_map.149 = bf16[32,32,128]{2,1,0:T(8,128)(2,1)} custom-call(bf16[8,512,128]{2,1,0:T(8,128)(2,1)S(1)} %all-to-all-done.1.received_ref, f32[14,64,128]{2,1,0:T(8,128)} %shard_map.148.pairs_ref), custom_call_target="tpu_custom_call" | custom-call | flops 5000000000 | tf_op jit(solution)/shard_map/pallas_call | solution.py:499
  100.7 3.7 %all-to-all-start.2 = ((bf16[32,32,128]{2,1,0:T(8,128)(2,1)}), bf16[32,32,128]{2,1,0:T(8,128)(2,1)S(1)}, u32[]{:S(2)}, u32[]{:S(2)}) async-start(bf16[32,32,128]{2,1,0:T(8,128)(2,1)} %shard_map.149), calls=%async_computation.2 | async-start | bytes 524288 | tf_op jit(solution)/shard_map/all_to_all | solution.py:618
  104.3 3.3 %shard_map.150 = (bf16[64,512]{1,0:T(8,128)(2,1)}, bf16[64,512]{1,0:T(8,128)(2,1)}, bf16[64,512]{1,0:T(8,128)(2,1)}, bf16[64,512]{1,0:T(8,128)(2,1)}) custom-call(s32[2]{0:T(128)} %pad_add_fusion.index_ref, bf16[256,2048]{1,0:T(8,128)(2,1)} %get-tuple-element.14.hidden_ref, bf16[2048,512]{1,0:T(8,128)(2,1)} %weight_ref.1), custom_call_target="tpu_custom_call" | custom-call | flops 1000000000 | tf_op jit(solution)/shard_map/pallas_call | solution.py:499
  107.7 0.3 collective-permute-start
  107.9 1.6 %collective-permute-start.1 = (bf16[64,512]{1,0:T(8,128)(2,1)}, bf16[64,512]{1,0:T(8,128)(2,1)S(1)}, u32[]{:S(2)}, u32[]{:S(2)}) collective-permute-start(bf16[64,512]{1,0:T(8,128)(2,1)} %get-tuple-element.17), channel_id=1, source_target_pairs={{0,2},{1,3},{2,0},{3,1},{4,6},{5,7},{6,4},{7,5},{8,10},{9,11},{10,... | collective-permute-start | bytes 196616 | tf_op jit(solution)/shard_map/ppermute | solution.py:600
  109.5 1.7 %constant_dynamic-slice_fusion.latent_ref = bf16[64,2048]{1,0:T(8,128)(2,1)} fusion(bf16[256,2048]{1,0:T(8,128)(2,1)} %latent_hbm.1, s32[]{:T(128)S(6)} %select_n.8), kind=kLoop, calls=%fused_computation.2 | loop fusion | bytes 524292 | tf_op jit(solution)/shard_map/dynamic_slice | solution.py:619
  111.2 1.8 %collective-permute-done.1.refs_2_ = bf16[64,512]{1,0:T(8,128)(2,1)S(1)} collective-permute-done((bf16[64,512]{1,0:T(8,128)(2,1)}, bf16[64,512]{1,0:T(8,128)(2,1)S(1)}, u32[]{:S(2)}, u32[]{:S(2)}) %collective-permute-start.1) | collective-permute-done | bytes 65568 | tf_op jit(solution)/shard_map/ppermute | solution.py:600
  113.1 1.4 %collective-permute-done.2.refs_3_ = bf16[64,512]{1,0:T(8,128)(2,1)S(1)} collective-permute-done((bf16[64,512]{1,0:T(8,128)(2,1)}, bf16[64,512]{1,0:T(8,128)(2,1)S(1)}, u32[]{:S(2)}, u32[]{:S(2)}) %collective-permute-start.2) | collective-permute-done | bytes 65568 | tf_op jit(solution)/shard_map/ppermute | solution.py:600
  114.4 0.5 all-to-all-done.2.attended_ref
  114.9 0.1 copy-done.4
  115.1 5.9 %shard_map.151 = bf16[64,2048]{1,0:T(8,128)(2,1)} custom-call(s32[2]{0:T(128)} %pad_add_fusion.index_ref, bf16[32,32,128]{2,1,0:T(8,128)(2,1)S(1)} %all-to-all-done.2.attended_ref, bf16[64,2048]{1,0:T(8,128)(2,1)} %constant_dynamic-slice_fusion.latent_ref, f32[1,2048]{1,0:T(1,128)} %get-tuple-element.13.gating_ref, f32[1,2048]{1,0:T(1,128)} %bitcast.14, ...), custom_call_target="tpu_custom_call" | custom-call | flops 1000000000 | tf_op jit(solution)/shard_map/pallas_call | solution.py:499
  (19 shorter events, 0.1 us)
Async XLA Ops:
  0.0 64.9 %copy-start = (f32[8,15,31]{2,0,1:T(8,128)S(1)}, f32[8,15,31]{2,0,1:T(8,128)}, u32[]{:S(2)}) copy-start(f32[8,15,31]{2,0,1:T(8,128)} %param.28) | copy-start | bytes 44644
  0.0 64.4 %collective-permute-start.4 = (bf16[512,2048]{1,0:T(8,128)(2,1)}, bf16[512,2048]{1,0:T(8,128)(2,1)}, u32[]{:S(2)}, u32[]{:S(2)}) collective-permute-start(bf16[512,2048]{1,0:T(8,128)(2,1)} %refs_4_.1), channel_id=1, source_target_pairs={{0,2},{1,3},{2,0},{3,1},{4,6},{5,7},{6,4},{7,5},{8,10},{9,11},{10,... | collective-permute-start | bytes 6291464 | tf_op jit(solution)/shard_map/ppermute | solution.py:559
  5.8 46.3 %all-to-all-start = ((bf16[32,20,128]{2,1,0:T(8,128)(2,1)}), bf16[32,20,128]{2,1,0:T(8,128)(2,1)S(1)}, u32[]{:S(2)}, u32[]{:S(2)}) async-start(bf16[32,20,128]{2,1,0:T(8,128)(2,1)} %shard_map.145), calls=%async_computation | async-start | bytes 393216 | tf_op jit(solution)/shard_map/all_to_all | solution.py:558
  59.3 5.0 %copy-start.1 = (bf16[512,2048]{1,0:T(8,128)(2,1)S(1)}, bf16[512,2048]{1,0:T(8,128)(2,1)}, u32[]{:S(2)}) copy-start(bf16[512,2048]{1,0:T(8,128)(2,1)} %refs_4_.1) | copy-start | bytes 6291460
  59.3 30.9 %all-to-all-start.1 = ((bf16[8,512,128]{2,1,0:T(8,128)(2,1)}), bf16[8,512,128]{2,1,0:T(8,128)(2,1)S(1)}, u32[]{:S(2)}, u32[]{:S(2)}) async-start(bf16[8,512,128]{2,1,0:T(8,128)(2,1)} %get-tuple-element.12), calls=%async_computation.1 | async-start | bytes 2097152 | tf_op jit(solution)/shard_map/all_to_all | solution.py:589
  64.3 50.1 %collective-permute-start.3 = (bf16[512,2048]{1,0:T(8,128)(2,1)S(1)}, bf16[512,2048]{1,0:T(8,128)(2,1)}, u32[]{:S(2)}, u32[]{:S(2)}) collective-permute-start(bf16[512,2048]{1,0:T(8,128)(2,1)S(1)} %copy-done.1), channel_id=1, source_target_pairs={{0,1},{1,0},{2,3},{3,2},{4,5},{5,4},{6,7},{7,6},{8,9},{9,8},{10,11... | collective-permute-start | bytes 6291464 | tf_op jit(solution)/shard_map/ppermute | solution.py:560
  64.4 50.5 %collective-permute-start.5 = (bf16[512,2048]{1,0:T(8,128)(2,1)}, bf16[512,2048]{1,0:T(8,128)(2,1)}, u32[]{:S(2)}, u32[]{:S(2)}) collective-permute-start(bf16[512,2048]{1,0:T(8,128)(2,1)} %collective-permute-done.4.refs_6_), channel_id=1, source_target_pairs={{0,1},{1,0},{2,3},{3,2},{4,5},{5,4},{6,7},{7,6},{8,9},{9,8},{10,11... | collective-permute-start | bytes 6291464 | tf_op jit(solution)/shard_map/ppermute | solution.py:603
  100.7 14.2 %all-to-all-start.2 = ((bf16[32,32,128]{2,1,0:T(8,128)(2,1)}), bf16[32,32,128]{2,1,0:T(8,128)(2,1)S(1)}, u32[]{:S(2)}, u32[]{:S(2)}) async-start(bf16[32,32,128]{2,1,0:T(8,128)(2,1)} %shard_map.149), calls=%async_computation.2 | async-start | bytes 524288 | tf_op jit(solution)/shard_map/all_to_all | solution.py:618
  107.7 3.6 %collective-permute-start = (bf16[64,512]{1,0:T(8,128)(2,1)}, bf16[64,512]{1,0:T(8,128)(2,1)S(1)}, u32[]{:S(2)}, u32[]{:S(2)}) collective-permute-start(bf16[64,512]{1,0:T(8,128)(2,1)} %get-tuple-element.16), channel_id=1, source_target_pairs={{0,1},{1,0},{2,3},{3,2},{4,5},{5,4},{6,7},{7,6},{8,9},{9,8},{10,11... | collective-permute-start | bytes 196616 | tf_op jit(solution)/shard_map/ppermute | solution.py:600
  107.9 5.2 %collective-permute-start.1 = (bf16[64,512]{1,0:T(8,128)(2,1)}, bf16[64,512]{1,0:T(8,128)(2,1)S(1)}, u32[]{:S(2)}, u32[]{:S(2)}) collective-permute-start(bf16[64,512]{1,0:T(8,128)(2,1)} %get-tuple-element.17), channel_id=1, source_target_pairs={{0,2},{1,3},{2,0},{3,1},{4,6},{5,7},{6,4},{7,5},{8,10},{9,11},{10,... | collective-permute-start | bytes 196616 | tf_op jit(solution)/shard_map/ppermute | solution.py:600
  109.5 4.9 %collective-permute-start.2 = (bf16[64,512]{1,0:T(8,128)(2,1)}, bf16[64,512]{1,0:T(8,128)(2,1)S(1)}, u32[]{:S(2)}, u32[]{:S(2)}) collective-permute-start(bf16[64,512]{1,0:T(8,128)(2,1)} %get-tuple-element.18), channel_id=1, source_target_pairs={{0,3},{1,2},{2,1},{3,0},{4,7},{5,6},{6,5},{7,4},{8,11},{9,10},{10,... | collective-permute-start | bytes 196616 | tf_op jit(solution)/shard_map/ppermute | solution.py:600
  111.2 3.7 %copy-start.2 = (bf16[64,512]{1,0:T(8,128)(2,1)}, bf16[64,512]{1,0:T(8,128)(2,1)S(1)}, u32[]{:S(2)}) copy-start(bf16[64,512]{1,0:T(8,128)(2,1)S(1)} %collective-permute-done.refs_1_) | copy-start | bytes 196612
  113.1 1.8 %copy-start.3 = (bf16[64,512]{1,0:T(8,128)(2,1)}, bf16[64,512]{1,0:T(8,128)(2,1)S(1)}, u32[]{:S(2)}) copy-start(bf16[64,512]{1,0:T(8,128)(2,1)S(1)} %collective-permute-done.1.refs_2_) | copy-start | bytes 196612
  114.4 0.6 copy-start.4

commit v3 on v2

--- a/solution.py
+++ b/solution.py
@@ -214,12 +214,14 @@
     )
 
 
-def partial_kernel(index_ref, condition_ref, context_ref, shift_ref, scale_ref, gate_ref, out_ref, active_ref):
+def partial_kernel(
+    condition_ref, context_ref, shift_ref, scale_ref, gate_ref, out_ref, active_ref
+):
     rows = shift_ref.shape[0] // LANES
     for kind, source in enumerate((condition_ref, context_ref)):
         values = source[...].astype(jnp.float32)
         active_ref[kind] = values / (1.0 + jnp.exp(-values))
-    own = pl.ds(index_ref[0] * rows, rows)
+    own = pl.ds(lax.axis_index("sp") * rows, rows)
     vectors = [active_ref[kind, own, :].astype(jnp.bfloat16) for kind in range(2)]
     width = shift_ref.shape[1] // LANES
     row = 0
@@ -239,43 +241,83 @@
                 row += 1
 
 
-def norm_kernel(latent_ref, context_ref, out_ref):
+def norms(values):
+    mean = jnp.sum(values * values, axis=-1, keepdims=True) * (1.0 / values.shape[-1])
+    return lax.rsqrt(mean + EPSILON)
+
+
+def norm_kernel(
+    latent_ref, before_ref, after_ref, context_hbm, out_ref, before_out, after_out, half_ref, semaphore
+):
+    count = half_ref.shape[0]
+    first = pl.multiple_of(lax.axis_index("tp") % 2 * count, count)
+    copy = pltpu.make_async_copy(context_hbm.at[pl.ds(first, count)], half_ref, semaphore)
+    copy.start()
+    before_out[...] = jnp.broadcast_to(before_ref[...], before_out.shape)
+    after_out[...] = jnp.broadcast_to(after_ref[...], after_out.shape)
     step = 32
-    first = 0
-    for source in (latent_ref, context_ref):
-
-        def body(index, carry, source=source, first=first):
-            start = pl.multiple_of(index * step, step)
-            values = source[pl.ds(start, step), :].astype(jnp.float32)
-            mean = jnp.sum(values * values, axis=-1, keepdims=True) * (1.0 / values.shape[-1])
-            out_ref[pl.ds(pl.multiple_of(first + start, step), step), :] = jnp.broadcast_to(
-                lax.rsqrt(mean + EPSILON), (step, LANES)
-            )
-            return carry
-
-        lax.fori_loop(0, source.shape[0] // step, body, 0)
-        first += source.shape[0]
-
-
-def project_kernel(
-    terms_ref, gain_ref, norm_ref, context_hbm, latent_hbm, key_hbm, value_hbm, query_hbm,
-    send_ref, hidden_ref, gating_ref,
-    context_ref, latent_ref, key_ref, value_ref, query_ref, context_hidden_ref, vectors_ref, semaphores,
-    *, sp_count, tp_count
-):
-    pairs = (
-        (context_hbm, context_ref),
-        (latent_hbm, latent_ref),
-        (key_hbm, key_ref),
-        (value_hbm, value_ref),
-        (query_hbm, query_ref),
-    )
+
+    def body(index, carry):
+        rows = pl.ds(pl.multiple_of(index * step, step), step)
+        norm = norms(latent_ref[rows, :].astype(jnp.float32))
+        out_ref[rows, :] = jnp.broadcast_to(norm, (step, LANES))
+        return carry
+
+    lax.fori_loop(0, latent_ref.shape[0] // step, body, 0)
+    copy.wait()
+
+
+def modulate_rows(source, target, first, count, vectors_ref, gain_ref, kind, norm_ref=None):
+    factor = gain_ref[:1, :] * (1.0 + vectors_ref[2 + kind : 3 + kind, :])
+    shift = vectors_ref[kind : kind + 1, :]
+    step = 32
+
+    def body(index, carry):
+        start = pl.multiple_of(index * step, step)
+        values = source[pl.ds(start, step), :].astype(jnp.float32)
+        norm = norms(values) if norm_ref is None else norm_ref[pl.ds(start, step), :][:, :1]
+        target[pl.ds(pl.multiple_of(first + start, step), step), :] = (
+            values * norm * factor + shift
+        ).astype(jnp.bfloat16)
+        return carry
+
+    lax.fori_loop(0, count // step, body, 0)
+
+
+def start_all(pairs, semaphores):
     copies = [
         pltpu.make_async_copy(source, target, semaphores.at[index])
         for index, (source, target) in enumerate(pairs)
     ]
     for copy in copies:
         copy.start()
+    return copies
+
+
+def project_kernel(
+    terms_ref, latent_hbm, norm_hbm, gain_hbm, key_hbm, value_hbm, query_hbm,
+    send_hbm, hidden_hbm, vectors_hbm,
+    latent_ref, norm_ref, gain_ref, key_ref, value_ref, query_ref,
+    send_ref, hidden_ref, vectors_ref, loads, stores,
+    *, sp_count, tp_count
+):
+    copies = start_all(
+        (
+            (norm_hbm, norm_ref),
+            (gain_hbm, gain_ref),
+            (latent_hbm, latent_ref),
+            (key_hbm, key_ref),
+            (value_hbm, value_ref),
+            (query_hbm, query_ref),
+        ),
+        loads,
+    )
+    saves = []
+
+    def save(source, target):
+        saves.append(pltpu.make_async_copy(source, target, stores.at[len(saves)]))
+        saves[-1].start()
+
     cols = key_ref.shape[1]
     width = cols // LANES
     for part in range(tp_count):
@@ -287,69 +329,96 @@
                 first = part * cols + lane * LANES
                 row = index * width + lane
                 vectors_ref[index : index + 1, first : first + LANES] = total[row : row + 1]
-    gating_ref[...] = vectors_ref[4:5, :]
+    vectors_ref[5:, :] = jnp.zeros((vectors_ref.shape[0] - 5, vectors_ref.shape[1]), jnp.float32)
+    save(vectors_ref, vectors_hbm)
     tokens = latent_ref.shape[0]
-    count = context_ref.shape[0]
-
-    def modulate_rows(source, target, first, kind):
-        factor = gain_ref[...] * (1.0 + vectors_ref[2 + kind : 3 + kind, :])
-        shift = vectors_ref[kind : kind + 1, :]
-        step = 32
-
-        def body(index, carry):
-            start = pl.multiple_of(index * step, step)
-            norm = norm_ref[pl.ds(pl.multiple_of(first + start, step), step), :][:, :1]
-            rows = source[pl.ds(start, step), :].astype(jnp.float32) * norm * factor + shift
-            target[pl.ds(start, step), :] = rows.astype(jnp.bfloat16)
-            return carry
-
-        lax.fori_loop(0, source.shape[0] // step, body, 0)
-
-    def store(keys, values, first):
-        for pair in range(width):
-            lanes = slice(pair * LANES, (pair + 1) * LANES)
-            for head, kv in enumerate(head_pair(keys[:, lanes], values[:, lanes])):
-                send_ref[2 * pair + head, first : first + keys.shape[0], :] = kv.astype(jnp.bfloat16)
-
-    copies[0].wait()
-    modulate_rows(context_ref, context_hidden_ref, tokens, 1)
-    copies[1].wait()
-    modulate_rows(latent_ref, hidden_ref, 0, 0)
-    copies[2].wait()
-    context_keys = jnp.dot(context_hidden_ref[...], key_ref[...], preferred_element_type=jnp.float32)
+    half = tokens // 2
+    for copy in copies[:3]:
+        copy.wait()
+    modulate_rows(latent_ref, hidden_ref, 0, tokens, vectors_ref, gain_ref, 0, norm_ref)
+    save(hidden_ref, hidden_hbm)
+    copies[3].wait()
     keys = jnp.dot(hidden_ref[...], key_ref[...], preferred_element_type=jnp.float32)
-    copies[3].wait()
-    values = jnp.dot(context_hidden_ref[...], value_ref[...], preferred_element_type=jnp.float32)
-    store(context_keys, values, tokens)
+    copies[4].wait()
     values = jnp.dot(hidden_ref[...], value_ref[...], preferred_element_type=jnp.float32)
-    store(keys, values, 0)
-    copies[4].wait()
+    for pair in range(width):
+        lanes = slice(pair * LANES, (pair + 1) * LANES)
+        for head, kv in enumerate(head_pair(keys[:, lanes], values[:, lanes])):
+            send_ref[2 * pair + head, :tokens, :] = kv.astype(jnp.bfloat16)
+    save(send_ref.at[:, pl.ds(0, tokens)], send_hbm.at[:, pl.ds(0, tokens)])
+    copies[5].wait()
     queries = jnp.dot(hidden_ref[...], query_ref[...], preferred_element_type=jnp.float32)
-    half = tokens // 2
     for pair in range(width):
         lanes = slice(pair * LANES, (pair + 1) * LANES)
         block = queries[:, lanes].astype(jnp.bfloat16).astype(jnp.float32) * HALF**-0.5
         for head, packed in enumerate(head_pair(block[:half], block[half:])):
-            send_ref[2 * pair + head, tokens + count :, :] = packed.astype(jnp.bfloat16)
-
-
-def gate_kernel(index_ref, hidden_ref, weight_ref, *out_refs):
+            send_ref[2 * pair + head, tokens:, :] = packed.astype(jnp.bfloat16)
+    save(send_ref.at[:, pl.ds(tokens, half)], send_hbm.at[:, pl.ds(tokens, half)])
+    for copy in saves:
+        copy.wait()
+
+
+def context_kernel(*refs, sp_count, sources):
+    heads = sp_count // 2
+    source_refs, (vectors_hbm, gain_hbm, key_hbm, value_hbm) = refs[:sources], refs[sources : sources + 4]
+    outs, refs = refs[sources + 4 : sources + 4 + heads], refs[sources + 4 + heads :]
+    (vectors_ref, gain_ref, key_ref, value_ref, hidden_ref, send_ref, loads, stores) = refs
+    own = lax.axis_index("sp")
+    width = key_ref.shape[1]
+    cols = pl.ds(pl.multiple_of(own // heads * width, width), width)
+    copies = start_all(
+        (
+            (vectors_hbm, vectors_ref),
+            (gain_hbm, gain_ref),
+            (key_hbm.at[:, cols], key_ref),
+            (value_hbm.at[:, cols], value_ref),
+        ),
+        loads,
+    )
+    for copy in copies[:2]:
+        copy.wait()
+    first = 0
+    for source in source_refs:
+        modulate_rows(source, hidden_ref, first, source.shape[0], vectors_ref, gain_ref, 1)
+        first += source.shape[0]
+    copies[2].wait()
+    keys = jnp.dot(hidden_ref[...], key_ref[...], preferred_element_type=jnp.float32)
+    copies[3].wait()
+    values = jnp.dot(hidden_ref[...], value_ref[...], preferred_element_type=jnp.float32)
+    for pair in range(heads // 2):
+        lanes = slice(pair * LANES, (pair + 1) * LANES)
+        for head, kv in enumerate(head_pair(keys[:, lanes], values[:, lanes])):
+            send_ref[2 * pair + head] = kv.astype(jnp.bfloat16)
+    for copy in start_all(
+        [(send_ref.at[own % heads ^ offset], out) for offset, out in enumerate(outs)], stores
+    ):
+        copy.wait()
+
+
+def gate_kernel(hidden_ref, weight_ref, *out_refs):
     *out_refs, rows_ref = out_refs
     rows_ref[...] = jnp.dot(hidden_ref[...], weight_ref[...], preferred_element_type=jnp.float32)
     for offset, out_ref in enumerate(out_refs):
         count = out_ref.shape[0]
-        first = pl.multiple_of((index_ref[1] ^ offset) * count, count)
+        first = pl.multiple_of((lax.axis_index("tp") ^ offset) * count, count)
         out_ref[...] = rows_ref[pl.ds(first, count), :].astype(jnp.bfloat16)
 
 
-def bias_kernel(base_ref, pairs_ref):
+def bias_kernel(table_ref, pairs_ref, rows_ref):
+    rows_ref[...] = jnp.zeros_like(rows_ref)
+    own = pl.ds(lax.axis_index("sp"), 1)
+    for index in range(table_ref.shape[0]):
+        rows_ref[index : index + 1, : table_ref.shape[2]] = table_ref[index, own, :]
     column = lax.broadcasted_iota(jnp.int32, (GRID_W, LANES), 0)
     key_column = lax.broadcasted_iota(jnp.int32, (GRID_W, LANES), 1) % GRID_W
     first_column = jnp.clip(column - WIN_COLS // 2, 0, GRID_W - WIN_COLS)
     inside = (key_column >= first_column) & (key_column < first_column + WIN_COLS)
-    for index in range(base_ref.shape[0]):
-        row = jnp.broadcast_to(base_ref[index : index + 1, :], (GRID_W, LANES))
-        toeplitz = pltpu.roll(row, 0, 1, stride=1, stride_axis=0)
+    count = pairs_ref.shape[0]
+    first = pltpu.roll(rows_ref[...], LANES - WIN_COLS + 1, 1)
+    second = pltpu.roll(rows_ref[...], HALF - WIN_COLS + 1, 1)
+    for index in range(count):
+        row = first[index : index + 1] + second[index + 1 : index + 2]
+        toeplitz = pltpu.roll(jnp.broadcast_to(row, (GRID_W, LANES)), 0, 1, stride=1, stride_axis=0)
         pairs_ref[index] = jnp.where(inside, toeplitz, HIDDEN_SCORE)
 
 
@@ -388,49 +457,50 @@
 CONTRACT_LANES = (((1,), (1,)), ((), ()))
 
 
-def attend_kernel(
-    received_ref, pairs_ref, out_ref, kv_ref, ones_ref, context_ref, context_ones_ref, query_ref, bias_ref
-):
+def attend_kernel(received_ref, *refs):
+    *sources, pairs_hbm, out_hbm = refs[:-8]
+    pairs_ref, out_ref, ones_ref, context_ref, context_ones_ref, query_ref, bias_ref, semaphores = refs[-8:]
     blocks = received_ref.shape[0]
-    tokens = kv_ref.shape[0] // blocks
-    context_tokens = context_ref.shape[0] // blocks
-    grid_rows = tokens // GRID_W
-    total_rows = blocks * grid_rows
-    band_rows = bias_ref.shape[1] // GRID_W
+    tokens = query_ref.shape[1]
+    rows = context_ref.shape[0] // len(sources)
+    loads = start_all([(pairs_hbm, pairs_ref)], semaphores)
+    for index, source in enumerate(sources):
+        kv = source[...]
+        context_ref[index * rows : (index + 1) * rows, :] = kv
+        context_ones_ref[index * rows : (index + 1) * rows, :] = with_ones(kv)
     parts = out_ref.shape[0] // blocks
     chunk = tokens // parts
     half = tokens // 2
     for block in range(blocks):
-        for first, count, values_ref, values_ones_ref in (
-            (0, tokens, kv_ref, ones_ref),
-            (tokens, context_tokens, context_ref, context_ones_ref),
-        ):
-            kv = received_ref[block, first : first + count, :]
-            values_ref[block * count : (block + 1) * count, :] = kv
-            values_ones_ref[block * count : (block + 1) * count, :] = with_ones(kv)
-        packed = received_ref[block, tokens + context_tokens :, :].astype(jnp.float32)
+        ones_ref[block * tokens : (block + 1) * tokens, :] = with_ones(received_ref[block, :tokens, :])
+        packed = received_ref[block, tokens:, :].astype(jnp.float32)
         low = low_half(packed.shape)
         query_ref[block, :half, :] = jnp.where(low, packed, 0.0).astype(jnp.bfloat16)
         query_ref[block, half:, :] = jnp.where(low, swap_halves(packed), 0.0).astype(jnp.bfloat16)
+    for load in loads:
+        load.wait()
     low = low_half((chunk // 2, LANES))
-
-    def body(block, carry):
-        for known in (0, 1, blocks - 1):
-            pl.when(block == known)(
-                functools.partial(fill_bias, bias_ref, pairs_ref, known, blocks)
-            )
-        band = jnp.clip(block * grid_rows - WIN_ROWS // 2, 0, total_rows - band_rows) * GRID_W
-        band = pl.ds(pl.multiple_of(band, GRID_W), band_rows * GRID_W)
+    saves = []
+    for block in range(blocks):
+        if block in (0, 1, blocks - 1):
+            fill_bias(bias_ref, pairs_ref, block, blocks)
+        band = min(max(block - 1, 0), blocks - 3)
         queries = query_ref[block]
         context = lax.dot_general(
             queries, context_ref[...], CONTRACT_LANES, preferred_element_type=jnp.float32
         )
-        window = (
-            lax.dot_general(
-                queries, kv_ref[band, :], CONTRACT_LANES, preferred_element_type=jnp.float32
-            )
-            + bias_ref[...]
-        )
+        window = jnp.concatenate(
+            [
+                lax.dot_general(
+                    queries,
+                    received_ref[band + part, :tokens, :],
+                    CONTRACT_LANES,
+                    preferred_element_type=jnp.float32,
+                )
+                for part in range(3)
+            ],
+            axis=1,
+        ) + bias_ref[...]
         maximum = jnp.maximum(
             jnp.max(window, axis=-1, keepdims=True), jnp.max(context, axis=-1, keepdims=True)
         )
@@ -440,7 +510,7 @@
             preferred_element_type=jnp.float32,
         ) + jnp.dot(
             jnp.exp(window - maximum).astype(jnp.bfloat16),
-            ones_ref[band, :],
+            ones_ref[band * tokens : (band + 3) * tokens, :],
             preferred_element_type=jnp.float32,
         )
         attended = sums / swap_halves(sums)
@@ -449,26 +519,35 @@
             out_ref[block * parts + part] = jnp.where(
                 low, swap_halves(rows[: chunk // 2]), rows[chunk // 2 :]
             ).astype(jnp.bfloat16)
-        return carry
-
-    lax.fori_loop(0, blocks, body, 0)
-
-
-def output_kernel(
-    index_ref, attended_ref, latent_ref, gating_ref, gain_ref, *refs, sp_count, tp_count
-):
-    gate_refs, sources = refs[:tp_count], refs[tp_count : 2 * tp_count]
-    out_ref, gated_ref, weight_ref, semaphores = refs[2 * tp_count :]
+        own = pl.ds(block * parts, parts)
+        saves.append(pltpu.make_async_copy(out_ref.at[own], out_hbm.at[own], semaphores.at[block]))
+        saves[-1].start()
+    for save in saves:
+        save.wait()
+
+
+def output_kernel(attended_ref, *refs, sp_count, tp_count):
+    small = 3
+    gate_refs, refs = refs[:tp_count], refs[tp_count:]
+    sources, weights, refs = refs[:small], refs[small : small + tp_count], refs[small + tp_count :]
+    out_ref, gated_ref, weight_ref, *targets, semaphores = refs
+    pieces = (semaphores.shape[0] - small) // tp_count
+    depth = weight_ref.shape[1] // pieces
+    pairs = list(zip(sources, targets)) + [
+        (source.at[rows], weight_ref.at[index, rows])
+        for index, source in enumerate(weights)
+        for rows in (pl.ds(piece * depth, depth) for piece in range(pieces))
+    ]
     copies = [
-        pltpu.make_async_copy(source, weight_ref.at[index], semaphores.at[index])
-        for index, source in enumerate(sources)
+        pltpu.make_async_copy(source, target, semaphores.at[index])
+        for index, (source, target) in enumerate(pairs)
     ]
     for copy in copies:
         copy.start()
+    latent_ref, vectors_ref, gain_ref = targets
     half = attended_ref.shape[1]
-    total = None
-    for offset, copy in enumerate(copies):
-        group = index_ref[1] ^ offset
+    for offset in range(tp_count):
+        group = lax.axis_index("tp") ^ offset
         for pair in range(sp_count // 2):
             first = attended_ref[2 * pair * tp_count + group].astype(jnp.float32)
             second = attended_ref[(2 * pair + 1) * tp_count + group].astype(jnp.float32)
@@ -478,14 +557,22 @@
                 gated_ref[offset, side * half : (side + 1) * half, lanes] = (
                     gate / (1.0 + jnp.exp(-gate)) * block
                 ).astype(jnp.bfloat16)
+    total = None
+    for index, copy in enumerate(copies[small:]):
+        offset, piece = divmod(index, pieces)
+        rows = slice(piece * depth, (piece + 1) * depth)
         copy.wait()
-        term = jnp.dot(gated_ref[offset], weight_ref[offset], preferred_element_type=jnp.float32)
+        term = jnp.dot(
+            gated_ref[offset, :, rows], weight_ref[offset, rows, :], preferred_element_type=jnp.float32
+        )
         total = term if total is None else total + term
+    for copy in copies[:small]:
+        copy.wait()
     branch = total.astype(jnp.bfloat16).astype(jnp.float32)
     mean = jnp.sum(branch * branch, axis=-1, keepdims=True) * (1.0 / branch.shape[-1])
     out_ref[...] = (
         latent_ref[...].astype(jnp.float32)
-        + gating_ref[...] * (branch * lax.rsqrt(mean + EPSILON)) * gain_ref[...]
+        + vectors_ref[4:5, :] * (branch * lax.rsqrt(mean + EPSILON)) * gain_ref[:1, :]
     ).astype(jnp.bfloat16)
 
 
@@ -493,13 +580,16 @@
     return pltpu.with_memory_space_constraint(array, pltpu.VMEM)
 
 
-def call(kernel, out_shape, operands, scratch=(), scalars=0, raw=0, flops=0, mib=58):
-    vmem = pl.BlockSpec()
-    smem, hbm = pl.BlockSpec(memory_space=pltpu.SMEM), pl.BlockSpec(memory_space=pl.ANY)
+def call(kernel, out_shape, operands, scratch=(), raw=0, raw_outs=(), flops=0, mib=58):
+    vmem, hbm = pl.BlockSpec(), pl.BlockSpec(memory_space=pl.ANY)
+    single = not isinstance(out_shape, tuple)
+    out_specs = [
+        hbm if index in raw_outs else vmem for index in range(1 if single else len(out_shape))
+    ]
     return pl.pallas_call(
         kernel,
-        in_specs=[smem] * scalars + [vmem] * (len(operands) - scalars - raw) + [hbm] * raw,
-        out_specs=jax.tree.map(lambda _: vmem, out_shape),
+        in_specs=[vmem] * (len(operands) - raw) + [hbm] * raw,
+        out_specs=out_specs[0] if single else out_specs,
         out_shape=out_shape,
         scratch_shapes=scratch,
         cost_estimate=pl.CostEstimate(flops=flops, transcendentals=0, bytes_accessed=0),
@@ -524,14 +614,12 @@
     offset_bias,
     w_out,
 ):
-    sp_index = lax.axis_index("sp")
     tp_index = lax.axis_index("tp")
     sp_count, tp_count = lax.axis_size("sp"), lax.axis_size("tp")
-    indices = jnp.stack([sp_index, tp_index]).astype(jnp.int32)
     cols = w_shift.shape[1]
     tokens, model_width = latent.shape
     context_tokens = context.shape[0]
-    rows = tokens + context_tokens
+    rows = tokens + tokens // 2
     width = cols // LANES
     f32, bf16 = jnp.float32, jnp.bfloat16
     vmem = pltpu.VMEM
@@ -545,7 +633,6 @@
         partial_kernel,
         shape((sp_count * tp_count, 5 * width, LANES), bf16),
         (
-            indices,
             condition.reshape(-1, LANES),
             context_condition.reshape(-1, LANES),
             w_shift,
@@ -553,47 +640,99 @@
             w_gate,
         ),
         scratch=[vmem((2, model_width // LANES, LANES), f32)],
-        scalars=1,
     )
     terms = lax.all_to_all(terms, ("sp", "tp"), 0, 0, tiled=True)
     far = lax.ppermute(w_out, "tp", across)
     near = lax.ppermute(w_out, "tp", beside)
-    norm = call(norm_kernel, shape((rows, LANES), f32), (latent, context), flops=3 * 10**9)
-    table = lax.dynamic_index_in_dim(offset_bias, sp_index, 0, keepdims=False)
-    rows_of, cols_of = table.shape
-    centre = WIN_COLS - 1
-    gap = jnp.zeros((rows_of - 1, (LANES - 2 * cols_of) // 2), f32)
-    base = jnp.concatenate([table[:-1, centre:], gap, table[1:], gap, table[:-1, :centre]], axis=1)
-    pairs = call(bias_kernel, shape((rows_of - 1, GRID_W, LANES), f32), (base,), flops=3 * 10**9)
-    send, hidden, gating = call(
+    norm, gain, gain_after, context_half = call(
+        norm_kernel,
+        (
+            shape((tokens, LANES), f32),
+            shape((8, model_width), f32),
+            shape((8, model_width), f32),
+            shape((context_tokens // 2, model_width), bf16),
+        ),
+        (latent, gain_pre.reshape(1, -1), gain_post.reshape(1, -1), context),
+        raw=1,
+        scratch=[dma],
+        flops=3 * 10**9,
+    )
+    opposite = [(index, index ^ (sp_count // 2)) for index in range(sp_count)]
+    far_context = lax.ppermute(context_half, "sp", opposite)
+    offsets = offset_bias.shape[1]
+    pairs = call(
+        bias_kernel,
+        shape((offsets - 1, GRID_W, LANES), f32),
+        (jnp.transpose(offset_bias, (1, 0, 2)),),
+        scratch=[vmem((16, LANES), f32)],
+        flops=3 * 10**9,
+    )
+    send, hidden, vectors = call(
         functools.partial(project_kernel, sp_count=sp_count, tp_count=tp_count),
         (
-            shape((sp_count, rows + tokens // 2, LANES), bf16),
+            shape((sp_count, rows, LANES), bf16),
             shape((tokens, model_width), bf16),
-            shape((1, model_width), f32),
+            shape((8, model_width), f32),
         ),
-        (in_vmem(terms), gain_pre.reshape(1, -1), norm, context, latent, w_key, w_value, w_query),
-        raw=5,
+        (in_vmem(terms), latent, norm, gain, w_key, w_value, w_query),
+        raw=6,
+        raw_outs=(0, 1, 2),
         scratch=[
-            vmem((context_tokens, model_width), bf16),
-            vmem((tokens, model_width), bf16),
+            vmem(latent.shape, bf16),
+            vmem(norm.shape, f32),
+            vmem((8, model_width), f32),
             vmem(w_key.shape, bf16),
             vmem(w_value.shape, bf16),
             vmem(w_query.shape, bf16),
-            vmem((context_tokens, model_width), bf16),
+            vmem((sp_count, rows, LANES), bf16),
+            vmem(latent.shape, bf16),
             vmem((8, model_width), f32),
-            dma((5,)),
+            dma((6,)),
+            dma((4,)),
         ],
         flops=10**9,
     )
     received = lax.all_to_all(send, "sp", 0, 0, tiled=True)
+    group = sp_count // 2
+
+    def context_heads(*sources):
+        count = sum(source.shape[0] for source in sources)
+        return call(
+            functools.partial(context_kernel, sp_count=sp_count, sources=len(sources)),
+            (shape((count, LANES), bf16),) * group,
+            (*sources, vectors, gain, w_key, w_value),
+            raw=4,
+            raw_outs=tuple(range(group)),
+            scratch=[
+                vmem((8, model_width), f32),
+                vmem((8, model_width), f32),
+                vmem((model_width, cols // 2), bf16),
+                vmem((model_width, cols // 2), bf16),
+                vmem((count, model_width), bf16),
+                vmem((group, count, LANES), bf16),
+                dma((4,)),
+                dma((group,)),
+            ],
+            flops=10**9,
+        )
+
+    def context_exchange(parts):
+        return [parts[0]] + [
+            lax.ppermute(
+                parts[offset], "sp", [(index, index ^ offset) for index in range(sp_count)]
+            )
+            for offset in range(1, group)
+        ]
+
+    context_kv = context_exchange(context_heads(context))
+    near_context = lax.ppermute(far_context, "tp", beside)
+    context_kv += context_exchange(context_heads(in_vmem(far_context), in_vmem(near_context)))
     out_rows = tokens // tp_count
     gates = call(
         gate_kernel,
         (shape((out_rows, cols), bf16),) * tp_count,
-        (indices, hidden, w_silu),
+        (hidden, w_silu),
         scratch=[vmem((tokens, cols), f32)],
-        scalars=1,
         flops=10**9,
     )
     gates = [gates[0]] + [
@@ -604,14 +743,18 @@
     attended = call(
         attend_kernel,
         shape((sp_count * tp_count, out_rows // 2, LANES), bf16),
-        (in_vmem(received), pairs),
+        (in_vmem(received), *map(in_vmem, context_kv), pairs),
+        raw=1,
+        raw_outs=(0,),
         scratch=[
-            vmem((sp_count * tokens, LANES), bf16),
+            vmem(pairs.shape, f32),
+            vmem((sp_count * tp_count, out_rows // 2, LANES), bf16),
             vmem((sp_count * tokens, LANES), bf16),
             vmem((sp_count * context_tokens, LANES), bf16),
             vmem((sp_count * context_tokens, LANES), bf16),
             vmem((sp_count, tokens, LANES), bf16),
-            vmem((tokens, 3 * WIN_ROWS // 2 * GRID_W), f32),
+            vmem((tokens, 3 * tokens), f32),
+            dma((sp_count,)),
         ],
         flops=5 * 10**9,
     )
@@ -621,20 +764,25 @@
         functools.partial(output_kernel, sp_count=sp_count, tp_count=tp_count),
         shape((out_rows, model_width), bf16),
         (
-            indices,
             in_vmem(attended),
+            *map(in_vmem, gates),
             own_rows,
-            gating,
-            gain_post.reshape(1, -1),
-            *gates,
+            vectors,
+            gain_after,
             w_out,
             near,
             far,
             relayed,
         ),
-        scratch=[vmem((tp_count, out_rows, cols), bf16), vmem((tp_count, cols, model_width), bf16), dma((tp_count,))],
-        scalars=1,
-        raw=tp_count,
+        scratch=[
+            vmem((tp_count, out_rows, cols), bf16),
+            vmem((tp_count, cols, model_width), bf16),
+            vmem((out_rows, model_width), bf16),
+            vmem((8, model_width), f32),
+            vmem((8, model_width), f32),
+            dma((2 * tp_count + 3,)),
+        ],
+        raw=tp_count + 3,
         flops=10**9,
     )
 
@@ -666,8 +814,8 @@
         grid_rows = arrays[0].shape[0] // GRID_W
         one_head_each = (
             heads == sp_count
-            and sp_count >= 3
             and tp_count == 4
+            and sp_count == 8
             and head_width == HALF
             and GRID_W == HALF
             and 2 * grid_rows == WIN_ROWS

time: 121 us -> 139 us (1.15)
  starting transfers between devices: 19 us -> 28.5 us
  waiting for transfers between devices: 64.5 us -> 71.9 us
  Pallas kernels: 34.2 us -> 35.7 us
    ppermute x0 -> x8, waiting for transfers between devices: none -> 29.2 us  [the longest x1 28.1 us: shards_by_heads(): far_context = lax.ppermute(context_half, 'sp', opposite)]
    all_to_all x1, waiting for transfers between devices: 22.9 us -> 0.01 us  [shards_by_heads(): received = lax.all_to_all(send, 'sp', 0, 0, tiled=True)]
    ppermute x0 -> x8, starting transfers between devices: none -> 9.96 us  [the longest x6 7.11 us: context_exchange(): lax.ppermute(parts[offset], 'sp', [(index, index ^ offset) for index in r...]
    pallas_call x7 -> x9, Pallas kernels: 34.2 us -> 35.7 us  [call(): pl.pallas_call(kernel, in_specs=[vmem] * (len(operands) - raw) + [hbm] *...]
  transfers between devices with their start and end apart: 9 -> 17, of which waited for: 5 -> 7; matrix products, arithmetic and copies ran while one was open for 3% -> 1% of each run, Pallas kernels for 23% -> 22%
where the time goes in v3:
time: 139 us
  waiting for transfers between devices  71.9 us (52%)
  Pallas kernels  35.7 us (26%)
  starting transfers between devices  28.5 us (21%)
  local copies, waits for them, and re-layouts  2.53 us (2%)
    all_to_all x1, waiting for transfers between devices, shards_by_heads(): terms = lax.all_to_all(terms, ('sp', 'tp'), 0, 0, tiled=True)  39 us
    pallas_call x9, Pallas kernels, call(): pl.pallas_call(kernel, in_specs=[vmem] * (len(operands) - raw) + [hbm] *...  35.7 us
    ppermute x1, waiting for transfers between devices, shards_by_heads(): far_context = lax.ppermute(context_half, 'sp', opposite)  28.1 us
    ppermute x6, starting transfers between devices, context_exchange(): lax.ppermute(parts[offset], 'sp', [(index, index ^ offset) for index in r...  7.11 us
    all_to_all x1, starting transfers between devices, shards_by_heads(): terms = lax.all_to_all(terms, ('sp', 'tp'), 0, 0, tiled=True)  4.92 us
    all_to_all x1, starting transfers between devices, shards_by_heads(): received = lax.all_to_all(send, 'sp', 0, 0, tiled=True)  4.89 us
    all_to_all x1, starting transfers between devices, shards_by_heads(): attended = lax.all_to_all(attended, ('sp', 'tp'), 0, 0, tiled=True)  3.31 us
    ppermute x3, waiting for transfers between devices, shards_by_heads(): lax.ppermute(gates[offset], 'tp', [(index, index ^ offset) for index in r...  3.19 us
  transfers between devices with their start and end apart: 17, of which 7 were waited for; matrix products, arithmetic and copies ran while one was open for 1% of the time, Pallas kernels for 22%

profile of v3, /device:TPU:0, one launch (start us, length us, event | category | flops | bytes accessed | tf_op | source)
XLA Modules:
  0.0 138.7 jit_solution(1886483505997333210)
XLA Ops:
  0.0 3.0 %collective-permute-start.12 = (bf16[512,2048]{1,0:T(8,128)(2,1)}, bf16[512,2048]{1,0:T(8,128)(2,1)}, u32[]{:S(2)}, u32[]{:S(2)}) collective-permute-start(bf16[512,2048]{1,0:T(8,128)(2,1)} %refs_7_.1), channel_id=1, source_target_pairs={{0,2},{1,3},{2,0},{3,1},{4,6},{5,7},{6,4},{7,5},{8,10},{9,11},{10,... | collective-permute-start | bytes 6291464 | tf_op jit(solution)/shard_map/ppermute | solution.py:645
  3.0 2.2 %shard_map.145 = bf16[32,20,128]{2,1,0:T(8,128)(2,1)} custom-call(bf16[16,128]{1,0:T(8,128)(2,1)} %bitcast.5, bf16[16,128]{1,0:T(8,128)(2,1)} %bitcast.6, bf16[256,512]{1,0:T(8,128)(2,1)} %shift_ref.1, bf16[256,512]{1,0:T(8,128)(2,1)} %scale_ref.1, bf16[256,512]{1,0:T(8,128)(2,1)} %gate_ref.1), custom_call_target="tpu_custom_call" | custom-call | tf_op jit(solution)/shard_map/pallas_call | solution.py:589
  5.2 4.9 %all-to-all-start = ((bf16[32,20,128]{2,1,0:T(8,128)(2,1)}), bf16[32,20,128]{2,1,0:T(8,128)(2,1)S(1)}, u32[]{:S(2)}, u32[]{:S(2)}) async-start(bf16[32,20,128]{2,1,0:T(8,128)(2,1)} %shard_map.145), calls=%async_computation | async-start | bytes 393216 | tf_op jit(solution)/shard_map/all_to_all | solution.py:644
  10.1 3.0 %shard_map.146 = (f32[256,128]{1,0:T(8,128)}, f32[8,2048]{1,0:T(8,128)}, f32[8,2048]{1,0:T(8,128)}, bf16[64,2048]{1,0:T(8,128)(2,1)}) custom-call(bf16[256,2048]{1,0:T(8,128)(2,1)} %latent_hbm.1, f32[1,2048]{1,0:T(1,128)} %bitcast.8, f32[1,2048]{1,0:T(1,128)} %bitcast.9, bf16[128,2048]{1,0:T(8,128)(2,1)} %refs_0_.1), custom_call_target="tpu_custom_call" | custom-call | flops 3000000000 | tf_op jit(solution)/shard_map/pallas_call | solution.py:589
  13.1 39.0 %all-to-all-done.terms_ref = bf16[32,20,128]{2,1,0:T(8,128)(2,1)S(1)} async-done(((bf16[32,20,128]{2,1,0:T(8,128)(2,1)}), bf16[32,20,128]{2,1,0:T(8,128)(2,1)S(1)}, u32[]{:S(2)}, u32[]{:S(2)}) %all-to-all-start) | async-done | bytes 163872 | tf_op jit(solution)/shard_map/all_to_all | solution.py:644
  52.1 5.4 %shard_map.147 = (bf16[8,384,128]{2,1,0:T(8,128)(2,1)}, bf16[256,2048]{1,0:T(8,128)(2,1)}, f32[8,2048]{1,0:T(8,128)}) custom-call(bf16[32,20,128]{2,1,0:T(8,128)(2,1)S(1)} %all-to-all-done.terms_ref, bf16[256,2048]{1,0:T(8,128)(2,1)} %latent_hbm.1, f32[256,128]{1,0:T(8,128)} %get-tuple-element.24.norm_hbm, ...), custom_call_target="tpu_custom_call" | custom-call | flops 1000000000 | tf_op jit(solution)/shard_map/pallas_call | solution.py:589
  57.5 4.9 %all-to-all-start.1 = ((bf16[8,384,128]{2,1,0:T(8,128)(2,1)}), bf16[8,384,128]{2,1,0:T(8,128)(2,1)S(1)}, u32[]{:S(2)}, u32[]{:S(2)}) async-start(bf16[8,384,128]{2,1,0:T(8,128)(2,1)} %get-tuple-element.26), calls=%async_computation.1 | async-start | bytes 1572864 | tf_op jit(solution)/shard_map/all_to_all | solution.py:695
  63.0 2.9 %collective-permute-start.3 = (bf16[64,2048]{1,0:T(8,128)(2,1)S(1)}, bf16[64,2048]{1,0:T(8,128)(2,1)S(1)}, u32[]{:S(2)}, u32[]{:S(2)}) collective-permute-start(bf16[64,2048]{1,0:T(8,128)(2,1)S(1)} %copy-done.4), channel_id=1, source_target_pairs={{0,16},{4,20},{8,24},{12,28},{16,0},{20,4},{24,8},{28,12},{1,17},{... | collective-permute-start | bytes 786440 | tf_op jit(solution)/shard_map/ppermute | solution.py:661
  65.8 28.1 %collective-permute-done.3.refs_0_ = bf16[64,2048]{1,0:T(8,128)(2,1)S(1)} collective-permute-done((bf16[64,2048]{1,0:T(8,128)(2,1)S(1)}, bf16[64,2048]{1,0:T(8,128)(2,1)S(1)}, u32[]{:S(2)}, u32[]{:S(2)}) %collective-permute-start.3) | collective-permute-done | bytes 262176 | tf_op jit(solution)/shard_map/ppermute | solution.py:661
  94.0 4.1 %shard_map.148 = (bf16[128,128]{1,0:T(8,128)(2,1)}, bf16[128,128]{1,0:T(8,128)(2,1)}, bf16[128,128]{1,0:T(8,128)(2,1)}, bf16[128,128]{1,0:T(8,128)(2,1)}) custom-call(bf16[128,2048]{1,0:T(8,128)(2,1)} %refs_0_.1, f32[8,2048]{1,0:T(8,128)} %get-tuple-element.27.refs_1_.refs_2_.refs_5_, f32[8,2048]{1,0:T(8,128)} %get-tuple-element.25.gain_hbm.refs_2_.refs_3_, ...), custom_call_target="tpu_custom_call" | custom-call | flops 1000000000 | tf_op jit(solution)/shard_map/pallas_call | solution.py:589
  98.1 1.4 %collective-permute-start = (bf16[128,128]{1,0:T(8,128)(2,1)}, bf16[128,128]{1,0:T(8,128)(2,1)S(1)}, u32[]{:S(2)}, u32[]{:S(2)}) collective-permute-start(bf16[128,128]{1,0:T(8,128)(2,1)} %get-tuple-element.29), channel_id=1, source_target_pairs={{0,4},{4,0},{8,12},{12,8},{16,20},{20,16},{24,28},{28,24},{1,5},{5... | collective-permute-start | bytes 98312 | tf_op jit(solution)/shard_map/ppermute | solution.py:721
  99.5 2.1 %collective-permute-start.2 = (bf16[128,128]{1,0:T(8,128)(2,1)}, bf16[128,128]{1,0:T(8,128)(2,1)S(1)}, u32[]{:S(2)}, u32[]{:S(2)}) collective-permute-start(bf16[128,128]{1,0:T(8,128)(2,1)} %get-tuple-element.31), channel_id=1, source_target_pairs={{0,12},{4,8},{8,4},{12,0},{16,28},{20,24},{24,20},{28,16},{1,13},{... | collective-permute-start | bytes 98312 | tf_op jit(solution)/shard_map/ppermute | solution.py:721
  101.7 3.1 %shard_map.149 = (bf16[128,128]{1,0:T(8,128)(2,1)}, bf16[128,128]{1,0:T(8,128)(2,1)}, bf16[128,128]{1,0:T(8,128)(2,1)}, bf16[128,128]{1,0:T(8,128)(2,1)}) custom-call(bf16[64,2048]{1,0:T(8,128)(2,1)S(1)} %collective-permute-done.3.refs_0_, bf16[64,2048]{1,0:T(8,128)(2,1)S(1)} %collective-permute-done.4.refs_1_, ...), custom_call_target="tpu_custom_call" | custom-call | flops 1000000000 | tf_op jit(solution)/shard_map/pallas_call | solution.py:589
  104.8 1.4 %collective-permute-start.5 = (bf16[128,128]{1,0:T(8,128)(2,1)}, bf16[128,128]{1,0:T(8,128)(2,1)S(1)}, u32[]{:S(2)}, u32[]{:S(2)}) collective-permute-start(bf16[128,128]{1,0:T(8,128)(2,1)} %get-tuple-element.34), channel_id=1, source_target_pairs={{0,4},{4,0},{8,12},{12,8},{16,20},{20,16},{24,28},{28,24},{1,5},{5... | collective-permute-start | bytes 98312 | tf_op jit(solution)/shard_map/ppermute | solution.py:721
  106.2 2.1 %collective-permute-start.7 = (bf16[128,128]{1,0:T(8,128)(2,1)}, bf16[128,128]{1,0:T(8,128)(2,1)S(1)}, u32[]{:S(2)}, u32[]{:S(2)}) collective-permute-start(bf16[128,128]{1,0:T(8,128)(2,1)} %get-tuple-element.36), channel_id=1, source_target_pairs={{0,12},{4,8},{8,4},{12,0},{16,28},{20,24},{24,20},{28,16},{1,13},{... | collective-permute-start | bytes 98312 | tf_op jit(solution)/shard_map/ppermute | solution.py:721
  108.3 1.9 %shard_map.150.refs_8_ = f32[14,64,128]{2,1,0:T(8,128)} custom-call(f32[15,8,31]{2,1,0:T(8,128)} %bitcast.7), custom_call_target="tpu_custom_call" | custom-call | flops 3000000000 | tf_op jit(solution)/shard_map/pallas_call | solution.py:589
  111.3 7.6 %shard_map.151 = bf16[32,32,128]{2,1,0:T(8,128)(2,1)} custom-call(bf16[8,384,128]{2,1,0:T(8,128)(2,1)S(1)} %all-to-all-done.1.received_ref, bf16[128,128]{1,0:T(8,128)(2,1)S(1)} %copy-done.1, bf16[128,128]{1,0:T(8,128)(2,1)S(1)} %collective-permute-done.refs_1_, bf16[128,128]{1,0:T(8,128)(2,1)S(1)} %collective-permute-done.1.refs_2_, ...), custom_call_target="tpu_custom_call" | custom-call | flops 5000000000 | tf_op jit(solution)/shard_map/pallas_call | solution.py:589
  118.9 3.3 %all-to-all-start.2 = ((bf16[32,32,128]{2,1,0:T(8,128)(2,1)}), bf16[32,32,128]{2,1,0:T(8,128)(2,1)S(1)}, u32[]{:S(2)}, u32[]{:S(2)}) async-start(bf16[32,32,128]{2,1,0:T(8,128)(2,1)} %shard_map.151), calls=%async_computation.2 | async-start | bytes 524288 | tf_op jit(solution)/shard_map/all_to_all | solution.py:761
  122.2 3.4 %shard_map.152 = (bf16[64,512]{1,0:T(8,128)(2,1)}, bf16[64,512]{1,0:T(8,128)(2,1)}, bf16[64,512]{1,0:T(8,128)(2,1)}, bf16[64,512]{1,0:T(8,128)(2,1)}) custom-call(bf16[256,2048]{1,0:T(8,128)(2,1)} %get-tuple-element.37.hidden_ref, bf16[2048,512]{1,0:T(8,128)(2,1)} %weight_ref.1), custom_call_target="tpu_custom_call" | custom-call | flops 1000000000 | tf_op jit(solution)/shard_map/pallas_call | solution.py:589
  125.9 1.6 %collective-permute-start.9 = (bf16[64,512]{1,0:T(8,128)(2,1)}, bf16[64,512]{1,0:T(8,128)(2,1)S(1)}, u32[]{:S(2)}, u32[]{:S(2)}) collective-permute-start(bf16[64,512]{1,0:T(8,128)(2,1)} %get-tuple-element.40), channel_id=1, source_target_pairs={{0,2},{1,3},{2,0},{3,1},{4,6},{5,7},{6,4},{7,5},{8,10},{9,11},{10,... | collective-permute-start | bytes 196616 | tf_op jit(solution)/shard_map/ppermute | solution.py:739
  127.5 1.7 %constant_dynamic-slice_fusion.refs_4_ = bf16[64,2048]{1,0:T(8,128)(2,1)} fusion(bf16[256,2048]{1,0:T(8,128)(2,1)} %latent_hbm.1, s32[]{:T(128)S(6)} %select_n.3), kind=kLoop, calls=%fused_computation | loop fusion | bytes 524292 | tf_op jit(solution)/shard_map/dynamic_slice | solution.py:762
  129.2 1.8 %collective-permute-done.9.refs_2_ = bf16[64,512]{1,0:T(8,128)(2,1)S(1)} collective-permute-done((bf16[64,512]{1,0:T(8,128)(2,1)}, bf16[64,512]{1,0:T(8,128)(2,1)S(1)}, u32[]{:S(2)}, u32[]{:S(2)}) %collective-permute-start.9) | collective-permute-done | bytes 65568 | tf_op jit(solution)/shard_map/ppermute | solution.py:739
  131.0 1.4 collective-permute-done.10.refs_3_
  133.7 5.1 %shard_map.153 = bf16[64,2048]{1,0:T(8,128)(2,1)} custom-call(bf16[32,32,128]{2,1,0:T(8,128)(2,1)S(1)} %all-to-all-done.2.attended_ref, bf16[64,512]{1,0:T(8,128)(2,1)S(1)} %copy-done, bf16[64,512]{1,0:T(8,128)(2,1)S(1)} %collective-permute-done.8.refs_1_, bf16[64,512]{1,0:T(8,128)(2,1)S(1)} %collective-permute-done.9.refs_2_, ...), custom_call_target="tpu_custom_call" | custom-call | flops 1000000000 | tf_op jit(solution)/shard_map/pallas_call | solution.py:589
  (30 shorter events, 3.2 us)
Async XLA Ops:
  0.0 62.5 %collective-permute-start.12 = (bf16[512,2048]{1,0:T(8,128)(2,1)}, bf16[512,2048]{1,0:T(8,128)(2,1)}, u32[]{:S(2)}, u32[]{:S(2)}) collective-permute-start(bf16[512,2048]{1,0:T(8,128)(2,1)} %refs_7_.1), channel_id=1, source_target_pairs={{0,2},{1,3},{2,0},{3,1},{4,6},{5,7},{6,4},{7,5},{8,10},{9,11},{10,... | collective-permute-start | bytes 6291464 | tf_op jit(solution)/shard_map/ppermute | solution.py:645
  5.2 47.0 %all-to-all-start = ((bf16[32,20,128]{2,1,0:T(8,128)(2,1)}), bf16[32,20,128]{2,1,0:T(8,128)(2,1)S(1)}, u32[]{:S(2)}, u32[]{:S(2)}) async-start(bf16[32,20,128]{2,1,0:T(8,128)(2,1)} %shard_map.145), calls=%async_computation | async-start | bytes 393216 | tf_op jit(solution)/shard_map/all_to_all | solution.py:644
  52.1 10.3 %copy-start.3 = (bf16[512,2048]{1,0:T(8,128)(2,1)S(1)}, bf16[512,2048]{1,0:T(8,128)(2,1)}, u32[]{:S(2)}) copy-start(bf16[512,2048]{1,0:T(8,128)(2,1)} %refs_7_.1) | copy-start | bytes 6291460
  52.1 10.9 %copy-start.4 = (bf16[64,2048]{1,0:T(8,128)(2,1)S(1)}, bf16[64,2048]{1,0:T(8,128)(2,1)}, u32[]{:S(2)}) copy-start(bf16[64,2048]{1,0:T(8,128)(2,1)} %get-tuple-element.32) | copy-start | bytes 786436
  57.5 53.8 %all-to-all-start.1 = ((bf16[8,384,128]{2,1,0:T(8,128)(2,1)}), bf16[8,384,128]{2,1,0:T(8,128)(2,1)S(1)}, u32[]{:S(2)}, u32[]{:S(2)}) async-start(bf16[8,384,128]{2,1,0:T(8,128)(2,1)} %get-tuple-element.26), calls=%async_computation.1 | async-start | bytes 1572864 | tf_op jit(solution)/shard_map/all_to_all | solution.py:695
  62.4 70.0 %collective-permute-start.11 = (bf16[512,2048]{1,0:T(8,128)(2,1)S(1)}, bf16[512,2048]{1,0:T(8,128)(2,1)}, u32[]{:S(2)}, u32[]{:S(2)}) collective-permute-start(bf16[512,2048]{1,0:T(8,128)(2,1)S(1)} %copy-done.3), channel_id=1, source_target_pairs={{0,1},{1,0},{2,3},{3,2},{4,5},{5,4},{6,7},{7,6},{8,9},{9,8},{10,11... | collective-permute-start | bytes 6291464 | tf_op jit(solution)/shard_map/ppermute | solution.py:646
  62.5 70.3 %collective-permute-start.13 = (bf16[512,2048]{1,0:T(8,128)(2,1)}, bf16[512,2048]{1,0:T(8,128)(2,1)}, u32[]{:S(2)}, u32[]{:S(2)}) collective-permute-start(bf16[512,2048]{1,0:T(8,128)(2,1)} %collective-permute-done.12.refs_9_), channel_id=1, source_target_pairs={{0,1},{1,0},{2,3},{3,2},{4,5},{5,4},{6,7},{7,6},{8,9},{9,8},{10,11... | collective-permute-start | bytes 6291464 | tf_op jit(solution)/shard_map/ppermute | solution.py:742
  63.0 31.0 %collective-permute-start.3 = (bf16[64,2048]{1,0:T(8,128)(2,1)S(1)}, bf16[64,2048]{1,0:T(8,128)(2,1)S(1)}, u32[]{:S(2)}, u32[]{:S(2)}) collective-permute-start(bf16[64,2048]{1,0:T(8,128)(2,1)S(1)} %copy-done.4), channel_id=1, source_target_pairs={{0,16},{4,20},{8,24},{12,28},{16,0},{20,4},{24,8},{28,12},{1,17},{... | collective-permute-start | bytes 786440 | tf_op jit(solution)/shard_map/ppermute | solution.py:661
  94.0 5.6 %collective-permute-start.4 = (bf16[64,2048]{1,0:T(8,128)(2,1)S(1)}, bf16[64,2048]{1,0:T(8,128)(2,1)S(1)}, u32[]{:S(2)}, u32[]{:S(2)}) collective-permute-start(bf16[64,2048]{1,0:T(8,128)(2,1)S(1)} %collective-permute-done.3.refs_0_), channel_id=1, source_target_pairs={{0,1},{1,0},{2,3},{3,2},{4,5},{5,4},{6,7},{7,6},{8,9},{9,8},{10,11... | collective-permute-start | bytes 786440 | tf_op jit(solution)/shard_map/ppermute | solution.py:728
  98.1 6.6 %collective-permute-start = (bf16[128,128]{1,0:T(8,128)(2,1)}, bf16[128,128]{1,0:T(8,128)(2,1)S(1)}, u32[]{:S(2)}, u32[]{:S(2)}) collective-permute-start(bf16[128,128]{1,0:T(8,128)(2,1)} %get-tuple-element.29), channel_id=1, source_target_pairs={{0,4},{4,0},{8,12},{12,8},{16,20},{20,16},{24,28},{28,24},{1,5},{5... | collective-permute-start | bytes 98312 | tf_op jit(solution)/shard_map/ppermute | solution.py:721
  99.5 6.7 %collective-permute-start.1 = (bf16[128,128]{1,0:T(8,128)(2,1)}, bf16[128,128]{1,0:T(8,128)(2,1)S(1)}, u32[]{:S(2)}, u32[]{:S(2)}) collective-permute-start(bf16[128,128]{1,0:T(8,128)(2,1)} %get-tuple-element.30), channel_id=1, source_target_pairs={{0,8},{4,12},{8,0},{12,4},{16,24},{20,28},{24,16},{28,20},{1,9},{5... | collective-permute-start | bytes 98312 | tf_op jit(solution)/shard_map/ppermute | solution.py:721
  99.5 6.7 %collective-permute-start.2 = (bf16[128,128]{1,0:T(8,128)(2,1)}, bf16[128,128]{1,0:T(8,128)(2,1)S(1)}, u32[]{:S(2)}, u32[]{:S(2)}) collective-permute-start(bf16[128,128]{1,0:T(8,128)(2,1)} %get-tuple-element.31), channel_id=1, source_target_pairs={{0,12},{4,8},{8,4},{12,0},{16,28},{20,24},{24,20},{28,16},{1,13},{... | collective-permute-start | bytes 98312 | tf_op jit(solution)/shard_map/ppermute | solution.py:721
  104.8 5.5 %collective-permute-start.5 = (bf16[128,128]{1,0:T(8,128)(2,1)}, bf16[128,128]{1,0:T(8,128)(2,1)S(1)}, u32[]{:S(2)}, u32[]{:S(2)}) collective-permute-start(bf16[128,128]{1,0:T(8,128)(2,1)} %get-tuple-element.34), channel_id=1, source_target_pairs={{0,4},{4,0},{8,12},{12,8},{16,20},{20,16},{24,28},{28,24},{1,5},{5... | collective-permute-start | bytes 98312 | tf_op jit(solution)/shard_map/ppermute | solution.py:721
  106.2 4.1 %collective-permute-start.6 = (bf16[128,128]{1,0:T(8,128)(2,1)}, bf16[128,128]{1,0:T(8,128)(2,1)S(1)}, u32[]{:S(2)}, u32[]{:S(2)}) collective-permute-start(bf16[128,128]{1,0:T(8,128)(2,1)} %get-tuple-element.35), channel_id=1, source_target_pairs={{0,8},{4,12},{8,0},{12,4},{16,24},{20,28},{24,16},{28,20},{1,9},{5... | collective-permute-start | bytes 98312 | tf_op jit(solution)/shard_map/ppermute | solution.py:721
  106.2 5.1 %collective-permute-start.7 = (bf16[128,128]{1,0:T(8,128)(2,1)}, bf16[128,128]{1,0:T(8,128)(2,1)S(1)}, u32[]{:S(2)}, u32[]{:S(2)}) collective-permute-start(bf16[128,128]{1,0:T(8,128)(2,1)} %get-tuple-element.36), channel_id=1, source_target_pairs={{0,12},{4,8},{8,4},{12,0},{16,28},{20,24},{24,20},{28,16},{1,13},{... | collective-permute-start | bytes 98312 | tf_op jit(solution)/shard_map/ppermute | solution.py:721
  108.3 3.0 %copy-start.1 = (bf16[128,128]{1,0:T(8,128)(2,1)S(1)}, bf16[128,128]{1,0:T(8,128)(2,1)}, u32[]{:S(2)}) copy-start(bf16[128,128]{1,0:T(8,128)(2,1)} %get-tuple-element.28.refs_0_) | copy-start | bytes 98308
  108.3 3.0 %copy-start.2 = (bf16[128,128]{1,0:T(8,128)(2,1)S(1)}, bf16[128,128]{1,0:T(8,128)(2,1)}, u32[]{:S(2)}) copy-start(bf16[128,128]{1,0:T(8,128)(2,1)} %get-tuple-element.33.refs_4_) | copy-start | bytes 98308
  118.9 13.9 %all-to-all-start.2 = ((bf16[32,32,128]{2,1,0:T(8,128)(2,1)}), bf16[32,32,128]{2,1,0:T(8,128)(2,1)S(1)}, u32[]{:S(2)}, u32[]{:S(2)}) async-start(bf16[32,32,128]{2,1,0:T(8,128)(2,1)} %shard_map.151), calls=%async_computation.2 | async-start | bytes 524288 | tf_op jit(solution)/shard_map/all_to_all | solution.py:761
  125.6 3.6 %collective-permute-start.8 = (bf16[64,512]{1,0:T(8,128)(2,1)}, bf16[64,512]{1,0:T(8,128)(2,1)S(1)}, u32[]{:S(2)}, u32[]{:S(2)}) collective-permute-start(bf16[64,512]{1,0:T(8,128)(2,1)} %get-tuple-element.39), channel_id=1, source_target_pairs={{0,1},{1,0},{2,3},{3,2},{4,5},{5,4},{6,7},{7,6},{8,9},{9,8},{10,11... | collective-permute-start | bytes 196616 | tf_op jit(solution)/shard_map/ppermute | solution.py:739
  125.9 5.2 %collective-permute-start.9 = (bf16[64,512]{1,0:T(8,128)(2,1)}, bf16[64,512]{1,0:T(8,128)(2,1)S(1)}, u32[]{:S(2)}, u32[]{:S(2)}) collective-permute-start(bf16[64,512]{1,0:T(8,128)(2,1)} %get-tuple-element.40), channel_id=1, source_target_pairs={{0,2},{1,3},{2,0},{3,1},{4,6},{5,7},{6,4},{7,5},{8,10},{9,11},{10,... | collective-permute-start | bytes 196616 | tf_op jit(solution)/shard_map/ppermute | solution.py:739
  127.5 4.9 %collective-permute-start.10 = (bf16[64,512]{1,0:T(8,128)(2,1)}, bf16[64,512]{1,0:T(8,128)(2,1)S(1)}, u32[]{:S(2)}, u32[]{:S(2)}) collective-permute-start(bf16[64,512]{1,0:T(8,128)(2,1)} %get-tuple-element.41), channel_id=1, source_target_pairs={{0,3},{1,2},{2,1},{3,0},{4,7},{5,6},{6,5},{7,4},{8,11},{9,10},{10,... | collective-permute-start | bytes 196616 | tf_op jit(solution)/shard_map/ppermute | solution.py:739
  132.8 0.8 copy-start

commit v4 on v3

--- a/solution.py
+++ b/solution.py
@@ -301,6 +301,7 @@
     send_ref, hidden_ref, vectors_ref, loads, stores,
     *, sp_count, tp_count
 ):
+    half_cols = query_ref.shape[1] // 2
     copies = start_all(
         (
             (norm_hbm, norm_ref),
@@ -308,7 +309,8 @@
             (latent_hbm, latent_ref),
             (key_hbm, key_ref),
             (value_hbm, value_ref),
-            (query_hbm, query_ref),
+            (query_hbm.at[:, pl.ds(0, half_cols)], query_ref.at[:, pl.ds(0, half_cols)]),
+            (query_hbm.at[:, pl.ds(half_cols, half_cols)], query_ref.at[:, pl.ds(half_cols, half_cols)]),
         ),
         loads,
     )
@@ -346,11 +348,17 @@
         for head, kv in enumerate(head_pair(keys[:, lanes], values[:, lanes])):
             send_ref[2 * pair + head, :tokens, :] = kv.astype(jnp.bfloat16)
     save(send_ref.at[:, pl.ds(0, tokens)], send_hbm.at[:, pl.ds(0, tokens)])
-    copies[5].wait()
-    queries = jnp.dot(hidden_ref[...], query_ref[...], preferred_element_type=jnp.float32)
     for pair in range(width):
-        lanes = slice(pair * LANES, (pair + 1) * LANES)
-        block = queries[:, lanes].astype(jnp.bfloat16).astype(jnp.float32) * HALF**-0.5
+        if pair % (width // 2) == 0:
+            part = pair // (width // 2)
+            copies[5 + part].wait()
+            queries = jnp.dot(
+                hidden_ref[...],
+                query_ref[:, part * half_cols : (part + 1) * half_cols],
+                preferred_element_type=jnp.float32,
+            )
+        first = pair * LANES - part * half_cols
+        block = queries[:, first : first + LANES].astype(jnp.bfloat16).astype(jnp.float32) * HALF**-0.5
         for head, packed in enumerate(head_pair(block[:half], block[half:])):
             send_ref[2 * pair + head, tokens:, :] = packed.astype(jnp.bfloat16)
     save(send_ref.at[:, pl.ds(tokens, half)], send_hbm.at[:, pl.ds(tokens, half)])
@@ -526,12 +534,16 @@
         save.wait()
 
 
-def output_kernel(attended_ref, *refs, sp_count, tp_count):
+def output_kernel(attended_ref, own_weight_ref, *refs, sp_count, tp_count):
     small = 3
     gate_refs, refs = refs[:tp_count], refs[tp_count:]
-    sources, weights, refs = refs[:small], refs[small : small + tp_count], refs[small + tp_count :]
+    sources, refs = refs[:small], refs[small:]
+    weights, refs = refs[: tp_count - 1], refs[tp_count - 1 :]
     out_ref, gated_ref, weight_ref, *targets, semaphores = refs
-    pieces = (semaphores.shape[0] - small) // tp_count
+    count = targets[0].shape[0]
+    own = pl.ds(pl.multiple_of(lax.axis_index("tp") * count, count), count)
+    sources = (sources[0].at[own], *sources[1:])
+    pieces = (semaphores.shape[0] - small) // (tp_count - 1)
     depth = weight_ref.shape[1] // pieces
     pairs = list(zip(sources, targets)) + [
         (source.at[rows], weight_ref.at[index, rows])
@@ -557,15 +569,16 @@
                 gated_ref[offset, side * half : (side + 1) * half, lanes] = (
                     gate / (1.0 + jnp.exp(-gate)) * block
                 ).astype(jnp.bfloat16)
-    total = None
+    total = jnp.dot(gated_ref[0], own_weight_ref[...], preferred_element_type=jnp.float32)
     for index, copy in enumerate(copies[small:]):
         offset, piece = divmod(index, pieces)
         rows = slice(piece * depth, (piece + 1) * depth)
         copy.wait()
-        term = jnp.dot(
-            gated_ref[offset, :, rows], weight_ref[offset, rows, :], preferred_element_type=jnp.float32
-        )
-        total = term if total is None else total + term
+        total = total + jnp.dot(
+            gated_ref[1 + offset, :, rows],
+            weight_ref[offset, rows, :],
+            preferred_element_type=jnp.float32,
+        )
     for copy in copies[:small]:
         copy.wait()
     branch = total.astype(jnp.bfloat16).astype(jnp.float32)
@@ -614,7 +627,6 @@
     offset_bias,
     w_out,
 ):
-    tp_index = lax.axis_index("tp")
     sp_count, tp_count = lax.axis_size("sp"), lax.axis_size("tp")
     cols = w_shift.shape[1]
     tokens, model_width = latent.shape
@@ -687,7 +699,7 @@
             vmem((sp_count, rows, LANES), bf16),
             vmem(latent.shape, bf16),
             vmem((8, model_width), f32),
-            dma((6,)),
+            dma((7,)),
             dma((4,)),
         ],
         flops=10**9,
@@ -759,30 +771,29 @@
         flops=5 * 10**9,
     )
     attended = lax.all_to_all(attended, ("sp", "tp"), 0, 0, tiled=True)
-    own_rows = lax.dynamic_slice_in_dim(latent, tp_index * out_rows, out_rows, 0)
     return call(
         functools.partial(output_kernel, sp_count=sp_count, tp_count=tp_count),
         shape((out_rows, model_width), bf16),
         (
             in_vmem(attended),
+            in_vmem(w_out),
             *map(in_vmem, gates),
-            own_rows,
+            latent,
             vectors,
             gain_after,
-            w_out,
             near,
             far,
             relayed,
         ),
         scratch=[
             vmem((tp_count, out_rows, cols), bf16),
-            vmem((tp_count, cols, model_width), bf16),
+            vmem((tp_count - 1, cols, model_width), bf16),
             vmem((out_rows, model_width), bf16),
             vmem((8, model_width), f32),
             vmem((8, model_width), f32),
-            dma((2 * tp_count + 3,)),
+            dma((2 * tp_count + 1,)),
         ],
-        raw=tp_count + 3,
+        raw=tp_count + 2,
         flops=10**9,
     )
 

time: 139 us -> 139 us (level)
  waiting for transfers between devices: 71.9 us -> 73.6 us
  local copies, waits for them, and re-layouts: 2.53 us -> 0.86 us
    ppermute x3, waiting for transfers between devices: 3.19 us -> 4.87 us  [shards_by_heads(): lax.ppermute(gates[offset], 'tp', [(index, index ^ offset) for index in r...]
    dynamic_slice x1 -> x0, local copies, waits for them, and re-layouts: 1.67 us -> none  [shards_by_heads(): lax.dynamic_slice_in_dim(latent, tp_index * out_rows, out_rows, 0)]
  transfers between devices with their start and end apart: 17 -> 17, of which waited for: 7 -> 7; matrix products, arithmetic and copies ran while one was open for 1% -> 0% of each run, Pallas kernels for 22% -> 23%
where the time goes in v4:
time: 139 us
  waiting for transfers between devices  73.6 us (53%)
  Pallas kernels  35.8 us (26%)
  starting transfers between devices  28.5 us (21%)
    all_to_all x1, waiting for transfers between devices, shards_by_heads(): terms = lax.all_to_all(terms, ('sp', 'tp'), 0, 0, tiled=True)  39 us
    pallas_call x9, Pallas kernels, call(): pl.pallas_call(kernel, in_specs=[vmem] * (len(operands) - raw) + [hbm] *...  35.8 us
    ppermute x1, waiting for transfers between devices, shards_by_heads(): far_context = lax.ppermute(context_half, 'sp', opposite)  28.1 us
    ppermute x6, starting transfers between devices, context_exchange(): lax.ppermute(parts[offset], 'sp', [(index, index ^ offset) for index in r...  7.11 us
    all_to_all x1, starting transfers between devices, shards_by_heads(): terms = lax.all_to_all(terms, ('sp', 'tp'), 0, 0, tiled=True)  4.92 us
    all_to_all x1, starting transfers between devices, shards_by_heads(): received = lax.all_to_all(send, 'sp', 0, 0, tiled=True)  4.89 us
    ppermute x3, waiting for transfers between devices, shards_by_heads(): lax.ppermute(gates[offset], 'tp', [(index, index ^ offset) for index in r...  4.87 us
    all_to_all x1, starting transfers between devices, shards_by_heads(): attended = lax.all_to_all(attended, ('sp', 'tp'), 0, 0, tiled=True)  3.31 us
  transfers between devices with their start and end apart: 17, of which 7 were waited for; matrix products, arithmetic and copies ran while one was open for 0% of the time, Pallas kernels for 23%

profile of v4, /device:TPU:0, one launch (start us, length us, event | category | flops | bytes accessed | tf_op | source)
XLA Modules:
  0.0 138.9 jit_solution(11695530655091428740)
XLA Ops:
  0.0 3.0 %collective-permute-start.12 = (bf16[512,2048]{1,0:T(8,128)(2,1)}, bf16[512,2048]{1,0:T(8,128)(2,1)}, u32[]{:S(2)}, u32[]{:S(2)}) collective-permute-start(bf16[512,2048]{1,0:T(8,128)(2,1)} %own_weight_ref.1), channel_id=1, source_target_pairs={{0,2},{1,3},{2,0},{3,1},{4,6},{5,7},{6,4},{7,5},{8,10},{9,11},{10,... | collective-permute-start | bytes 6291464 | tf_op jit(solution)/shard_map/ppermute | solution.py:657
  3.0 2.2 %shard_map.145 = bf16[32,20,128]{2,1,0:T(8,128)(2,1)} custom-call(bf16[16,128]{1,0:T(8,128)(2,1)} %bitcast.5, bf16[16,128]{1,0:T(8,128)(2,1)} %bitcast.6, bf16[256,512]{1,0:T(8,128)(2,1)} %shift_ref.1, bf16[256,512]{1,0:T(8,128)(2,1)} %scale_ref.1, bf16[256,512]{1,0:T(8,128)(2,1)} %gate_ref.1), custom_call_target="tpu_custom_call" | custom-call | tf_op jit(solution)/shard_map/pallas_call | solution.py:602
  5.2 4.9 %all-to-all-start = ((bf16[32,20,128]{2,1,0:T(8,128)(2,1)}), bf16[32,20,128]{2,1,0:T(8,128)(2,1)S(1)}, u32[]{:S(2)}, u32[]{:S(2)}) async-start(bf16[32,20,128]{2,1,0:T(8,128)(2,1)} %shard_map.145), calls=%async_computation | async-start | bytes 393216 | tf_op jit(solution)/shard_map/all_to_all | solution.py:656
  10.1 3.0 %shard_map.146 = (f32[256,128]{1,0:T(8,128)}, f32[8,2048]{1,0:T(8,128)}, f32[8,2048]{1,0:T(8,128)}, bf16[64,2048]{1,0:T(8,128)(2,1)}) custom-call(bf16[256,2048]{1,0:T(8,128)(2,1)} %refs_4_.5, f32[1,2048]{1,0:T(1,128)} %bitcast.8, f32[1,2048]{1,0:T(1,128)} %bitcast.9, bf16[128,2048]{1,0:T(8,128)(2,1)} %refs_0_.1), custom_call_target="tpu_custom_call" | custom-call | flops 3000000000 | tf_op jit(solution)/shard_map/pallas_call | solution.py:602
  13.1 39.0 %all-to-all-done.terms_ref = bf16[32,20,128]{2,1,0:T(8,128)(2,1)S(1)} async-done(((bf16[32,20,128]{2,1,0:T(8,128)(2,1)}), bf16[32,20,128]{2,1,0:T(8,128)(2,1)S(1)}, u32[]{:S(2)}, u32[]{:S(2)}) %all-to-all-start) | async-done | bytes 163872 | tf_op jit(solution)/shard_map/all_to_all | solution.py:656
  52.1 6.1 %shard_map.147 = (bf16[8,384,128]{2,1,0:T(8,128)(2,1)}, bf16[256,2048]{1,0:T(8,128)(2,1)}, f32[8,2048]{1,0:T(8,128)}) custom-call(bf16[32,20,128]{2,1,0:T(8,128)(2,1)S(1)} %all-to-all-done.terms_ref, bf16[256,2048]{1,0:T(8,128)(2,1)} %refs_4_.5, f32[256,128]{1,0:T(8,128)} %get-tuple-element.24.norm_hbm, ...), custom_call_target="tpu_custom_call" | custom-call | flops 1000000000 | tf_op jit(solution)/shard_map/pallas_call | solution.py:602
  58.3 4.9 %all-to-all-start.1 = ((bf16[8,384,128]{2,1,0:T(8,128)(2,1)}), bf16[8,384,128]{2,1,0:T(8,128)(2,1)S(1)}, u32[]{:S(2)}, u32[]{:S(2)}) async-start(bf16[8,384,128]{2,1,0:T(8,128)(2,1)} %get-tuple-element.26), calls=%async_computation.1 | async-start | bytes 1572864 | tf_op jit(solution)/shard_map/all_to_all | solution.py:707
  63.7 2.9 %collective-permute-start.3 = (bf16[64,2048]{1,0:T(8,128)(2,1)S(1)}, bf16[64,2048]{1,0:T(8,128)(2,1)S(1)}, u32[]{:S(2)}, u32[]{:S(2)}) collective-permute-start(bf16[64,2048]{1,0:T(8,128)(2,1)S(1)} %copy-done.4), channel_id=1, source_target_pairs={{0,16},{4,20},{8,24},{12,28},{16,0},{20,4},{24,8},{28,12},{1,17},{... | collective-permute-start | bytes 786440 | tf_op jit(solution)/shard_map/ppermute | solution.py:673
  66.6 28.1 %collective-permute-done.3.refs_0_ = bf16[64,2048]{1,0:T(8,128)(2,1)S(1)} collective-permute-done((bf16[64,2048]{1,0:T(8,128)(2,1)S(1)}, bf16[64,2048]{1,0:T(8,128)(2,1)S(1)}, u32[]{:S(2)}, u32[]{:S(2)}) %collective-permute-start.3) | collective-permute-done | bytes 262176 | tf_op jit(solution)/shard_map/ppermute | solution.py:673
  94.7 4.1 %shard_map.148 = (bf16[128,128]{1,0:T(8,128)(2,1)}, bf16[128,128]{1,0:T(8,128)(2,1)}, bf16[128,128]{1,0:T(8,128)(2,1)}, bf16[128,128]{1,0:T(8,128)(2,1)}) custom-call(bf16[128,2048]{1,0:T(8,128)(2,1)} %refs_0_.1, f32[8,2048]{1,0:T(8,128)} %get-tuple-element.27.refs_1_.refs_2_.refs_5_, f32[8,2048]{1,0:T(8,128)} %get-tuple-element.25.gain_hbm.refs_2_.refs_3_, ...), custom_call_target="tpu_custom_call" | custom-call | flops 1000000000 | tf_op jit(solution)/shard_map/pallas_call | solution.py:602
  98.8 1.4 %collective-permute-start = (bf16[128,128]{1,0:T(8,128)(2,1)}, bf16[128,128]{1,0:T(8,128)(2,1)S(1)}, u32[]{:S(2)}, u32[]{:S(2)}) collective-permute-start(bf16[128,128]{1,0:T(8,128)(2,1)} %get-tuple-element.29), channel_id=1, source_target_pairs={{0,4},{4,0},{8,12},{12,8},{16,20},{20,16},{24,28},{28,24},{1,5},{5... | collective-permute-start | bytes 98312 | tf_op jit(solution)/shard_map/ppermute | solution.py:733
  100.3 2.1 %collective-permute-start.2 = (bf16[128,128]{1,0:T(8,128)(2,1)}, bf16[128,128]{1,0:T(8,128)(2,1)S(1)}, u32[]{:S(2)}, u32[]{:S(2)}) collective-permute-start(bf16[128,128]{1,0:T(8,128)(2,1)} %get-tuple-element.31), channel_id=1, source_target_pairs={{0,12},{4,8},{8,4},{12,0},{16,28},{20,24},{24,20},{28,16},{1,13},{... | collective-permute-start | bytes 98312 | tf_op jit(solution)/shard_map/ppermute | solution.py:733
  102.4 3.1 %shard_map.149 = (bf16[128,128]{1,0:T(8,128)(2,1)}, bf16[128,128]{1,0:T(8,128)(2,1)}, bf16[128,128]{1,0:T(8,128)(2,1)}, bf16[128,128]{1,0:T(8,128)(2,1)}) custom-call(bf16[64,2048]{1,0:T(8,128)(2,1)S(1)} %collective-permute-done.3.refs_0_, bf16[64,2048]{1,0:T(8,128)(2,1)S(1)} %collective-permute-done.4.refs_1_, ...), custom_call_target="tpu_custom_call" | custom-call | flops 1000000000 | tf_op jit(solution)/shard_map/pallas_call | solution.py:602
  105.5 1.4 %collective-permute-start.5 = (bf16[128,128]{1,0:T(8,128)(2,1)}, bf16[128,128]{1,0:T(8,128)(2,1)S(1)}, u32[]{:S(2)}, u32[]{:S(2)}) collective-permute-start(bf16[128,128]{1,0:T(8,128)(2,1)} %get-tuple-element.34), channel_id=1, source_target_pairs={{0,4},{4,0},{8,12},{12,8},{16,20},{20,16},{24,28},{28,24},{1,5},{5... | collective-permute-start | bytes 98312 | tf_op jit(solution)/shard_map/ppermute | solution.py:733
  107.0 2.1 %collective-permute-start.7 = (bf16[128,128]{1,0:T(8,128)(2,1)}, bf16[128,128]{1,0:T(8,128)(2,1)S(1)}, u32[]{:S(2)}, u32[]{:S(2)}) collective-permute-start(bf16[128,128]{1,0:T(8,128)(2,1)} %get-tuple-element.36), channel_id=1, source_target_pairs={{0,12},{4,8},{8,4},{12,0},{16,28},{20,24},{24,20},{28,16},{1,13},{... | collective-permute-start | bytes 98312 | tf_op jit(solution)/shard_map/ppermute | solution.py:733
  109.1 1.9 %shard_map.150.refs_8_ = f32[14,64,128]{2,1,0:T(8,128)} custom-call(f32[15,8,31]{2,1,0:T(8,128)} %bitcast.7), custom_call_target="tpu_custom_call" | custom-call | flops 3000000000 | tf_op jit(solution)/shard_map/pallas_call | solution.py:602
  111.1 1.0 collective-permute-done.7.refs_7_
  112.1 7.6 %shard_map.151 = bf16[32,32,128]{2,1,0:T(8,128)(2,1)} custom-call(bf16[8,384,128]{2,1,0:T(8,128)(2,1)S(1)} %all-to-all-done.1.received_ref, bf16[128,128]{1,0:T(8,128)(2,1)S(1)} %copy-done.2, bf16[128,128]{1,0:T(8,128)(2,1)S(1)} %collective-permute-done.refs_1_, bf16[128,128]{1,0:T(8,128)(2,1)S(1)} %collective-permute-done.1.refs_2_, ...), custom_call_target="tpu_custom_call" | custom-call | flops 5000000000 | tf_op jit(solution)/shard_map/pallas_call | solution.py:602
  119.7 3.3 %all-to-all-start.2 = ((bf16[32,32,128]{2,1,0:T(8,128)(2,1)}), bf16[32,32,128]{2,1,0:T(8,128)(2,1)S(1)}, u32[]{:S(2)}, u32[]{:S(2)}) async-start(bf16[32,32,128]{2,1,0:T(8,128)(2,1)} %shard_map.151), calls=%async_computation.2 | async-start | bytes 524288 | tf_op jit(solution)/shard_map/all_to_all | solution.py:773
  123.0 3.4 %shard_map.152 = (bf16[64,512]{1,0:T(8,128)(2,1)}, bf16[64,512]{1,0:T(8,128)(2,1)}, bf16[64,512]{1,0:T(8,128)(2,1)}, bf16[64,512]{1,0:T(8,128)(2,1)}) custom-call(bf16[256,2048]{1,0:T(8,128)(2,1)} %get-tuple-element.37.hidden_ref, bf16[2048,512]{1,0:T(8,128)(2,1)} %weight_ref.1), custom_call_target="tpu_custom_call" | custom-call | flops 1000000000 | tf_op jit(solution)/shard_map/pallas_call | solution.py:602
  126.6 1.6 %collective-permute-start.9 = (bf16[64,512]{1,0:T(8,128)(2,1)}, bf16[64,512]{1,0:T(8,128)(2,1)S(1)}, u32[]{:S(2)}, u32[]{:S(2)}) collective-permute-start(bf16[64,512]{1,0:T(8,128)(2,1)} %get-tuple-element.40), channel_id=1, source_target_pairs={{0,2},{1,3},{2,0},{3,1},{4,6},{5,7},{6,4},{7,5},{8,10},{9,11},{10,... | collective-permute-start | bytes 196616 | tf_op jit(solution)/shard_map/ppermute | solution.py:751
  128.2 3.5 %collective-permute-done.9.refs_2_ = bf16[64,512]{1,0:T(8,128)(2,1)S(1)} collective-permute-done((bf16[64,512]{1,0:T(8,128)(2,1)}, bf16[64,512]{1,0:T(8,128)(2,1)S(1)}, u32[]{:S(2)}, u32[]{:S(2)}) %collective-permute-start.9) | collective-permute-done | bytes 65568 | tf_op jit(solution)/shard_map/ppermute | solution.py:751
  131.7 1.4 collective-permute-done.10.refs_3_
  134.4 4.4 %shard_map.153 = bf16[64,2048]{1,0:T(8,128)(2,1)} custom-call(bf16[32,32,128]{2,1,0:T(8,128)(2,1)S(1)} %all-to-all-done.2.attended_ref, bf16[512,2048]{1,0:T(8,128)(2,1)S(1)} %copy-done, bf16[64,512]{1,0:T(8,128)(2,1)S(1)} %copy-done.1, bf16[64,512]{1,0:T(8,128)(2,1)S(1)} %collective-permute-done.8.refs_1_, ...), custom_call_target="tpu_custom_call" | custom-call | flops 1000000000 | tf_op jit(solution)/shard_map/pallas_call | solution.py:602
  (29 shorter events, 2.2 us)
Async XLA Ops:
  0.0 63.2 %collective-permute-start.12 = (bf16[512,2048]{1,0:T(8,128)(2,1)}, bf16[512,2048]{1,0:T(8,128)(2,1)}, u32[]{:S(2)}, u32[]{:S(2)}) collective-permute-start(bf16[512,2048]{1,0:T(8,128)(2,1)} %own_weight_ref.1), channel_id=1, source_target_pairs={{0,2},{1,3},{2,0},{3,1},{4,6},{5,7},{6,4},{7,5},{8,10},{9,11},{10,... | collective-permute-start | bytes 6291464 | tf_op jit(solution)/shard_map/ppermute | solution.py:657
  5.2 47.0 %all-to-all-start = ((bf16[32,20,128]{2,1,0:T(8,128)(2,1)}), bf16[32,20,128]{2,1,0:T(8,128)(2,1)S(1)}, u32[]{:S(2)}, u32[]{:S(2)}) async-start(bf16[32,20,128]{2,1,0:T(8,128)(2,1)} %shard_map.145), calls=%async_computation | async-start | bytes 393216 | tf_op jit(solution)/shard_map/all_to_all | solution.py:656
  52.1 11.0 %copy-start = (bf16[512,2048]{1,0:T(8,128)(2,1)S(1)}, bf16[512,2048]{1,0:T(8,128)(2,1)}, u32[]{:S(2)}) copy-start(bf16[512,2048]{1,0:T(8,128)(2,1)} %own_weight_ref.1) | copy-start | bytes 6291460
  52.1 11.6 %copy-start.4 = (bf16[64,2048]{1,0:T(8,128)(2,1)S(1)}, bf16[64,2048]{1,0:T(8,128)(2,1)}, u32[]{:S(2)}) copy-start(bf16[64,2048]{1,0:T(8,128)(2,1)} %get-tuple-element.32) | copy-start | bytes 786436
  58.3 53.8 %all-to-all-start.1 = ((bf16[8,384,128]{2,1,0:T(8,128)(2,1)}), bf16[8,384,128]{2,1,0:T(8,128)(2,1)S(1)}, u32[]{:S(2)}, u32[]{:S(2)}) async-start(bf16[8,384,128]{2,1,0:T(8,128)(2,1)} %get-tuple-element.26), calls=%async_computation.1 | async-start | bytes 1572864 | tf_op jit(solution)/shard_map/all_to_all | solution.py:707
  63.2 70.0 %collective-permute-start.11 = (bf16[512,2048]{1,0:T(8,128)(2,1)S(1)}, bf16[512,2048]{1,0:T(8,128)(2,1)}, u32[]{:S(2)}, u32[]{:S(2)}) collective-permute-start(bf16[512,2048]{1,0:T(8,128)(2,1)S(1)} %copy-done), channel_id=1, source_target_pairs={{0,1},{1,0},{2,3},{3,2},{4,5},{5,4},{6,7},{7,6},{8,9},{9,8},{10,11... | collective-permute-start | bytes 6291464 | tf_op jit(solution)/shard_map/ppermute | solution.py:658
  63.3 70.3 %collective-permute-start.13 = (bf16[512,2048]{1,0:T(8,128)(2,1)}, bf16[512,2048]{1,0:T(8,128)(2,1)}, u32[]{:S(2)}, u32[]{:S(2)}) collective-permute-start(bf16[512,2048]{1,0:T(8,128)(2,1)} %collective-permute-done.12.refs_8_), channel_id=1, source_target_pairs={{0,1},{1,0},{2,3},{3,2},{4,5},{5,4},{6,7},{7,6},{8,9},{9,8},{10,11... | collective-permute-start | bytes 6291464 | tf_op jit(solution)/shard_map/ppermute | solution.py:754
  63.7 31.0 %collective-permute-start.3 = (bf16[64,2048]{1,0:T(8,128)(2,1)S(1)}, bf16[64,2048]{1,0:T(8,128)(2,1)S(1)}, u32[]{:S(2)}, u32[]{:S(2)}) collective-permute-start(bf16[64,2048]{1,0:T(8,128)(2,1)S(1)} %copy-done.4), channel_id=1, source_target_pairs={{0,16},{4,20},{8,24},{12,28},{16,0},{20,4},{24,8},{28,12},{1,17},{... | collective-permute-start | bytes 786440 | tf_op jit(solution)/shard_map/ppermute | solution.py:673
  94.7 5.5 %collective-permute-start.4 = (bf16[64,2048]{1,0:T(8,128)(2,1)S(1)}, bf16[64,2048]{1,0:T(8,128)(2,1)S(1)}, u32[]{:S(2)}, u32[]{:S(2)}) collective-permute-start(bf16[64,2048]{1,0:T(8,128)(2,1)S(1)} %collective-permute-done.3.refs_0_), channel_id=1, source_target_pairs={{0,1},{1,0},{2,3},{3,2},{4,5},{5,4},{6,7},{7,6},{8,9},{9,8},{10,11... | collective-permute-start | bytes 786440 | tf_op jit(solution)/shard_map/ppermute | solution.py:740
  98.8 6.6 %collective-permute-start = (bf16[128,128]{1,0:T(8,128)(2,1)}, bf16[128,128]{1,0:T(8,128)(2,1)S(1)}, u32[]{:S(2)}, u32[]{:S(2)}) collective-permute-start(bf16[128,128]{1,0:T(8,128)(2,1)} %get-tuple-element.29), channel_id=1, source_target_pairs={{0,4},{4,0},{8,12},{12,8},{16,20},{20,16},{24,28},{28,24},{1,5},{5... | collective-permute-start | bytes 98312 | tf_op jit(solution)/shard_map/ppermute | solution.py:733
  100.3 6.7 %collective-permute-start.1 = (bf16[128,128]{1,0:T(8,128)(2,1)}, bf16[128,128]{1,0:T(8,128)(2,1)S(1)}, u32[]{:S(2)}, u32[]{:S(2)}) collective-permute-start(bf16[128,128]{1,0:T(8,128)(2,1)} %get-tuple-element.30), channel_id=1, source_target_pairs={{0,8},{4,12},{8,0},{12,4},{16,24},{20,28},{24,16},{28,20},{1,9},{5... | collective-permute-start | bytes 98312 | tf_op jit(solution)/shard_map/ppermute | solution.py:733
  100.3 6.7 %collective-permute-start.2 = (bf16[128,128]{1,0:T(8,128)(2,1)}, bf16[128,128]{1,0:T(8,128)(2,1)S(1)}, u32[]{:S(2)}, u32[]{:S(2)}) collective-permute-start(bf16[128,128]{1,0:T(8,128)(2,1)} %get-tuple-element.31), channel_id=1, source_target_pairs={{0,12},{4,8},{8,4},{12,0},{16,28},{20,24},{24,20},{28,16},{1,13},{... | collective-permute-start | bytes 98312 | tf_op jit(solution)/shard_map/ppermute | solution.py:733
  105.5 5.5 %collective-permute-start.5 = (bf16[128,128]{1,0:T(8,128)(2,1)}, bf16[128,128]{1,0:T(8,128)(2,1)S(1)}, u32[]{:S(2)}, u32[]{:S(2)}) collective-permute-start(bf16[128,128]{1,0:T(8,128)(2,1)} %get-tuple-element.34), channel_id=1, source_target_pairs={{0,4},{4,0},{8,12},{12,8},{16,20},{20,16},{24,28},{28,24},{1,5},{5... | collective-permute-start | bytes 98312 | tf_op jit(solution)/shard_map/ppermute | solution.py:733
  106.9 4.1 %collective-permute-start.6 = (bf16[128,128]{1,0:T(8,128)(2,1)}, bf16[128,128]{1,0:T(8,128)(2,1)S(1)}, u32[]{:S(2)}, u32[]{:S(2)}) collective-permute-start(bf16[128,128]{1,0:T(8,128)(2,1)} %get-tuple-element.35), channel_id=1, source_target_pairs={{0,8},{4,12},{8,0},{12,4},{16,24},{20,28},{24,16},{28,20},{1,9},{5... | collective-permute-start | bytes 98312 | tf_op jit(solution)/shard_map/ppermute | solution.py:733
  107.0 5.1 %collective-permute-start.7 = (bf16[128,128]{1,0:T(8,128)(2,1)}, bf16[128,128]{1,0:T(8,128)(2,1)S(1)}, u32[]{:S(2)}, u32[]{:S(2)}) collective-permute-start(bf16[128,128]{1,0:T(8,128)(2,1)} %get-tuple-element.36), channel_id=1, source_target_pairs={{0,12},{4,8},{8,4},{12,0},{16,28},{20,24},{24,20},{28,16},{1,13},{... | collective-permute-start | bytes 98312 | tf_op jit(solution)/shard_map/ppermute | solution.py:733
  109.1 3.0 %copy-start.2 = (bf16[128,128]{1,0:T(8,128)(2,1)S(1)}, bf16[128,128]{1,0:T(8,128)(2,1)}, u32[]{:S(2)}) copy-start(bf16[128,128]{1,0:T(8,128)(2,1)} %get-tuple-element.28.refs_0_) | copy-start | bytes 98308
  109.1 3.0 %copy-start.3 = (bf16[128,128]{1,0:T(8,128)(2,1)S(1)}, bf16[128,128]{1,0:T(8,128)(2,1)}, u32[]{:S(2)}) copy-start(bf16[128,128]{1,0:T(8,128)(2,1)} %get-tuple-element.33.refs_4_) | copy-start | bytes 98308
  119.7 13.9 %all-to-all-start.2 = ((bf16[32,32,128]{2,1,0:T(8,128)(2,1)}), bf16[32,32,128]{2,1,0:T(8,128)(2,1)S(1)}, u32[]{:S(2)}, u32[]{:S(2)}) async-start(bf16[32,32,128]{2,1,0:T(8,128)(2,1)} %shard_map.151), calls=%async_computation.2 | async-start | bytes 524288 | tf_op jit(solution)/shard_map/all_to_all | solution.py:773
  126.3 1.9 %collective-permute-start.8 = (bf16[64,512]{1,0:T(8,128)(2,1)}, bf16[64,512]{1,0:T(8,128)(2,1)S(1)}, u32[]{:S(2)}, u32[]{:S(2)}) collective-permute-start(bf16[64,512]{1,0:T(8,128)(2,1)} %get-tuple-element.39), channel_id=1, source_target_pairs={{0,1},{1,0},{2,3},{3,2},{4,5},{5,4},{6,7},{7,6},{8,9},{9,8},{10,11... | collective-permute-start | bytes 196616 | tf_op jit(solution)/shard_map/ppermute | solution.py:751
  126.6 5.1 %collective-permute-start.9 = (bf16[64,512]{1,0:T(8,128)(2,1)}, bf16[64,512]{1,0:T(8,128)(2,1)S(1)}, u32[]{:S(2)}, u32[]{:S(2)}) collective-permute-start(bf16[64,512]{1,0:T(8,128)(2,1)} %get-tuple-element.40), channel_id=1, source_target_pairs={{0,2},{1,3},{2,0},{3,1},{4,6},{5,7},{6,4},{7,5},{8,10},{9,11},{10,... | collective-permute-start | bytes 196616 | tf_op jit(solution)/shard_map/ppermute | solution.py:751
  128.2 4.9 %collective-permute-start.10 = (bf16[64,512]{1,0:T(8,128)(2,1)}, bf16[64,512]{1,0:T(8,128)(2,1)S(1)}, u32[]{:S(2)}, u32[]{:S(2)}) collective-permute-start(bf16[64,512]{1,0:T(8,128)(2,1)} %get-tuple-element.41), channel_id=1, source_target_pairs={{0,3},{1,2},{2,1},{3,0},{4,7},{5,6},{6,5},{7,4},{8,11},{9,10},{10,... | collective-permute-start | bytes 196616 | tf_op jit(solution)/shard_map/ppermute | solution.py:751
  133.6 0.8 copy-start.1

commit v5 on v4

--- a/solution.py
+++ b/solution.py
@@ -301,7 +301,6 @@
     send_ref, hidden_ref, vectors_ref, loads, stores,
     *, sp_count, tp_count
 ):
-    half_cols = query_ref.shape[1] // 2
     copies = start_all(
         (
             (norm_hbm, norm_ref),
@@ -309,8 +308,7 @@
             (latent_hbm, latent_ref),
             (key_hbm, key_ref),
             (value_hbm, value_ref),
-            (query_hbm.at[:, pl.ds(0, half_cols)], query_ref.at[:, pl.ds(0, half_cols)]),
-            (query_hbm.at[:, pl.ds(half_cols, half_cols)], query_ref.at[:, pl.ds(half_cols, half_cols)]),
+            (query_hbm, query_ref),
         ),
         loads,
     )
@@ -348,17 +346,11 @@
         for head, kv in enumerate(head_pair(keys[:, lanes], values[:, lanes])):
             send_ref[2 * pair + head, :tokens, :] = kv.astype(jnp.bfloat16)
     save(send_ref.at[:, pl.ds(0, tokens)], send_hbm.at[:, pl.ds(0, tokens)])
+    copies[5].wait()
+    queries = jnp.dot(hidden_ref[...], query_ref[...], preferred_element_type=jnp.float32)
     for pair in range(width):
-        if pair % (width // 2) == 0:
-            part = pair // (width // 2)
-            copies[5 + part].wait()
-            queries = jnp.dot(
-                hidden_ref[...],
-                query_ref[:, part * half_cols : (part + 1) * half_cols],
-                preferred_element_type=jnp.float32,
-            )
-        first = pair * LANES - part * half_cols
-        block = queries[:, first : first + LANES].astype(jnp.bfloat16).astype(jnp.float32) * HALF**-0.5
+        lanes = slice(pair * LANES, (pair + 1) * LANES)
+        block = queries[:, lanes].astype(jnp.bfloat16).astype(jnp.float32) * HALF**-0.5
         for head, packed in enumerate(head_pair(block[:half], block[half:])):
             send_ref[2 * pair + head, tokens:, :] = packed.astype(jnp.bfloat16)
     save(send_ref.at[:, pl.ds(tokens, half)], send_hbm.at[:, pl.ds(tokens, half)])
@@ -366,11 +358,11 @@
         copy.wait()
 
 
-def context_kernel(*refs, sp_count, sources):
+def context_kernel(*refs, sp_count, sources, copied):
     heads = sp_count // 2
     source_refs, (vectors_hbm, gain_hbm, key_hbm, value_hbm) = refs[:sources], refs[sources : sources + 4]
     outs, refs = refs[sources + 4 : sources + 4 + heads], refs[sources + 4 + heads :]
-    (vectors_ref, gain_ref, key_ref, value_ref, hidden_ref, send_ref, loads, stores) = refs
+    (vectors_ref, gain_ref, key_ref, value_ref, hidden_ref, send_ref, loads, stores, *rows_refs) = refs
     own = lax.axis_index("sp")
     width = key_ref.shape[1]
     cols = pl.ds(pl.multiple_of(own // heads * width, width), width)
@@ -378,20 +370,21 @@
         (
             (vectors_hbm, vectors_ref),
             (gain_hbm, gain_ref),
+            *(zip(source_refs, rows_refs) if copied else ()),
             (key_hbm.at[:, cols], key_ref),
             (value_hbm.at[:, cols], value_ref),
         ),
         loads,
     )
-    for copy in copies[:2]:
+    for copy in copies[:-2]:
         copy.wait()
     first = 0
-    for source in source_refs:
+    for source in rows_refs if copied else source_refs:
         modulate_rows(source, hidden_ref, first, source.shape[0], vectors_ref, gain_ref, 1)
         first += source.shape[0]
-    copies[2].wait()
+    copies[-2].wait()
     keys = jnp.dot(hidden_ref[...], key_ref[...], preferred_element_type=jnp.float32)
-    copies[3].wait()
+    copies[-1].wait()
     values = jnp.dot(hidden_ref[...], value_ref[...], preferred_element_type=jnp.float32)
     for pair in range(heads // 2):
         lanes = slice(pair * LANES, (pair + 1) * LANES)
@@ -485,18 +478,19 @@
         low = low_half(packed.shape)
         query_ref[block, :half, :] = jnp.where(low, packed, 0.0).astype(jnp.bfloat16)
         query_ref[block, half:, :] = jnp.where(low, swap_halves(packed), 0.0).astype(jnp.bfloat16)
-    for load in loads:
-        load.wait()
     low = low_half((chunk // 2, LANES))
     saves = []
     for block in range(blocks):
-        if block in (0, 1, blocks - 1):
-            fill_bias(bias_ref, pairs_ref, block, blocks)
         band = min(max(block - 1, 0), blocks - 3)
         queries = query_ref[block]
         context = lax.dot_general(
             queries, context_ref[...], CONTRACT_LANES, preferred_element_type=jnp.float32
         )
+        if block == 0:
+            for load in loads:
+                load.wait()
+        if block in (0, 1, blocks - 1):
+            fill_bias(bias_ref, pairs_ref, block, blocks)
         window = jnp.concatenate(
             [
                 lax.dot_general(
@@ -699,7 +693,7 @@
             vmem((sp_count, rows, LANES), bf16),
             vmem(latent.shape, bf16),
             vmem((8, model_width), f32),
-            dma((7,)),
+            dma((6,)),
             dma((4,)),
         ],
         flops=10**9,
@@ -707,13 +701,15 @@
     received = lax.all_to_all(send, "sp", 0, 0, tiled=True)
     group = sp_count // 2
 
-    def context_heads(*sources):
+    def context_heads(*sources, copied=False):
         count = sum(source.shape[0] for source in sources)
         return call(
-            functools.partial(context_kernel, sp_count=sp_count, sources=len(sources)),
+            functools.partial(
+                context_kernel, sp_count=sp_count, sources=len(sources), copied=copied
+            ),
             (shape((count, LANES), bf16),) * group,
             (*sources, vectors, gain, w_key, w_value),
-            raw=4,
+            raw=4 + copied * len(sources),
             raw_outs=tuple(range(group)),
             scratch=[
                 vmem((8, model_width), f32),
@@ -722,9 +718,10 @@
                 vmem((model_width, cols // 2), bf16),
                 vmem((count, model_width), bf16),
                 vmem((group, count, LANES), bf16),
-                dma((4,)),
+                dma((4 + copied * len(sources),)),
                 dma((group,)),
-            ],
+            ]
+            + [vmem(source.shape, bf16) for source in sources if copied],
             flops=10**9,
         )
 
@@ -736,7 +733,7 @@
             for offset in range(1, group)
         ]
 
-    context_kv = context_exchange(context_heads(context))
+    context_kv = context_exchange(context_heads(context, copied=True))
     near_context = lax.ppermute(far_context, "tp", beside)
     context_kv += context_exchange(context_heads(in_vmem(far_context), in_vmem(near_context)))
     out_rows = tokens // tp_count

time: 139 us -> 138 us (level)
  Pallas kernels: 35.8 us -> 34.2 us
    pallas_call x9, Pallas kernels: 35.8 us -> 34.2 us  [call(): pl.pallas_call(kernel, in_specs=[vmem] * (len(operands) - raw) + [hbm] *...]
  transfers between devices with their start and end apart: 17 -> 17, of which waited for: 7 -> 7; matrix products, arithmetic and copies ran while one was open for 0% -> 0% of each run, Pallas kernels for 23% -> 22%
where the time goes in v5:
time: 138 us; the launch traced here: 137 us
  waiting for transfers between devices  73.6 us (53%)
  Pallas kernels  34.2 us (25%)
  starting transfers between devices  28.5 us (21%)
    all_to_all x1, waiting for transfers between devices, shards_by_heads(): terms = lax.all_to_all(terms, ('sp', 'tp'), 0, 0, tiled=True)  39 us
    pallas_call x9, Pallas kernels, call(): pl.pallas_call(kernel, in_specs=[vmem] * (len(operands) - raw) + [hbm] *...  34.2 us
    ppermute x1, waiting for transfers between devices, shards_by_heads(): far_context = lax.ppermute(context_half, 'sp', opposite)  28.1 us
    ppermute x6, starting transfers between devices, context_exchange(): lax.ppermute(parts[offset], 'sp', [(index, index ^ offset) for index in r...  7.11 us
    all_to_all x1, starting transfers between devices, shards_by_heads(): terms = lax.all_to_all(terms, ('sp', 'tp'), 0, 0, tiled=True)  4.92 us
    all_to_all x1, starting transfers between devices, shards_by_heads(): received = lax.all_to_all(send, 'sp', 0, 0, tiled=True)  4.89 us
    ppermute x3, waiting for transfers between devices, shards_by_heads(): lax.ppermute(gates[offset], 'tp', [(index, index ^ offset) for index in r...  4.87 us
    all_to_all x1, starting transfers between devices, shards_by_heads(): attended = lax.all_to_all(attended, ('sp', 'tp'), 0, 0, tiled=True)  3.31 us
  transfers between devices with their start and end apart: 17, of which 7 were waited for; matrix products, arithmetic and copies ran while one was open for 0% of the time, Pallas kernels for 22%

profile of v5, /device:TPU:0, one launch (start us, length us, event | category | flops | bytes accessed | tf_op | source)
XLA Modules:
  0.0 137.2 jit_solution(10268045400080099292)
XLA Ops:
  0.0 3.0 %collective-permute-start.12 = (bf16[512,2048]{1,0:T(8,128)(2,1)}, bf16[512,2048]{1,0:T(8,128)(2,1)}, u32[]{:S(2)}, u32[]{:S(2)}) collective-permute-start(bf16[512,2048]{1,0:T(8,128)(2,1)} %own_weight_ref.1), channel_id=1, source_target_pairs={{0,2},{1,3},{2,0},{3,1},{4,6},{5,7},{6,4},{7,5},{8,10},{9,11},{10,... | collective-permute-start | bytes 6291464 | tf_op jit(solution)/shard_map/ppermute | solution.py:651
  3.0 2.2 %shard_map.145 = bf16[32,20,128]{2,1,0:T(8,128)(2,1)} custom-call(bf16[16,128]{1,0:T(8,128)(2,1)} %bitcast.5, bf16[16,128]{1,0:T(8,128)(2,1)} %bitcast.6, bf16[256,512]{1,0:T(8,128)(2,1)} %shift_ref.1, bf16[256,512]{1,0:T(8,128)(2,1)} %scale_ref.1, bf16[256,512]{1,0:T(8,128)(2,1)} %gate_ref.1), custom_call_target="tpu_custom_call" | custom-call | tf_op jit(solution)/shard_map/pallas_call | solution.py:596
  5.2 4.9 %all-to-all-start = ((bf16[32,20,128]{2,1,0:T(8,128)(2,1)}), bf16[32,20,128]{2,1,0:T(8,128)(2,1)S(1)}, u32[]{:S(2)}, u32[]{:S(2)}) async-start(bf16[32,20,128]{2,1,0:T(8,128)(2,1)} %shard_map.145), calls=%async_computation | async-start | bytes 393216 | tf_op jit(solution)/shard_map/all_to_all | solution.py:650
  10.1 3.0 %shard_map.146 = (f32[256,128]{1,0:T(8,128)}, f32[8,2048]{1,0:T(8,128)}, f32[8,2048]{1,0:T(8,128)}, bf16[64,2048]{1,0:T(8,128)(2,1)}) custom-call(bf16[256,2048]{1,0:T(8,128)(2,1)} %refs_4_.5, f32[1,2048]{1,0:T(1,128)} %bitcast.8, f32[1,2048]{1,0:T(1,128)} %bitcast.9, bf16[128,2048]{1,0:T(8,128)(2,1)} %refs_0_.1), custom_call_target="tpu_custom_call" | custom-call | flops 3000000000 | tf_op jit(solution)/shard_map/pallas_call | solution.py:596
  13.1 39.0 %all-to-all-done.terms_ref = bf16[32,20,128]{2,1,0:T(8,128)(2,1)S(1)} async-done(((bf16[32,20,128]{2,1,0:T(8,128)(2,1)}), bf16[32,20,128]{2,1,0:T(8,128)(2,1)S(1)}, u32[]{:S(2)}, u32[]{:S(2)}) %all-to-all-start) | async-done | bytes 163872 | tf_op jit(solution)/shard_map/all_to_all | solution.py:650
  52.1 5.4 %shard_map.147 = (bf16[8,384,128]{2,1,0:T(8,128)(2,1)}, bf16[256,2048]{1,0:T(8,128)(2,1)}, f32[8,2048]{1,0:T(8,128)}) custom-call(bf16[32,20,128]{2,1,0:T(8,128)(2,1)S(1)} %all-to-all-done.terms_ref, bf16[256,2048]{1,0:T(8,128)(2,1)} %refs_4_.5, f32[256,128]{1,0:T(8,128)} %get-tuple-element.24.norm_hbm, ...), custom_call_target="tpu_custom_call" | custom-call | flops 1000000000 | tf_op jit(solution)/shard_map/pallas_call | solution.py:596
  57.5 4.9 %all-to-all-start.1 = ((bf16[8,384,128]{2,1,0:T(8,128)(2,1)}), bf16[8,384,128]{2,1,0:T(8,128)(2,1)S(1)}, u32[]{:S(2)}, u32[]{:S(2)}) async-start(bf16[8,384,128]{2,1,0:T(8,128)(2,1)} %get-tuple-element.26), calls=%async_computation.1 | async-start | bytes 1572864 | tf_op jit(solution)/shard_map/all_to_all | solution.py:701
  63.0 2.9 %collective-permute-start.3 = (bf16[64,2048]{1,0:T(8,128)(2,1)S(1)}, bf16[64,2048]{1,0:T(8,128)(2,1)S(1)}, u32[]{:S(2)}, u32[]{:S(2)}) collective-permute-start(bf16[64,2048]{1,0:T(8,128)(2,1)S(1)} %copy-done.4), channel_id=1, source_target_pairs={{0,16},{4,20},{8,24},{12,28},{16,0},{20,4},{24,8},{28,12},{1,17},{... | collective-permute-start | bytes 786440 | tf_op jit(solution)/shard_map/ppermute | solution.py:667
  65.8 28.1 %collective-permute-done.3.refs_0_ = bf16[64,2048]{1,0:T(8,128)(2,1)S(1)} collective-permute-done((bf16[64,2048]{1,0:T(8,128)(2,1)S(1)}, bf16[64,2048]{1,0:T(8,128)(2,1)S(1)}, u32[]{:S(2)}, u32[]{:S(2)}) %collective-permute-start.3) | collective-permute-done | bytes 262176 | tf_op jit(solution)/shard_map/ppermute | solution.py:667
  94.0 3.3 %shard_map.148 = (bf16[128,128]{1,0:T(8,128)(2,1)}, bf16[128,128]{1,0:T(8,128)(2,1)}, bf16[128,128]{1,0:T(8,128)(2,1)}, bf16[128,128]{1,0:T(8,128)(2,1)}) custom-call(bf16[128,2048]{1,0:T(8,128)(2,1)} %refs_0_.1, f32[8,2048]{1,0:T(8,128)} %get-tuple-element.27.refs_1_.refs_2_.refs_5_, f32[8,2048]{1,0:T(8,128)} %get-tuple-element.25.gain_hbm.refs_2_.refs_3_, ...), custom_call_target="tpu_custom_call" | custom-call | flops 1000000000 | tf_op jit(solution)/shard_map/pallas_call | solution.py:596
  97.3 1.4 %collective-permute-start = (bf16[128,128]{1,0:T(8,128)(2,1)}, bf16[128,128]{1,0:T(8,128)(2,1)S(1)}, u32[]{:S(2)}, u32[]{:S(2)}) collective-permute-start(bf16[128,128]{1,0:T(8,128)(2,1)} %get-tuple-element.29), channel_id=1, source_target_pairs={{0,4},{4,0},{8,12},{12,8},{16,20},{20,16},{24,28},{28,24},{1,5},{5... | collective-permute-start | bytes 98312 | tf_op jit(solution)/shard_map/ppermute | solution.py:730
  98.8 2.1 %collective-permute-start.2 = (bf16[128,128]{1,0:T(8,128)(2,1)}, bf16[128,128]{1,0:T(8,128)(2,1)S(1)}, u32[]{:S(2)}, u32[]{:S(2)}) collective-permute-start(bf16[128,128]{1,0:T(8,128)(2,1)} %get-tuple-element.31), channel_id=1, source_target_pairs={{0,12},{4,8},{8,4},{12,0},{16,28},{20,24},{24,20},{28,16},{1,13},{... | collective-permute-start | bytes 98312 | tf_op jit(solution)/shard_map/ppermute | solution.py:730
  100.9 3.1 %shard_map.149 = (bf16[128,128]{1,0:T(8,128)(2,1)}, bf16[128,128]{1,0:T(8,128)(2,1)}, bf16[128,128]{1,0:T(8,128)(2,1)}, bf16[128,128]{1,0:T(8,128)(2,1)}) custom-call(bf16[64,2048]{1,0:T(8,128)(2,1)S(1)} %collective-permute-done.3.refs_0_, bf16[64,2048]{1,0:T(8,128)(2,1)S(1)} %collective-permute-done.4.refs_1_, ...), custom_call_target="tpu_custom_call" | custom-call | flops 1000000000 | tf_op jit(solution)/shard_map/pallas_call | solution.py:596
  104.0 1.4 %collective-permute-start.5 = (bf16[128,128]{1,0:T(8,128)(2,1)}, bf16[128,128]{1,0:T(8,128)(2,1)S(1)}, u32[]{:S(2)}, u32[]{:S(2)}) collective-permute-start(bf16[128,128]{1,0:T(8,128)(2,1)} %get-tuple-element.34), channel_id=1, source_target_pairs={{0,4},{4,0},{8,12},{12,8},{16,20},{20,16},{24,28},{28,24},{1,5},{5... | collective-permute-start | bytes 98312 | tf_op jit(solution)/shard_map/ppermute | solution.py:730
  105.4 2.1 %collective-permute-start.7 = (bf16[128,128]{1,0:T(8,128)(2,1)}, bf16[128,128]{1,0:T(8,128)(2,1)S(1)}, u32[]{:S(2)}, u32[]{:S(2)}) collective-permute-start(bf16[128,128]{1,0:T(8,128)(2,1)} %get-tuple-element.36), channel_id=1, source_target_pairs={{0,12},{4,8},{8,4},{12,0},{16,28},{20,24},{24,20},{28,16},{1,13},{... | collective-permute-start | bytes 98312 | tf_op jit(solution)/shard_map/ppermute | solution.py:730
  107.5 1.9 %shard_map.150.refs_8_ = f32[14,64,128]{2,1,0:T(8,128)} custom-call(f32[15,8,31]{2,1,0:T(8,128)} %bitcast.7), custom_call_target="tpu_custom_call" | custom-call | flops 3000000000 | tf_op jit(solution)/shard_map/pallas_call | solution.py:596
  109.5 1.0 collective-permute-done.7.refs_7_
  110.5 7.5 %shard_map.151 = bf16[32,32,128]{2,1,0:T(8,128)(2,1)} custom-call(bf16[8,384,128]{2,1,0:T(8,128)(2,1)S(1)} %all-to-all-done.1.received_ref, bf16[128,128]{1,0:T(8,128)(2,1)S(1)} %copy-done.2, bf16[128,128]{1,0:T(8,128)(2,1)S(1)} %collective-permute-done.refs_1_, bf16[128,128]{1,0:T(8,128)(2,1)S(1)} %collective-permute-done.1.refs_2_, ...), custom_call_target="tpu_custom_call" | custom-call | flops 5000000000 | tf_op jit(solution)/shard_map/pallas_call | solution.py:596
  118.0 3.3 %all-to-all-start.2 = ((bf16[32,32,128]{2,1,0:T(8,128)(2,1)}), bf16[32,32,128]{2,1,0:T(8,128)(2,1)S(1)}, u32[]{:S(2)}, u32[]{:S(2)}) async-start(bf16[32,32,128]{2,1,0:T(8,128)(2,1)} %shard_map.151), calls=%async_computation.2 | async-start | bytes 524288 | tf_op jit(solution)/shard_map/all_to_all | solution.py:770
  121.3 3.4 %shard_map.152 = (bf16[64,512]{1,0:T(8,128)(2,1)}, bf16[64,512]{1,0:T(8,128)(2,1)}, bf16[64,512]{1,0:T(8,128)(2,1)}, bf16[64,512]{1,0:T(8,128)(2,1)}) custom-call(bf16[256,2048]{1,0:T(8,128)(2,1)} %get-tuple-element.37.hidden_ref, bf16[2048,512]{1,0:T(8,128)(2,1)} %weight_ref.1), custom_call_target="tpu_custom_call" | custom-call | flops 1000000000 | tf_op jit(solution)/shard_map/pallas_call | solution.py:596
  124.9 1.6 %collective-permute-start.9 = (bf16[64,512]{1,0:T(8,128)(2,1)}, bf16[64,512]{1,0:T(8,128)(2,1)S(1)}, u32[]{:S(2)}, u32[]{:S(2)}) collective-permute-start(bf16[64,512]{1,0:T(8,128)(2,1)} %get-tuple-element.40), channel_id=1, source_target_pairs={{0,2},{1,3},{2,0},{3,1},{4,6},{5,7},{6,4},{7,5},{8,10},{9,11},{10,... | collective-permute-start | bytes 196616 | tf_op jit(solution)/shard_map/ppermute | solution.py:748
  126.6 3.5 %collective-permute-done.9.refs_2_ = bf16[64,512]{1,0:T(8,128)(2,1)S(1)} collective-permute-done((bf16[64,512]{1,0:T(8,128)(2,1)}, bf16[64,512]{1,0:T(8,128)(2,1)S(1)}, u32[]{:S(2)}, u32[]{:S(2)}) %collective-permute-start.9) | collective-permute-done | bytes 65568 | tf_op jit(solution)/shard_map/ppermute | solution.py:748
  130.1 1.4 collective-permute-done.10.refs_3_
  132.8 4.4 %shard_map.153 = bf16[64,2048]{1,0:T(8,128)(2,1)} custom-call(bf16[32,32,128]{2,1,0:T(8,128)(2,1)S(1)} %all-to-all-done.2.attended_ref, bf16[512,2048]{1,0:T(8,128)(2,1)S(1)} %copy-done, bf16[64,512]{1,0:T(8,128)(2,1)S(1)} %copy-done.1, bf16[64,512]{1,0:T(8,128)(2,1)S(1)} %collective-permute-done.8.refs_1_, ...), custom_call_target="tpu_custom_call" | custom-call | flops 1000000000 | tf_op jit(solution)/shard_map/pallas_call | solution.py:596
  (29 shorter events, 2.2 us)
Async XLA Ops:
  0.0 62.5 %collective-permute-start.12 = (bf16[512,2048]{1,0:T(8,128)(2,1)}, bf16[512,2048]{1,0:T(8,128)(2,1)}, u32[]{:S(2)}, u32[]{:S(2)}) collective-permute-start(bf16[512,2048]{1,0:T(8,128)(2,1)} %own_weight_ref.1), channel_id=1, source_target_pairs={{0,2},{1,3},{2,0},{3,1},{4,6},{5,7},{6,4},{7,5},{8,10},{9,11},{10,... | collective-permute-start | bytes 6291464 | tf_op jit(solution)/shard_map/ppermute | solution.py:651
  5.2 47.0 %all-to-all-start = ((bf16[32,20,128]{2,1,0:T(8,128)(2,1)}), bf16[32,20,128]{2,1,0:T(8,128)(2,1)S(1)}, u32[]{:S(2)}, u32[]{:S(2)}) async-start(bf16[32,20,128]{2,1,0:T(8,128)(2,1)} %shard_map.145), calls=%async_computation | async-start | bytes 393216 | tf_op jit(solution)/shard_map/all_to_all | solution.py:650
  52.1 10.3 %copy-start = (bf16[512,2048]{1,0:T(8,128)(2,1)S(1)}, bf16[512,2048]{1,0:T(8,128)(2,1)}, u32[]{:S(2)}) copy-start(bf16[512,2048]{1,0:T(8,128)(2,1)} %own_weight_ref.1) | copy-start | bytes 6291460
  52.1 10.9 %copy-start.4 = (bf16[64,2048]{1,0:T(8,128)(2,1)S(1)}, bf16[64,2048]{1,0:T(8,128)(2,1)}, u32[]{:S(2)}) copy-start(bf16[64,2048]{1,0:T(8,128)(2,1)} %get-tuple-element.32) | copy-start | bytes 786436
  57.5 53.0 %all-to-all-start.1 = ((bf16[8,384,128]{2,1,0:T(8,128)(2,1)}), bf16[8,384,128]{2,1,0:T(8,128)(2,1)S(1)}, u32[]{:S(2)}, u32[]{:S(2)}) async-start(bf16[8,384,128]{2,1,0:T(8,128)(2,1)} %get-tuple-element.26), calls=%async_computation.1 | async-start | bytes 1572864 | tf_op jit(solution)/shard_map/all_to_all | solution.py:701
  62.4 69.1 %collective-permute-start.11 = (bf16[512,2048]{1,0:T(8,128)(2,1)S(1)}, bf16[512,2048]{1,0:T(8,128)(2,1)}, u32[]{:S(2)}, u32[]{:S(2)}) collective-permute-start(bf16[512,2048]{1,0:T(8,128)(2,1)S(1)} %copy-done), channel_id=1, source_target_pairs={{0,1},{1,0},{2,3},{3,2},{4,5},{5,4},{6,7},{7,6},{8,9},{9,8},{10,11... | collective-permute-start | bytes 6291464 | tf_op jit(solution)/shard_map/ppermute | solution.py:652
  62.5 69.4 %collective-permute-start.13 = (bf16[512,2048]{1,0:T(8,128)(2,1)}, bf16[512,2048]{1,0:T(8,128)(2,1)}, u32[]{:S(2)}, u32[]{:S(2)}) collective-permute-start(bf16[512,2048]{1,0:T(8,128)(2,1)} %collective-permute-done.12.refs_8_), channel_id=1, source_target_pairs={{0,1},{1,0},{2,3},{3,2},{4,5},{5,4},{6,7},{7,6},{8,9},{9,8},{10,11... | collective-permute-start | bytes 6291464 | tf_op jit(solution)/shard_map/ppermute | solution.py:751
  63.0 31.0 %collective-permute-start.3 = (bf16[64,2048]{1,0:T(8,128)(2,1)S(1)}, bf16[64,2048]{1,0:T(8,128)(2,1)S(1)}, u32[]{:S(2)}, u32[]{:S(2)}) collective-permute-start(bf16[64,2048]{1,0:T(8,128)(2,1)S(1)} %copy-done.4), channel_id=1, source_target_pairs={{0,16},{4,20},{8,24},{12,28},{16,0},{20,4},{24,8},{28,12},{1,17},{... | collective-permute-start | bytes 786440 | tf_op jit(solution)/shard_map/ppermute | solution.py:667
  94.0 4.8 %collective-permute-start.4 = (bf16[64,2048]{1,0:T(8,128)(2,1)S(1)}, bf16[64,2048]{1,0:T(8,128)(2,1)S(1)}, u32[]{:S(2)}, u32[]{:S(2)}) collective-permute-start(bf16[64,2048]{1,0:T(8,128)(2,1)S(1)} %collective-permute-done.3.refs_0_), channel_id=1, source_target_pairs={{0,1},{1,0},{2,3},{3,2},{4,5},{5,4},{6,7},{7,6},{8,9},{9,8},{10,11... | collective-permute-start | bytes 786440 | tf_op jit(solution)/shard_map/ppermute | solution.py:737
  97.3 6.6 %collective-permute-start = (bf16[128,128]{1,0:T(8,128)(2,1)}, bf16[128,128]{1,0:T(8,128)(2,1)S(1)}, u32[]{:S(2)}, u32[]{:S(2)}) collective-permute-start(bf16[128,128]{1,0:T(8,128)(2,1)} %get-tuple-element.29), channel_id=1, source_target_pairs={{0,4},{4,0},{8,12},{12,8},{16,20},{20,16},{24,28},{28,24},{1,5},{5... | collective-permute-start | bytes 98312 | tf_op jit(solution)/shard_map/ppermute | solution.py:730
  98.7 6.7 %collective-permute-start.1 = (bf16[128,128]{1,0:T(8,128)(2,1)}, bf16[128,128]{1,0:T(8,128)(2,1)S(1)}, u32[]{:S(2)}, u32[]{:S(2)}) collective-permute-start(bf16[128,128]{1,0:T(8,128)(2,1)} %get-tuple-element.30), channel_id=1, source_target_pairs={{0,8},{4,12},{8,0},{12,4},{16,24},{20,28},{24,16},{28,20},{1,9},{5... | collective-permute-start | bytes 98312 | tf_op jit(solution)/shard_map/ppermute | solution.py:730
  98.8 6.7 %collective-permute-start.2 = (bf16[128,128]{1,0:T(8,128)(2,1)}, bf16[128,128]{1,0:T(8,128)(2,1)S(1)}, u32[]{:S(2)}, u32[]{:S(2)}) collective-permute-start(bf16[128,128]{1,0:T(8,128)(2,1)} %get-tuple-element.31), channel_id=1, source_target_pairs={{0,12},{4,8},{8,4},{12,0},{16,28},{20,24},{24,20},{28,16},{1,13},{... | collective-permute-start | bytes 98312 | tf_op jit(solution)/shard_map/ppermute | solution.py:730
  104.0 5.5 %collective-permute-start.5 = (bf16[128,128]{1,0:T(8,128)(2,1)}, bf16[128,128]{1,0:T(8,128)(2,1)S(1)}, u32[]{:S(2)}, u32[]{:S(2)}) collective-permute-start(bf16[128,128]{1,0:T(8,128)(2,1)} %get-tuple-element.34), channel_id=1, source_target_pairs={{0,4},{4,0},{8,12},{12,8},{16,20},{20,16},{24,28},{28,24},{1,5},{5... | collective-permute-start | bytes 98312 | tf_op jit(solution)/shard_map/ppermute | solution.py:730
  105.4 4.1 %collective-permute-start.6 = (bf16[128,128]{1,0:T(8,128)(2,1)}, bf16[128,128]{1,0:T(8,128)(2,1)S(1)}, u32[]{:S(2)}, u32[]{:S(2)}) collective-permute-start(bf16[128,128]{1,0:T(8,128)(2,1)} %get-tuple-element.35), channel_id=1, source_target_pairs={{0,8},{4,12},{8,0},{12,4},{16,24},{20,28},{24,16},{28,20},{1,9},{5... | collective-permute-start | bytes 98312 | tf_op jit(solution)/shard_map/ppermute | solution.py:730
  105.4 5.1 %collective-permute-start.7 = (bf16[128,128]{1,0:T(8,128)(2,1)}, bf16[128,128]{1,0:T(8,128)(2,1)S(1)}, u32[]{:S(2)}, u32[]{:S(2)}) collective-permute-start(bf16[128,128]{1,0:T(8,128)(2,1)} %get-tuple-element.36), channel_id=1, source_target_pairs={{0,12},{4,8},{8,4},{12,0},{16,28},{20,24},{24,20},{28,16},{1,13},{... | collective-permute-start | bytes 98312 | tf_op jit(solution)/shard_map/ppermute | solution.py:730
  107.5 3.0 %copy-start.2 = (bf16[128,128]{1,0:T(8,128)(2,1)S(1)}, bf16[128,128]{1,0:T(8,128)(2,1)}, u32[]{:S(2)}) copy-start(bf16[128,128]{1,0:T(8,128)(2,1)} %get-tuple-element.28.refs_0_) | copy-start | bytes 98308
  107.5 3.0 %copy-start.3 = (bf16[128,128]{1,0:T(8,128)(2,1)S(1)}, bf16[128,128]{1,0:T(8,128)(2,1)}, u32[]{:S(2)}) copy-start(bf16[128,128]{1,0:T(8,128)(2,1)} %get-tuple-element.33.refs_4_) | copy-start | bytes 98308
  118.0 13.9 %all-to-all-start.2 = ((bf16[32,32,128]{2,1,0:T(8,128)(2,1)}), bf16[32,32,128]{2,1,0:T(8,128)(2,1)S(1)}, u32[]{:S(2)}, u32[]{:S(2)}) async-start(bf16[32,32,128]{2,1,0:T(8,128)(2,1)} %shard_map.151), calls=%async_computation.2 | async-start | bytes 524288 | tf_op jit(solution)/shard_map/all_to_all | solution.py:770
  124.7 1.9 %collective-permute-start.8 = (bf16[64,512]{1,0:T(8,128)(2,1)}, bf16[64,512]{1,0:T(8,128)(2,1)S(1)}, u32[]{:S(2)}, u32[]{:S(2)}) collective-permute-start(bf16[64,512]{1,0:T(8,128)(2,1)} %get-tuple-element.39), channel_id=1, source_target_pairs={{0,1},{1,0},{2,3},{3,2},{4,5},{5,4},{6,7},{7,6},{8,9},{9,8},{10,11... | collective-permute-start | bytes 196616 | tf_op jit(solution)/shard_map/ppermute | solution.py:748
  124.9 5.1 %collective-permute-start.9 = (bf16[64,512]{1,0:T(8,128)(2,1)}, bf16[64,512]{1,0:T(8,128)(2,1)S(1)}, u32[]{:S(2)}, u32[]{:S(2)}) collective-permute-start(bf16[64,512]{1,0:T(8,128)(2,1)} %get-tuple-element.40), channel_id=1, source_target_pairs={{0,2},{1,3},{2,0},{3,1},{4,6},{5,7},{6,4},{7,5},{8,10},{9,11},{10,... | collective-permute-start | bytes 196616 | tf_op jit(solution)/shard_map/ppermute | solution.py:748
  126.6 4.9 %collective-permute-start.10 = (bf16[64,512]{1,0:T(8,128)(2,1)}, bf16[64,512]{1,0:T(8,128)(2,1)S(1)}, u32[]{:S(2)}, u32[]{:S(2)}) collective-permute-start(bf16[64,512]{1,0:T(8,128)(2,1)} %get-tuple-element.41), channel_id=1, source_target_pairs={{0,3},{1,2},{2,1},{3,0},{4,7},{5,6},{6,5},{7,4},{8,11},{9,10},{10,... | collective-permute-start | bytes 196616 | tf_op jit(solution)/shard_map/ppermute | solution.py:748
  131.9 0.8 copy-start.1
